TPU v7x, 512 devices: a whole 4x4x16 slice. The times are simulated.
512 devices in a mesh: sp: 256 (over z, y, x), tp: 2 (over core).
Axes of the slice: x: 4, y: 4, z: 16, core: 2. Of those that a mesh axis runs over, the one named last changes fastest.
Arguments:
- query_rows: bfloat16 [65536, 1024], P('sp', 'tp'), may hold values from -6 to 6
- key_rows: bfloat16 [65536, 1024], P('sp', 'tp'), may hold values from -6 to 6
- value_rows: bfloat16 [65536, 1024], P('sp', 'tp'), may hold values from -6 to 6
- out_weight: bfloat16 [1024, 2048], P('tp'), may hold values from -0.75 to 0.75
Outputs:
- layer_out: bfloat16 [65536, 2048], P(('sp', 'tp'))
All inputs are finite; a program needn't handle non-finite values.
Results may differ from a plain program's by a relative error of at most 0.012.
Values may be sent and summed in bfloat16 or wider, within the bound.
No kernel may reach another device: no remote copies, remote signals or barrier semaphores. Data moves between devices by JAX's collectives and lax.ppermute only.
A program may use at most 64 MiB of HBM per device.

v0:
```python
import functools
import math

import jax
import jax.numpy as jnp
import numpy as np
from jax import lax
from jax.experimental import pallas as pl
from jax.experimental.pallas import tpu as pltpu
from jax.sharding import Mesh, PartitionSpec as P


HD = 64
BACK = 128
THETA = 500000.0
TOK = 256
GROUP = 8
SP = ("z", "g", "b", "x")
NEG = -1e30
BF = jnp.bfloat16
F32 = jnp.float32


def row_tokens():
    p = np.arange(TOK)
    residue4, a, n = p // 64, (p % 64) // 16, p % 16
    return 16 * n + residue4 + 4 * a


def make_tables(blocks):
    t = row_tokens()
    inverse = np.float64(THETA) ** (-np.arange(32, dtype=np.float64) / 32)
    lanes = inverse[np.arange(128) % 32]
    inner = t[:, None] * lanes[None, :]
    fine = np.arange(16) * TOK
    coarse = np.arange(blocks // 16) * (16 * TOK)
    anchor = np.concatenate([fine, coarse])[:, None] * lanes[None, :]
    anchors = np.concatenate([np.cos(anchor), np.sin(anchor)], axis=1)
    perm = np.zeros((TOK, TOK), np.float32)
    perm[np.arange(TOK), t] = 1.0

    def band(query, key):
        distance = query[:, None] - key[None, :]
        return np.where((distance >= 0) & (distance <= BACK), 0.0, NEG).astype(np.float32)

    mask1 = band(t, np.concatenate([t - TOK, t]))
    row = np.arange(64)
    sub = 4 * (row % 16) + row // 16
    query4 = np.concatenate([sub, sub + 64])
    mask4 = band(query4, np.concatenate([query4 - 128, query4]))
    query16 = np.arange(128)
    mask16 = band(query16, np.concatenate([query16 - 128, query16]))
    return dict(
        cos=np.cos(inner).astype(np.float32),
        sin=np.sin(inner).astype(np.float32),
        anchors=anchors.astype(np.float32),
        perm=perm,
        mask1=mask1,
        mask4=mask4,
        mask16=mask16,
    )


def dot(a, b):
    return lax.dot_general(a, b, (((1,), (0,)), ((), ())), preferred_element_type=F32)


def dot_t(a, b):
    return lax.dot_general(a, b, (((1,), (1,)), ((), ())), preferred_element_type=F32)


def half(rows):
    return lax.broadcasted_iota(jnp.int32, (rows, 128), 1) < 64


def pack_kernel(index_ref, q_ref, k_ref, v_ref, perm_ref, cos_ref, sin_ref, anchor_ref, out_ref):
    block = index_ref[0]
    fine = anchor_ref[pl.ds(block % 16, 1), :]
    coarse = anchor_ref[pl.ds(16 + block // 16, 1), :]
    cos_a = fine[:, :128] * coarse[:, :128] - fine[:, 128:] * coarse[:, 128:]
    sin_a = fine[:, 128:] * coarse[:, :128] + fine[:, :128] * coarse[:, 128:]
    lane = lax.broadcasted_iota(jnp.int32, (TOK, 128), 1)
    low64 = lane < 64
    low32 = (lane & 63) < 32
    sign = jnp.where(low32[:1], -1.0, 1.0).astype(F32)
    cosine = cos_a * cos_ref[...] - sin_a * sin_ref[...]
    sine = (sin_a * sign) * cos_ref[...] + (cos_a * sign) * sin_ref[...]

    def turn(rows):
        other = jnp.where(low32, pltpu.roll(rows, 96, 1), pltpu.roll(rows, 32, 1))
        return rows * cosine + other * sine

    perm = perm_ref[...]
    for j in range(4):
        cols = slice(128 * j, 128 * j + 128)
        query = turn(dot(perm, q_ref[:, cols])) * (1.0 / math.sqrt(HD))
        key = turn(dot(perm, k_ref[:, cols]))
        value = dot(perm, v_ref[:, cols])
        out_ref[2 * j, 0:TOK] = jnp.where(low64, key, pltpu.roll(value, 64, 1)).astype(BF)
        out_ref[2 * j + 1, 0:TOK] = jnp.where(low64, pltpu.roll(key, 64, 1), value).astype(BF)
        first, second = query[:128], query[128:]
        out_ref[2 * j, TOK : TOK + 128] = jnp.where(low64[:128], first, pltpu.roll(second, 64, 1)).astype(BF)
        out_ref[2 * j + 1, TOK : TOK + 128] = jnp.where(low64[:128], pltpu.roll(first, 64, 1), second).astype(BF)


def wide(x, n):
    return jnp.concatenate([x] * n, axis=1) if n > 1 else x


def lane_of(x, lane):
    return jnp.broadcast_to(x[:, lane : lane + 1], x.shape)


def value_masks(rows):
    low = half(rows)
    return jnp.where(low, 1.0, 0.0).astype(BF), jnp.where(low, 0.0, 1.0).astype(BF)


def stamp(total, peak):
    lane = lax.broadcasted_iota(jnp.int32, total.shape, 1)
    return jnp.where((lane >= 32) & (lane < 64), peak, total)


def fresh(query, keys, values, mask):
    scores = dot_t(query, keys) + mask
    peak = jnp.broadcast_to(jnp.max(scores, axis=1, keepdims=True), (scores.shape[0], 128))
    probs = jnp.exp(scores - wide(peak, scores.shape[1] // 128)).astype(BF)
    return dot(probs, values), peak


def merge(state, query, keys, values, mask):
    scores = dot_t(query, keys) + mask
    before = lane_of(state, 32)
    peak = jnp.maximum(before, jnp.max(scores, axis=1, keepdims=True))
    probs = jnp.exp(scores - wide(peak, scores.shape[1] // 128)).astype(BF)
    return state * jnp.exp(before - peak) + dot(probs, values), peak


def own_kernel(own_ref, mask1_ref, mask4_ref, mask16_ref, acc_ref, qs_ref, vown):
    low256, high256 = value_masks(TOK)
    low_bf = low256[:128]
    for i in range(GROUP):
        packed = own_ref[i, TOK : TOK + 128]
        qs_ref[i, 0:128] = packed * low_bf
        qs_ref[i, 128:256] = pltpu.roll(packed.astype(F32), 64, 1).astype(BF) * low_bf
        vown[i] = own_ref[i, 0:TOK] * high256 + low256
    for r in range(16):
        rows = slice(16 * r, 16 * r + 16)
        total, peak = fresh(
            qs_ref[:, rows].reshape(128, 128),
            own_ref[:, rows].reshape(128, 128),
            vown[:, rows].reshape(128, 128),
            mask16_ref[:, 128:256],
        )
        acc_ref[:, rows] = stamp(total, peak).reshape(8, 16, 128)
    for b in range(4):
        for r in range(4):
            rows = slice(64 * r, 64 * r + 64)
            at = slice(2 * b, 2 * b + 2)
            seen = slice(max(0, 2 * b - 2), 2 * b + 2)
            n = 64 * (seen.stop - seen.start)
            total, peak = merge(
                acc_ref[at, rows].reshape(128, 128),
                qs_ref[at, rows].reshape(128, 128),
                own_ref[seen, rows].reshape(n, 128),
                vown[seen, rows].reshape(n, 128),
                mask4_ref[:, 256 - n : 256],
            )
            acc_ref[at, rows] = stamp(total, peak).reshape(2, 64, 128)
    for i in range(GROUP):
        first = max(0, i - 1)
        n = TOK * (i + 1 - first)
        total, peak = merge(
            acc_ref[i],
            qs_ref[i],
            own_ref[first : i + 1, 0:TOK].reshape(n, 128),
            vown[first : i + 1].reshape(n, 128),
            mask1_ref[:, 2 * TOK - n : 2 * TOK],
        )
        acc_ref[i] = stamp(total, peak)


def halo_rows(index_ref, acc_ref, qs_ref, halo_ref, vhalo, mask4_ref, mask16_ref, new_ref, base):
    bias = jnp.where(index_ref[0] < GROUP, NEG, 0.0).astype(F32)
    low, high = value_masks(128)
    for i in range(GROUP):
        vhalo[i] = halo_ref[i] * high + low
    mask16 = mask16_ref[:, 0:128] + bias
    for r in range(8):
        rows = slice(16 * r, 16 * r + 16)
        full = slice(base + 16 * r, base + 16 * r + 16)
        total, peak = merge(
            acc_ref[:, full].reshape(128, 128),
            qs_ref[:, full].reshape(128, 128),
            halo_ref[:, rows].reshape(128, 128),
            vhalo[:, rows].reshape(128, 128),
            mask16,
        )
        new_ref[:, rows] = stamp(total, peak).reshape(8, 16, 128)
    mask4 = mask4_ref[:, 0:128] + bias
    for r in range(2):
        rows = slice(64 * r, 64 * r + 64)
        full = slice(base + 64 * r, base + 64 * r + 64)
        total, peak = merge(
            new_ref[0:2, rows].reshape(128, 128),
            qs_ref[0:2, full].reshape(128, 128),
            halo_ref[6:8, rows].reshape(128, 128),
            vhalo[6:8, rows].reshape(128, 128),
            mask4,
        )
        new_ref[0:2, rows] = stamp(total, peak).reshape(2, 64, 128)


def first_kernel(index_ref, acc_ref, qs_ref, halo_ref, mask4_ref, mask16_ref, new_ref, vhalo):
    halo_rows(index_ref, acc_ref, qs_ref, halo_ref, vhalo, mask4_ref, mask16_ref, new_ref, 0)


def last_kernel(
    index_ref, acc_ref, qs_ref, done_ref, before_ref, halo_ref, perm_ref, mask1_ref, mask4_ref, mask16_ref, out_ref, vhalo, new
):
    halo_rows(index_ref, acc_ref, qs_ref, halo_ref, vhalo, mask4_ref, mask16_ref, new, 128)
    bias = jnp.where(index_ref[0] < GROUP, NEG, 0.0).astype(F32)
    low256, high256 = value_masks(TOK)
    low_rows = half(64)
    for i in range(GROUP):
        total = jnp.concatenate([done_ref[i], new[i]], axis=0)
        if i == 0:
            keys = jnp.concatenate([before_ref[7], halo_ref[7]], axis=0)
            total, _ = merge(total, qs_ref[0], keys, keys * high256 + low256, mask1_ref[:, 0:TOK] + bias)
        mixed = (total / lane_of(total, 0)).astype(BF) * high256
        natural = dot(perm_ref[...], mixed)
        out_ref[2 * i] = jnp.where(low_rows, pltpu.roll(natural[0:64], 64, 1), natural[64:128]).astype(BF)
        out_ref[2 * i + 1] = jnp.where(low_rows, pltpu.roll(natural[128:192], 64, 1), natural[192:256]).astype(BF)


def project_kernel(core_ref, rows_ref, own_ref, other_ref, out_ref, mixed):
    low = half(64)
    for side in range(2):
        core = core_ref[0] if side == 0 else 1 - core_ref[0]
        for j in range(4):
            first = rows_ref[4 * j + core].astype(F32)
            second = rows_ref[4 * j + 2 + core].astype(F32)
            cols = slice(128 * j, 128 * j + 128)
            mixed[side, 0:64, cols] = jnp.where(low, first, pltpu.roll(second, 64, 1)).astype(BF)
            mixed[side, 64:128, cols] = jnp.where(low, pltpu.roll(first, 64, 1), second).astype(BF)
    for n in range(4):
        cols = slice(512 * n, 512 * n + 512)
        out_ref[:, cols] = (dot(mixed[0], own_ref[:, cols]) + dot(mixed[1], other_ref[:, cols])).astype(BF)


def vmem():
    return pl.BlockSpec(memory_space=pltpu.VMEM)


def limit(mib):
    return pltpu.CompilerParams(vmem_limit_bytes=mib * 2**20)


def per_device(query_rows, key_rows, value_rows, out_weight, blocks):
    tables = make_tables(blocks)
    index = lax.axis_index(SP).astype(jnp.int32).reshape(1)
    core = lax.axis_index("tp").astype(jnp.int32).reshape(1)

    def full(shape):
        return pl.BlockSpec(shape, lambda i, s: (0,) * len(shape))

    send = pl.pallas_call(
        pack_kernel,
        grid_spec=pltpu.PrefetchScalarGridSpec(
            num_scalar_prefetch=1,
            grid=(1,),
            in_specs=[
                full((TOK, 512)),
                full((TOK, 512)),
                full((TOK, 512)),
                full((TOK, TOK)),
                full((TOK, 128)),
                full((TOK, 128)),
                full((16 + blocks // 16, 256)),
            ],
            out_specs=full((GROUP, TOK + 128, 128)),
        ),
        out_shape=jax.ShapeDtypeStruct((GROUP, TOK + 128, 128), BF),
        compiler_params=limit(12),
        name="pack",
    )(
        index,
        query_rows,
        key_rows,
        value_rows,
        jnp.asarray(tables["perm"], BF),
        jnp.asarray(tables["cos"]),
        jnp.asarray(tables["sin"]),
        jnp.asarray(tables["anchors"]),
    )
    own = lax.all_to_all(send, ("b", "x"), 0, 0, tiled=True)
    following = [(s, s + GROUP) for s in range(blocks - GROUP)]
    halo_a = lax.ppermute(own[:, 0:128], SP, following)
    halo_b = lax.ppermute(own[:, 128:256], SP, following)
    weight, _ = lax.optimization_barrier((out_weight, own))
    other_weight = lax.ppermute(weight, "tp", [(0, 1), (1, 0)])
    mask1, mask4, mask16 = (jnp.asarray(tables[name]) for name in ("mask1", "mask4", "mask16"))
    smem = pl.BlockSpec(memory_space=pltpu.SMEM)
    acc, qs = pl.pallas_call(
        own_kernel,
        in_specs=[vmem()] * 4,
        out_specs=[vmem()] * 2,
        out_shape=[
            jax.ShapeDtypeStruct((GROUP, TOK, 128), F32),
            jax.ShapeDtypeStruct((GROUP, TOK, 128), BF),
        ],
        scratch_shapes=[pltpu.VMEM((GROUP, TOK, 128), BF)],
        compiler_params=limit(16),
        cost_estimate=pl.CostEstimate(flops=20 * 10**9, bytes_accessed=2 * 2**20, transcendentals=0),
        name="attend_own",
    )(own, mask1, mask4, mask16)
    done = pl.pallas_call(
        first_kernel,
        in_specs=[smem] + [vmem()] * 5,
        out_specs=vmem(),
        out_shape=jax.ShapeDtypeStruct((GROUP, 128, 128), F32),
        scratch_shapes=[pltpu.VMEM((GROUP, 128, 128), BF)],
        compiler_params=limit(16),
        cost_estimate=pl.CostEstimate(flops=4 * 10**9, bytes_accessed=2 * 2**20, transcendentals=0),
        name="attend_first",
    )(index, acc, qs, halo_a, mask4, mask16)
    back = pl.pallas_call(
        last_kernel,
        in_specs=[smem] + [vmem()] * 9,
        out_specs=vmem(),
        out_shape=jax.ShapeDtypeStruct((2 * GROUP, 64, 128), BF),
        scratch_shapes=[
            pltpu.VMEM((GROUP, 128, 128), BF),
            pltpu.VMEM((GROUP, 128, 128), F32),
        ],
        compiler_params=limit(16),
        cost_estimate=pl.CostEstimate(flops=4 * 10**9, bytes_accessed=2 * 2**20, transcendentals=0),
        name="attend_last",
    )(index, acc, qs, done, halo_a, halo_b, jnp.asarray(tables["perm"].T, BF), mask1, mask4, mask16)
    rows = lax.all_to_all(back, ("b", "x", "tp"), 0, 0, tiled=True)
    return pl.pallas_call(
        project_kernel,
        in_specs=[pl.BlockSpec(memory_space=pltpu.SMEM)] + [vmem()] * 3,
        out_specs=vmem(),
        out_shape=jax.ShapeDtypeStruct((TOK // 2, 2048), BF),
        scratch_shapes=[pltpu.VMEM((2, TOK // 2, 512), BF)],
        compiler_params=limit(16),
        name="project",
    )(core, rows, out_weight, other_weight)


def solution(mesh):
    blocks = mesh.shape["sp"]
    fine = Mesh(mesh.devices.reshape(blocks // 16, 2, 2, 4, 2), SP + ("tp",))
    return jax.shard_map(
        functools.partial(per_device, blocks=blocks),
        mesh=fine,
        in_specs=(P(SP, "tp"), P(SP, "tp"), P(SP, "tp"), P("tp", None)),
        out_specs=P(SP + ("tp",), None),
        check_vma=False,
    )
```

profile of v0, /device:TPU:96, one launch (start us, length us, event | category | flops | bytes accessed | tf_op | source)
XLA Modules:
  0.0 67.3 jit_solution(2769135174589055147)
XLA Ops:
  0.0 0.9 %copy-done.1 = bf16[256,512]{1,0:T(8,128)(2,1)S(1)} copy-done((bf16[256,512]{1,0:T(8,128)(2,1)S(1)}, bf16[256,512]{1,0:T(8,128)(2,1)}, u32[]{:S(2)}) %copy-start.1) | copy-done | bytes 262168
  1.0 0.9 %copy-done.2 = bf16[256,512]{1,0:T(8,128)(2,1)S(1)} copy-done((bf16[256,512]{1,0:T(8,128)(2,1)S(1)}, bf16[256,512]{1,0:T(8,128)(2,1)}, u32[]{:S(2)}) %copy-start.2) | copy-done | bytes 262168
  1.9 0.9 %copy-done.3 = bf16[256,512]{1,0:T(8,128)(2,1)S(1)} copy-done((bf16[256,512]{1,0:T(8,128)(2,1)S(1)}, bf16[256,512]{1,0:T(8,128)(2,1)}, u32[]{:S(2)}) %copy-start.3) | copy-done | bytes 262168
  2.9 0.9 %copy-done.4 = f32[256,128]{1,0:T(8,128)S(1)} copy-done((f32[256,128]{1,0:T(8,128)S(1)}, f32[256,128]{1,0:T(8,128)}, u32[]{:S(2)}) %copy-start.4) | copy-done | bytes 131096
  3.8 0.9 %copy-done.5 = f32[256,128]{1,0:T(8,128)S(1)} copy-done((f32[256,128]{1,0:T(8,128)S(1)}, f32[256,128]{1,0:T(8,128)}, u32[]{:S(2)}) %copy-start.5) | copy-done | bytes 131096
  4.7 0.9 %copy-done.6 = bf16[256,256]{1,0:T(8,128)(2,1)S(1)} copy-done((bf16[256,256]{1,0:T(8,128)(2,1)S(1)}, bf16[256,256]{1,0:T(8,128)(2,1)}, u32[]{:S(2)}) %copy-start.6) | copy-done | bytes 131096
  5.6 0.8 %copy-done.7 = f32[32,256]{1,0:T(8,128)S(1)} copy-done((f32[32,256]{1,0:T(8,128)S(1)}, f32[32,256]{1,0:T(8,128)}, u32[]{:S(2)}) %copy-start.7) | copy-done | bytes 32792
  6.3 1.1 %pack.1 = bf16[8,384,128]{2,1,0:T(8,128)(2,1)S(1)} custom-call(s32[1]{0:T(128)} %bitcast.1.index_ref, bf16[256,512]{1,0:T(8,128)(2,1)S(1)} %copy-done.1, bf16[256,512]{1,0:T(8,128)(2,1)S(1)} %copy-done.2, bf16[256,512]{1,0:T(8,128)(2,1)S(1)} %copy-done.3, bf16[256,256]{1,0:T(8,128)(2,1)S(1)} %copy-done.6, f32[256,128]{1,0:T(8,128)S(1)} %copy-done.5, ...), custom_call_target="tpu_custom_call" | custom-call | tf_op jit(solution)/shard_map/pack/pallas_call | solution.py:267
  7.5 18.0 %all_to_all.10.own_ref = bf16[8,384,128]{2,1,0:T(8,128)(2,1)S(1)} all-to-all(bf16[8,384,128]{2,1,0:T(8,128)(2,1)S(1)} %pack.1), channel_id=1, replica_groups=mesh['z'=16,'g'=2,'b'=2,'x'=4,'tp'=2] {'b','x'}, dimensions={0} | all-to-all | bytes 1572864 | tf_op jit(solution)/shard_map/all_to_all | solution.py:296
  25.5 4.8 %collective-permute-start.1 = (bf16[8,128,128]{2,1,0:T(8,128)(2,1)S(1)}, bf16[8,128,128]{2,1,0:T(8,128)(2,1)S(1)}, u32[]{:S(2)}, u32[]{:S(2)}) collective-permute-start(bf16[8,128,128]{2,1,0:T(8,128)(2,1)S(1)} %get-tuple-element.11), channel_id=1, source_target_pairs={{0,16},{2,18},{4,20},{6,22},{8,24},{10,26},{12,28},{14,30},{16,32}... | collective-permute-start | bytes 786440 | tf_op jit(solution)/shard_map/ppermute | solution.py:299
  30.3 5.1 %collective-permute-start = (bf16[8,128,128]{2,1,0:T(8,128)(2,1)S(1)}, bf16[8,128,128]{2,1,0:T(8,128)(2,1)S(1)}, u32[]{:S(2)}, u32[]{:S(2)}) collective-permute-start(bf16[8,128,128]{2,1,0:T(8,128)(2,1)S(1)} %get-tuple-element.12), channel_id=1, source_target_pairs={{0,16},{2,18},{4,20},{6,22},{8,24},{10,26},{12,28},{14,30},{16,32}... | collective-permute-start | bytes 786440 | tf_op jit(solution)/shard_map/ppermute | solution.py:298
  35.5 0.0 copy-done
  35.5 1.9 %collective-permute-start.2 = (bf16[512,2048]{1,0:T(8,128)(2,1)S(1)}, bf16[512,2048]{1,0:T(8,128)(2,1)}, u32[]{:S(2)}, u32[]{:S(2)}) collective-permute-start(bf16[512,2048]{1,0:T(8,128)(2,1)S(1)} %copy-done), channel_id=1, source_target_pairs={{0,1},{1,0},{2,3},{3,2},{4,5},{5,4},{6,7},{7,6},{8,9},{9,8},{10,11... | collective-permute-start | bytes 6291464 | tf_op jit(solution)/shard_map/ppermute | solution.py:301
  37.4 0.0 copy-done.8
  37.4 8.4 %attend_own.1 = (f32[8,256,128]{2,1,0:T(8,128)S(1)}, bf16[8,256,128]{2,1,0:T(8,128)(2,1)S(1)}) custom-call(bf16[8,384,128]{2,1,0:T(8,128)(2,1)S(1)} %all_to_all.10.own_ref, f32[256,512]{1,0:T(8,128)S(1)} %copy-done.8, f32[128,256]{1,0:T(8,128)S(1)} %copy-done.10, f32[128,256]{1,0:T(8,128)S(1)} %copy-done.9), custom_call_target="tpu_custom_call" | custom-call | flops 20000000000 | bytes 2097152 | tf_op jit(solution)/shard_map/attend_own/pallas_call | solution.py:304
  45.8 0.0 collective-permute-done.halo_ref.before_ref
  45.8 0.0 copy-start.11
  45.8 2.6 %attend_first.1.done_ref = f32[8,128,128]{2,1,0:T(8,128)S(1)} custom-call(s32[1]{0:T(128)} %bitcast.1.index_ref, f32[8,256,128]{2,1,0:T(8,128)S(1)} %get-tuple-element.8.acc_ref, bf16[8,256,128]{2,1,0:T(8,128)(2,1)S(1)} %get-tuple-element.9.qs_ref, bf16[8,128,128]{2,1,0:T(8,128)(2,1)S(1)} %collective-permute-done.halo_ref.before_ref, ...), custom_call_target="tpu_custom_call" | custom-call | flops 4000000000 | bytes 2097152 | tf_op jit(solution)/shard_map/attend_first/pallas_call | solution.py:317
  48.5 0.0 collective-permute-done.1.halo_ref
  48.5 4.3 %attend_last.1 = bf16[16,64,128]{2,1,0:T(8,128)(2,1)} custom-call(s32[1]{0:T(128)} %bitcast.1.index_ref, f32[8,256,128]{2,1,0:T(8,128)S(1)} %get-tuple-element.8.acc_ref, bf16[8,256,128]{2,1,0:T(8,128)(2,1)S(1)} %get-tuple-element.9.qs_ref, f32[8,128,128]{2,1,0:T(8,128)S(1)} %attend_first.1.done_ref, ...), custom_call_target="tpu_custom_call" | custom-call | flops 4000000000 | bytes 2097152 | tf_op jit(solution)/shard_map/attend_last/pallas_call | solution.py:327
  52.8 3.5 %all-to-all-start.1 = ((bf16[16,64,128]{2,1,0:T(8,128)(2,1)}), bf16[16,64,128]{2,1,0:T(8,128)(2,1)S(1)}, u32[]{:S(2)}, u32[]{:S(2)}) async-start(bf16[16,64,128]{2,1,0:T(8,128)(2,1)} %attend_last.1), calls=%async_computation.1 | async-start | bytes 524288 | tf_op jit(solution)/shard_map/all_to_all | solution.py:340
  56.3 7.8 %all-to-all-done.1.rows_ref = bf16[16,64,128]{2,1,0:T(8,128)(2,1)S(1)} async-done(((bf16[16,64,128]{2,1,0:T(8,128)(2,1)}), bf16[16,64,128]{2,1,0:T(8,128)(2,1)S(1)}, u32[]{:S(2)}, u32[]{:S(2)}) %all-to-all-start.1) | async-done | bytes 262176 | tf_op jit(solution)/shard_map/all_to_all | solution.py:340
  64.1 0.0 collective-permute-done.2.other_ref
  64.1 3.2 %project.1 = bf16[128,2048]{1,0:T(8,128)(2,1)} custom-call(s32[1]{0:T(128)} %bitcast.core_ref, bf16[16,64,128]{2,1,0:T(8,128)(2,1)S(1)} %all-to-all-done.1.rows_ref, bf16[512,2048]{1,0:T(8,128)(2,1)S(1)} %copy-done, bf16[512,2048]{1,0:T(8,128)(2,1)} %collective-permute-done.2.other_ref), custom_call_target="tpu_custom_call" | custom-call | tf_op jit(solution)/shard_map/project/pallas_call | solution.py:341
  (15 shorter events, 0.1 us)
Async XLA Ops:
  0.0 0.9 %copy-start.1 = (bf16[256,512]{1,0:T(8,128)(2,1)S(1)}, bf16[256,512]{1,0:T(8,128)(2,1)}, u32[]{:S(2)}) copy-start(bf16[256,512]{1,0:T(8,128)(2,1)} %q_ref.1) | copy-start | bytes 786436
  1.0 0.9 %copy-start.2 = (bf16[256,512]{1,0:T(8,128)(2,1)S(1)}, bf16[256,512]{1,0:T(8,128)(2,1)}, u32[]{:S(2)}) copy-start(bf16[256,512]{1,0:T(8,128)(2,1)} %k_ref.1) | copy-start | bytes 786436
  1.9 0.9 %copy-start.3 = (bf16[256,512]{1,0:T(8,128)(2,1)S(1)}, bf16[256,512]{1,0:T(8,128)(2,1)}, u32[]{:S(2)}) copy-start(bf16[256,512]{1,0:T(8,128)(2,1)} %v_ref.1) | copy-start | bytes 786436
  2.9 0.9 %copy-start.4 = (f32[256,128]{1,0:T(8,128)S(1)}, f32[256,128]{1,0:T(8,128)}, u32[]{:S(2)}) copy-start(f32[256,128]{1,0:T(8,128)} %constant.44.clone.sin_ref) | copy-start | bytes 393220
  3.8 0.9 %copy-start.5 = (f32[256,128]{1,0:T(8,128)S(1)}, f32[256,128]{1,0:T(8,128)}, u32[]{:S(2)}) copy-start(f32[256,128]{1,0:T(8,128)} %constant.43.clone.cos_ref) | copy-start | bytes 393220
  4.7 0.9 %copy-start.6 = (bf16[256,256]{1,0:T(8,128)(2,1)S(1)}, bf16[256,256]{1,0:T(8,128)(2,1)}, u32[]{:S(2)}) copy-start(bf16[256,256]{1,0:T(8,128)(2,1)} %constant.42.clone.perm_ref) | copy-start | bytes 393220
  5.6 0.8 %copy-start.7 = (f32[32,256]{1,0:T(8,128)S(1)}, f32[32,256]{1,0:T(8,128)}, u32[]{:S(2)}) copy-start(f32[32,256]{1,0:T(8,128)} %constant.45.clone.anchor_ref) | copy-start | bytes 98308
  6.3 29.1 %copy-start = (bf16[512,2048]{1,0:T(8,128)(2,1)S(1)}, bf16[512,2048]{1,0:T(8,128)(2,1)}, u32[]{:S(2)}) copy-start(bf16[512,2048]{1,0:T(8,128)(2,1)} %own_ref.1) | copy-start | bytes 6291460
  6.3 31.1 %copy-start.8 = (f32[256,512]{1,0:T(8,128)S(1)}, f32[256,512]{1,0:T(8,128)}, u32[]{:S(2)}) copy-start(f32[256,512]{1,0:T(8,128)} %constant.46.clone.mask1_ref) | copy-start | bytes 1572868
  6.3 31.1 %copy-start.9 = (f32[128,256]{1,0:T(8,128)S(1)}, f32[128,256]{1,0:T(8,128)}, u32[]{:S(2)}) copy-start(f32[128,256]{1,0:T(8,128)} %constant.48.clone.mask16_ref) | copy-start | bytes 393220
  6.3 31.1 %copy-start.10 = (f32[128,256]{1,0:T(8,128)S(1)}, f32[128,256]{1,0:T(8,128)}, u32[]{:S(2)}) copy-start(f32[128,256]{1,0:T(8,128)} %constant.47.clone.mask4_ref) | copy-start | bytes 393220
  25.5 22.9 %collective-permute-start.1 = (bf16[8,128,128]{2,1,0:T(8,128)(2,1)S(1)}, bf16[8,128,128]{2,1,0:T(8,128)(2,1)S(1)}, u32[]{:S(2)}, u32[]{:S(2)}) collective-permute-start(bf16[8,128,128]{2,1,0:T(8,128)(2,1)S(1)} %get-tuple-element.11), channel_id=1, source_target_pairs={{0,16},{2,18},{4,20},{6,22},{8,24},{10,26},{12,28},{14,30},{16,32}... | collective-permute-start | bytes 786440 | tf_op jit(solution)/shard_map/ppermute | solution.py:299
  30.3 15.5 %collective-permute-start = (bf16[8,128,128]{2,1,0:T(8,128)(2,1)S(1)}, bf16[8,128,128]{2,1,0:T(8,128)(2,1)S(1)}, u32[]{:S(2)}, u32[]{:S(2)}) collective-permute-start(bf16[8,128,128]{2,1,0:T(8,128)(2,1)S(1)} %get-tuple-element.12), channel_id=1, source_target_pairs={{0,16},{2,18},{4,20},{6,22},{8,24},{10,26},{12,28},{14,30},{16,32}... | collective-permute-start | bytes 786440 | tf_op jit(solution)/shard_map/ppermute | solution.py:298
  35.5 28.7 %collective-permute-start.2 = (bf16[512,2048]{1,0:T(8,128)(2,1)S(1)}, bf16[512,2048]{1,0:T(8,128)(2,1)}, u32[]{:S(2)}, u32[]{:S(2)}) collective-permute-start(bf16[512,2048]{1,0:T(8,128)(2,1)S(1)} %copy-done), channel_id=1, source_target_pairs={{0,1},{1,0},{2,3},{3,2},{4,5},{5,4},{6,7},{7,6},{8,9},{9,8},{10,11... | collective-permute-start | bytes 6291464 | tf_op jit(solution)/shard_map/ppermute | solution.py:301
  45.8 2.7 %copy-start.11 = (bf16[256,256]{1,0:T(8,128)(2,1)S(1)}, bf16[256,256]{1,0:T(8,128)(2,1)}, u32[]{:S(2)}) copy-start(bf16[256,256]{1,0:T(8,128)(2,1)} %constant.49.clone.perm_ref) | copy-start | bytes 393220
  52.8 11.4 %all-to-all-start.1 = ((bf16[16,64,128]{2,1,0:T(8,128)(2,1)}), bf16[16,64,128]{2,1,0:T(8,128)(2,1)S(1)}, u32[]{:S(2)}, u32[]{:S(2)}) async-start(bf16[16,64,128]{2,1,0:T(8,128)(2,1)} %attend_last.1), calls=%async_computation.1 | async-start | bytes 524288 | tf_op jit(solution)/shard_map/all_to_all | solution.py:340
where the time goes:
time: 67.8 us; the launch traced here: 67.3 us
  Pallas kernels  19.6 us (29%)
  blocking collectives  18 us (27%)
  starting transfers between devices  15.4 us (23%)
  waiting for transfers between devices  7.82 us (12%)
  local copies, waits for them, and re-layouts  6.38 us (9%)
    all_to_all x1, blocking collectives, per_device(): own = lax.all_to_all(send, ('b', 'x'), 0, 0, tiled=True)  18 us
    pallas_call x1, Pallas kernels, per_device(): pl.pallas_call(own_kernel, in_specs=[vmem()] * 4, out_specs=[vmem()] * 2,...  8.38 us
    all_to_all x1, waiting for transfers between devices, per_device(): rows = lax.all_to_all(back, ('b', 'x', 'tp'), 0, 0, tiled=True)  7.81 us
    unnamed x24, local copies, waits for them, and re-layouts  6.34 us
    ppermute x1, starting transfers between devices, per_device(): halo_a = lax.ppermute(own[:, 0:128], SP, following)  5.1 us
    ppermute x1, starting transfers between devices, per_device(): halo_b = lax.ppermute(own[:, 128:256], SP, following)  4.81 us
    pallas_call x1, Pallas kernels, per_device(): pl.pallas_call(last_kernel, in_specs=[smem] + [vmem()] * 9, out_specs=vme...  4.27 us
    all_to_all x1, starting transfers between devices, per_device(): rows = lax.all_to_all(back, ('b', 'x', 'tp'), 0, 0, tiled=True)  3.53 us
  transfers between devices with their start and end apart: 4, of which 1 were waited for; matrix products, arithmetic and copies ran while one was open for 0% of the time, Pallas kernels for 23%

commit v1 on v0

v1 whole, which is shorter than its diff:
```python
import functools
import math

import jax
import jax.numpy as jnp
import numpy as np
from jax import lax
from jax.experimental import pallas as pl
from jax.experimental.pallas import tpu as pltpu
from jax.sharding import Mesh, PartitionSpec as P


HD = 64
BACK = 128
THETA = 500000.0
TOK = 256
GROUP = 8
SP = ("z", "g", "b", "x")
NEG = -1e30
BF = jnp.bfloat16
F32 = jnp.float32


def row_tokens():
    p = np.arange(TOK)
    residue4, a, n = p // 64, (p % 64) // 16, p % 16
    return 16 * n + residue4 + 4 * a


def make_tables(blocks):
    t = row_tokens()
    inverse = np.float64(THETA) ** (-np.arange(32, dtype=np.float64) / 32)
    lanes = inverse[np.arange(128) % 32]
    inner = t[:, None] * lanes[None, :]
    fine = np.arange(16) * TOK
    coarse = np.arange(blocks // 16) * (16 * TOK)
    anchor = np.concatenate([fine, coarse])[:, None] * lanes[None, :]
    anchors = np.concatenate([np.cos(anchor), np.sin(anchor)], axis=1)
    perm = np.zeros((TOK, TOK), np.float32)
    perm[np.arange(TOK), t] = 1.0

    def band(query, key):
        distance = query[:, None] - key[None, :]
        return np.where((distance >= 0) & (distance <= BACK), 0.0, NEG).astype(np.float32)

    mask1 = band(t, np.concatenate([t - TOK, t]))
    row = np.arange(64)
    sub = 4 * (row % 16) + row // 16
    query4 = np.concatenate([sub, sub + 64])
    mask4 = band(query4, np.concatenate([query4 - 128, query4]))
    query16 = np.arange(128)
    mask16 = band(query16, np.concatenate([query16 - 128, query16]))
    return dict(
        cos=np.cos(inner).astype(np.float32),
        sin=np.sin(inner).astype(np.float32),
        anchors=anchors.astype(np.float32),
        perm=perm,
        mask1=mask1,
        mask4=mask4,
        mask16=mask16,
    )


def dot(a, b):
    return lax.dot_general(a, b, (((1,), (0,)), ((), ())), preferred_element_type=F32)


def dot_t(a, b):
    return lax.dot_general(a, b, (((1,), (1,)), ((), ())), preferred_element_type=F32)


def half(rows):
    return lax.broadcasted_iota(jnp.int32, (rows, 128), 1) < 64


def pack_kernel(
    index_ref, core_ref, q_hbm, k_hbm, v_hbm, perm_hbm, cos_hbm, sin_hbm, anchor_hbm, out_ref,
    q_ref, k_ref, v_ref, perm_ref, cos_ref, sin_ref, anchor_ref, sems,
):
    pairs = (
        (anchor_hbm, anchor_ref), (cos_hbm, cos_ref), (sin_hbm, sin_ref), (perm_hbm, perm_ref),
        (q_hbm, q_ref), (k_hbm, k_ref), (v_hbm, v_ref),
    )
    copies = [pltpu.make_async_copy(source, target, sems.at[n]) for n, (source, target) in enumerate(pairs)]
    for copy in copies:
        copy.start()
    for copy in copies:
        copy.wait()
    block = index_ref[0]
    flip = 4 * ((block // GROUP) % 2)
    fine = anchor_ref[pl.ds(block % 16, 1), :]
    coarse = anchor_ref[pl.ds(16 + block // 16, 1), :]
    cos_a = fine[:, :128] * coarse[:, :128] - fine[:, 128:] * coarse[:, 128:]
    sin_a = fine[:, 128:] * coarse[:, :128] + fine[:, :128] * coarse[:, 128:]
    lane = lax.broadcasted_iota(jnp.int32, (TOK, 128), 1)
    low64 = lane < 64
    low32 = (lane & 63) < 32
    sign = jnp.where(low32[:1], -1.0, 1.0).astype(F32)
    cosine = cos_a * cos_ref[...] - sin_a * sin_ref[...]
    sine = (sin_a * sign) * cos_ref[...] + (cos_a * sign) * sin_ref[...]

    def turn(rows):
        other = jnp.where(low32, pltpu.roll(rows, 96, 1), pltpu.roll(rows, 32, 1))
        return rows * cosine + other * sine

    perm = perm_ref[...]
    for j in range(4):
        cols = slice(128 * j, 128 * j + 128)
        query = turn(dot(perm, q_ref[:, cols])) * (1.0 / math.sqrt(HD))
        key = turn(dot(perm, k_ref[:, cols]))
        value = dot(perm, v_ref[:, cols])
        even = (2 * j) ^ flip
        odd = even + 1
        out_ref[even, 0:TOK] = jnp.where(low64, key, pltpu.roll(value, 64, 1)).astype(BF)
        out_ref[odd, 0:TOK] = jnp.where(low64, pltpu.roll(key, 64, 1), value).astype(BF)
        first, second = query[:128], query[128:]
        out_ref[even, TOK : TOK + 128] = jnp.where(low64[:128], first, pltpu.roll(second, 64, 1)).astype(BF)
        out_ref[odd, TOK : TOK + 128] = jnp.where(low64[:128], pltpu.roll(first, 64, 1), second).astype(BF)


def wide(x, n):
    return jnp.concatenate([x] * n, axis=1) if n > 1 else x


def value_masks(rows):
    low = half(rows)
    return jnp.where(low, 1.0, 0.0).astype(BF), jnp.where(low, 0.0, 1.0).astype(BF)


def merge(total, before, query, keys, values, mask):
    scores = dot_t(query, keys) + mask
    peak = jnp.maximum(before, jnp.max(scores, axis=1, keepdims=True))
    probs = jnp.exp(scores - wide(peak, scores.shape[1] // 128)).astype(BF)
    return total * jnp.exp(before - peak) + dot(probs, values), peak


def normal(total):
    return total / pltpu.roll(total, 64, 1)


def own_kernel(own_ref, mask1_ref, mask4_ref, mask16_ref, acc_ref, top_ref, qs_ref, ks, vs):
    low256, high256 = value_masks(TOK)
    low_bf = low256[:128]
    for i in range(GROUP):
        packed = own_ref[i, TOK : TOK + 128]
        qs_ref[i, 0:128] = packed * low_bf
        qs_ref[i, 128:256] = pltpu.roll(packed.astype(F32), 64, 1).astype(BF) * low_bf
        key = own_ref[i, 0:TOK]
        ks[i, 0:TOK] = key
        vs[i, 0:TOK] = key * high256 + low256
    for r in range(16):
        rows = slice(16 * r, 16 * r + 16)
        scores = dot_t(qs_ref[:, rows].reshape(128, 128), ks[:, rows].reshape(128, 128)) + mask16_ref[:, 128:256]
        peak = jnp.broadcast_to(jnp.max(scores, axis=1, keepdims=True), (128, 128))
        probs = jnp.exp(scores - peak).astype(BF)
        acc_ref[:, rows] = dot(probs, vs[:, rows].reshape(128, 128)).reshape(8, 16, 128)
        top_ref[:, rows] = peak.reshape(8, 16, 128)
    for b in range(4):
        for r in range(4):
            rows = slice(64 * r, 64 * r + 64)
            at = slice(2 * b, 2 * b + 2)
            seen = slice(max(0, 2 * b - 2), 2 * b + 2)
            n = 64 * (seen.stop - seen.start)
            total, peak = merge(
                acc_ref[at, rows].reshape(128, 128),
                top_ref[at, rows].reshape(128, 128),
                qs_ref[at, rows].reshape(128, 128),
                ks[seen, rows].reshape(n, 128),
                vs[seen, rows].reshape(n, 128),
                mask4_ref[:, 256 - n : 256],
            )
            acc_ref[at, rows] = total.reshape(2, 64, 128)
            top_ref[at, rows] = peak.reshape(2, 64, 128)
    for i in range(GROUP):
        first = max(0, i - 1)
        n = TOK * (i + 1 - first)
        total, peak = merge(
            acc_ref[i, 0:TOK],
            top_ref[i, 0:TOK],
            qs_ref[i, 0:TOK],
            ks[first : i + 1, 0:TOK].reshape(n, 128),
            vs[first : i + 1, 0:TOK].reshape(n, 128),
            mask1_ref[:, 2 * TOK - n : 2 * TOK],
        )
        acc_ref[i, 0:TOK] = total
        top_ref[i, 0:TOK] = peak


def halo_rows(acc_ref, top_ref, qs_ref, ks, vs, mask4, mask16, new, head, base, store):
    for r in range(2):
        rows = slice(64 * r, 64 * r + 64)
        full = slice(base + 64 * r, base + 64 * r + 64)
        total, peak = merge(
            acc_ref[0:2, full].reshape(128, 128),
            top_ref[0:2, full].reshape(128, 128),
            qs_ref[0:2, full].reshape(128, 128),
            ks[6:8, rows].reshape(128, 128),
            vs[6:8, rows].reshape(128, 128),
            mask4,
        )
        new[0:2, rows] = total.reshape(2, 64, 128)
        head[0:2, rows] = peak.reshape(2, 64, 128)
    for r in range(8):
        rows = slice(16 * r, 16 * r + 16)
        full = slice(base + 16 * r, base + 16 * r + 16)
        total, _ = merge(
            jnp.concatenate([new[0:2, rows], acc_ref[2:8, full]], axis=0).reshape(128, 128),
            jnp.concatenate([head[0:2, rows], top_ref[2:8, full]], axis=0).reshape(128, 128),
            qs_ref[:, full].reshape(128, 128),
            ks[0:8, rows].reshape(128, 128),
            vs[0:8, rows].reshape(128, 128),
            mask16,
        )
        store(rows, normal(total).reshape(8, 16, 128).astype(BF))


def spread(halo_ref, ks, vs, n):
    low, high = value_masks(128)
    for i in range(n):
        key = halo_ref[i]
        ks[i, 0:128] = key
        vs[i, 0:128] = key * high + low


def first_kernel(
    index_ref, acc_ref, top_ref, qs_ref, halo_ref, mask1_ref, mask4_ref, mask16_ref,
    lo_ref, acc0_ref, top0_ref, ks, vs, new, head, state, peaks,
):
    bias = jnp.where(index_ref[0] < GROUP, NEG, 0.0).astype(F32)
    spread(halo_ref, ks, vs, GROUP + 1)
    total, peak = merge(
        acc_ref[0, 0:TOK],
        top_ref[0, 0:TOK],
        qs_ref[0, 0:TOK],
        ks[7:9, 0:128].reshape(TOK, 128),
        vs[7:9, 0:128].reshape(TOK, 128),
        mask1_ref[:, 0:TOK] + bias,
    )
    acc0_ref[...] = total[128:]
    top0_ref[...] = peak[128:]
    state[0, 0:128] = total[:128]
    peaks[0, 0:128] = peak[:128]
    state[1, 0:128] = acc_ref[1, 0:128]
    peaks[1, 0:128] = top_ref[1, 0:128]

    def store(rows, value):
        lo_ref[:, rows] = value

    halo_rows(
        Stacked(state, acc_ref), Stacked(peaks, top_ref), qs_ref, ks, vs,
        mask4_ref[:, 0:128] + bias, mask16_ref[:, 0:128] + bias, new, head, 0, store,
    )


def last_kernel(
    index_ref, acc_ref, top_ref, acc0_ref, top0_ref, qs_ref, lo_ref, halo_ref, perm_ref, mask4_ref, mask16_ref,
    out_ref, ks, vs, new, head, state, peaks, hi,
):
    bias = jnp.where(index_ref[0] < GROUP, NEG, 0.0).astype(F32)
    spread(halo_ref, ks, vs, GROUP)
    state[0, 128:256] = acc0_ref[...]
    peaks[0, 128:256] = top0_ref[...]
    state[1, 128:256] = acc_ref[1, 128:256]
    peaks[1, 128:256] = top_ref[1, 128:256]

    def store(rows, value):
        hi[:, rows] = value

    halo_rows(
        Stacked(state, acc_ref), Stacked(peaks, top_ref), qs_ref, ks, vs,
        mask4_ref[:, 0:128] + bias, mask16_ref[:, 0:128] + bias, new, head, 128, store,
    )
    _, high = value_masks(TOK)
    low_rows = half(64)
    for i in range(GROUP):
        mixed = jnp.concatenate([lo_ref[i, 0:128], hi[i, 0:128]], axis=0) * high
        natural = dot(perm_ref[...], mixed)
        out_ref[2 * i] = jnp.where(low_rows, pltpu.roll(natural[0:64], 64, 1), natural[64:128]).astype(BF)
        out_ref[2 * i + 1] = jnp.where(low_rows, pltpu.roll(natural[128:192], 64, 1), natural[192:256]).astype(BF)


class Stacked:

    def __init__(self, start, rest):
        self.start, self.rest = start, rest

    def __getitem__(self, at):
        blocks, rows = at
        return (self.start if blocks.stop <= 2 else self.rest)[blocks, rows]


def project_kernel(index_ref, core_ref, rows_ref, own_ref, other_ref, out_ref, mixed):
    low = half(64)
    flip = 4 * ((index_ref[0] // GROUP) % 2)
    for side in range(2):
        core = core_ref[0] if side == 0 else 1 - core_ref[0]
        for j in range(4):
            first = rows_ref[2 * ((2 * j) ^ flip) + core].astype(F32)
            second = rows_ref[2 * ((2 * j) ^ flip) + 2 + core].astype(F32)
            cols = slice(128 * j, 128 * j + 128)
            mixed[side, 0:64, cols] = jnp.where(low, first, pltpu.roll(second, 64, 1)).astype(BF)
            mixed[side, 64:128, cols] = jnp.where(low, pltpu.roll(first, 64, 1), second).astype(BF)
    for n in range(4):
        cols = slice(512 * n, 512 * n + 512)
        out_ref[:, cols] = (dot(mixed[0], own_ref[:, cols]) + dot(mixed[1], other_ref[:, cols])).astype(BF)


def vmem():
    return pl.BlockSpec(memory_space=pltpu.VMEM)


def limit(mib):
    return pltpu.CompilerParams(vmem_limit_bytes=mib * 2**20)


def per_device(query_rows, key_rows, value_rows, out_weight, blocks):
    tables = make_tables(blocks)
    index = lax.axis_index(SP).astype(jnp.int32).reshape(1)
    core = lax.axis_index("tp").astype(jnp.int32).reshape(1)

    smem = pl.BlockSpec(memory_space=pltpu.SMEM)
    hbm = pl.BlockSpec(memory_space=pltpu.HBM)
    send = pl.pallas_call(
        pack_kernel,
        in_specs=[smem] * 2 + [hbm] * 7,
        out_specs=vmem(),
        out_shape=jax.ShapeDtypeStruct((GROUP, TOK + 128, 128), BF),
        scratch_shapes=[
            pltpu.VMEM((TOK, 512), BF),
            pltpu.VMEM((TOK, 512), BF),
            pltpu.VMEM((TOK, 512), BF),
            pltpu.VMEM((TOK, TOK), BF),
            pltpu.VMEM((TOK, 128), F32),
            pltpu.VMEM((TOK, 128), F32),
            pltpu.VMEM((16 + blocks // 16, 256), F32),
            pltpu.SemaphoreType.DMA((7,)),
        ],
        compiler_params=limit(12),
        name="pack",
    )(
        index,
        core,
        *(
            pltpu.with_memory_space_constraint(array, pltpu.HBM)
            for array in (
                query_rows,
                key_rows,
                value_rows,
                jnp.asarray(tables["perm"], BF),
                jnp.asarray(tables["cos"]),
                jnp.asarray(tables["sin"]),
                jnp.asarray(tables["anchors"]),
            )
        ),
    )
    own = lax.all_to_all(send, ("b", "x"), 0, 0, tiled=True)
    following = [(s, (s // GROUP + 1) * GROUP + ((s % GROUP) ^ 4)) for s in range(blocks - GROUP)]
    halo_a = lax.ppermute(jnp.concatenate([own[:, 0:128], own[7:8, 128:256]], axis=0), SP, following)
    halo_b = lax.ppermute(own[:, 128:256], SP, following)
    weight, _ = lax.optimization_barrier((out_weight, own))
    other_weight = lax.ppermute(weight, "tp", [(0, 1), (1, 0)])
    mask1, mask4, mask16 = (jnp.asarray(tables[name]) for name in ("mask1", "mask4", "mask16"))
    state = jax.ShapeDtypeStruct((GROUP, TOK + 8, 128), F32)
    acc, top, qs = pl.pallas_call(
        own_kernel,
        in_specs=[vmem()] * 4,
        out_specs=[vmem()] * 3,
        out_shape=[state, state, jax.ShapeDtypeStruct((GROUP, TOK + 16, 128), BF)],
        scratch_shapes=[pltpu.VMEM((GROUP, TOK + 16, 128), BF)] * 2,
        compiler_params=limit(16),
        cost_estimate=pl.CostEstimate(flops=20 * 10**9, bytes_accessed=2 * 2**20, transcendentals=0),
        name="attend_own",
    )(own, mask1, mask4, mask16)
    part = jax.ShapeDtypeStruct((128, 128), F32)
    lo, acc0, top0 = pl.pallas_call(
        first_kernel,
        in_specs=[smem] + [vmem()] * 7,
        out_specs=[vmem()] * 3,
        out_shape=[jax.ShapeDtypeStruct((GROUP, 144, 128), BF), part, part],
        scratch_shapes=[pltpu.VMEM((GROUP + 1, 144, 128), BF)] * 2
        + [pltpu.VMEM((2, 136, 128), F32)] * 2
        + [pltpu.VMEM((2, TOK + 8, 128), F32)] * 2,
        compiler_params=limit(16),
        cost_estimate=pl.CostEstimate(flops=4 * 10**9, bytes_accessed=2 * 2**20, transcendentals=0),
        name="attend_first",
    )(index, acc, top, qs, halo_a, mask1, mask4, mask16)
    back = pl.pallas_call(
        last_kernel,
        in_specs=[smem] + [vmem()] * 10,
        out_specs=vmem(),
        out_shape=jax.ShapeDtypeStruct((2 * GROUP, 64, 128), BF),
        scratch_shapes=[pltpu.VMEM((GROUP, 144, 128), BF)] * 2
        + [pltpu.VMEM((2, 136, 128), F32)] * 2
        + [pltpu.VMEM((2, TOK + 8, 128), F32)] * 2
        + [pltpu.VMEM((GROUP, 144, 128), BF)],
        compiler_params=limit(16),
        cost_estimate=pl.CostEstimate(flops=4 * 10**9, bytes_accessed=2 * 2**20, transcendentals=0),
        name="attend_last",
    )(index, acc, top, acc0, top0, qs, lo, halo_b, jnp.asarray(tables["perm"].T, BF), mask4, mask16)
    back, other_weight = lax.optimization_barrier((back, other_weight))
    rows = lax.all_to_all(back, ("b", "x", "tp"), 0, 0, tiled=True)
    return pl.pallas_call(
        project_kernel,
        in_specs=[smem] * 2 + [vmem()] * 3,
        out_specs=vmem(),
        out_shape=jax.ShapeDtypeStruct((TOK // 2, 2048), BF),
        scratch_shapes=[pltpu.VMEM((2, TOK // 2, 512), BF)],
        compiler_params=limit(16),
        name="project",
    )(index, core, rows, out_weight, other_weight)


def solution(mesh):
    blocks = mesh.shape["sp"]
    fine = Mesh(mesh.devices.reshape(blocks // 16, 2, 2, 4, 2), SP + ("tp",))
    return jax.shard_map(
        functools.partial(per_device, blocks=blocks),
        mesh=fine,
        in_specs=(P(SP, "tp"), P(SP, "tp"), P(SP, "tp"), P("tp", None)),
        out_specs=P(SP + ("tp",), None),
        check_vma=False,
    )
```

time: 67.8 us -> 58.8 us (0.87)
  the two profiles are of different devices: /device:TPU:96 before, /device:TPU:224 now
where the time goes in v1:
time: 58.8 us; the launch traced here: 58.6 us
  blocking collectives  28.7 us (49%)
  Pallas kernels  18 us (31%)
  starting transfers between devices  11.5 us (20%)
    all_to_all x1, blocking collectives, per_device(): own = lax.all_to_all(send, ('b', 'x'), 0, 0, tiled=True)  18.3 us
    all_to_all x1, blocking collectives, per_device(): rows = lax.all_to_all(back, ('b', 'x', 'tp'), 0, 0, tiled=True)  10.4 us
    pallas_call x1, Pallas kernels, per_device(): pl.pallas_call(own_kernel, in_specs=[vmem()] * 4, out_specs=[vmem()] * 3,...  8.13 us
    ppermute x1, starting transfers between devices, per_device(): lax.ppermute(jnp.concatenate([own[:, 0:128], own[7:8, 128:256]], axis=0),...  5.72 us
    ppermute x1, starting transfers between devices, per_device(): halo_b = lax.ppermute(own[:, 128:256], SP, following)  3.91 us
    pallas_call x1, Pallas kernels, per_device(): pl.pallas_call(last_kernel, in_specs=[smem] + [vmem()] * 10, out_specs=vm...  3.11 us
    pallas_call x1, Pallas kernels, per_device(): pl.pallas_call(first_kernel, in_specs=[smem] + [vmem()] * 7, out_specs=[v...  2.72 us
    pallas_call x1, Pallas kernels, per_device(): pl.pallas_call(pack_kernel, in_specs=[smem] * 2 + [hbm] * 7, out_specs=vm...  2.47 us
  transfers between devices with their start and end apart: 3, of which 0 were waited for; matrix products, arithmetic and copies ran while one was open for 0% of the time, Pallas kernels for 24%

profile of v1, /device:TPU:224, one launch (start us, length us, event | category | flops | bytes accessed | tf_op | source)
XLA Modules:
  0.0 58.6 jit_solution(5457523522744096164)
XLA Ops:
  0.0 2.5 %pack.1 = bf16[8,384,128]{2,1,0:T(8,128)(2,1)S(1)} custom-call(s32[1]{0:T(128)} %bitcast.index_ref, s32[1]{0:T(128)} %bitcast.1.core_ref, bf16[256,512]{1,0:T(8,128)(2,1)} %q_hbm.1, bf16[256,512]{1,0:T(8,128)(2,1)} %k_hbm.1, bf16[256,512]{1,0:T(8,128)(2,1)} %v_hbm.1, bf16[256,256]{1,0:T(8,128)(2,1)} %constant.42.clone.perm_hbm, ...), custom_call_target="tpu_custom_call" | custom-call | tf_op jit(solution)/shard_map/pack/pallas_call | solution.py:323
  2.5 0.0 copy-start
  2.5 0.0 copy-start.1
  2.5 0.0 copy-start.2
  2.5 0.0 copy-start.3
  2.5 18.3 %all_to_all.10.own_ref = bf16[8,384,128]{2,1,0:T(8,128)(2,1)S(1)} all-to-all(bf16[8,384,128]{2,1,0:T(8,128)(2,1)S(1)} %pack.1), channel_id=1, replica_groups=mesh['z'=16,'g'=2,'b'=2,'x'=4,'tp'=2] {'b','x'}, dimensions={0} | all-to-all | bytes 1572864 | tf_op jit(solution)/shard_map/all_to_all | solution.py:356
  20.8 3.9 %collective-permute-start.1 = (bf16[8,128,128]{2,1,0:T(8,128)(2,1)S(1)}, bf16[8,128,128]{2,1,0:T(8,128)(2,1)S(1)}, u32[]{:S(2)}, u32[]{:S(2)}) collective-permute-start(bf16[8,128,128]{2,1,0:T(8,128)(2,1)S(1)} %get-tuple-element.23), channel_id=1, source_target_pairs={{0,24},{2,26},{4,28},{6,30},{8,16},{10,18},{12,20},{14,22},{16,40}... | collective-permute-start | bytes 786440 | tf_op jit(solution)/shard_map/ppermute | solution.py:359
  24.8 5.7 %collective-permute-start = (bf16[9,128,128]{2,1,0:T(8,128)(2,1)S(1)}, bf16[9,128,128]{2,1,0:T(8,128)(2,1)S(1)}, u32[]{:S(2)}, u32[]{:S(2)}) collective-permute-start(bf16[9,128,128]{2,1,0:T(8,128)(2,1)S(1)} %pad_maximum_fusion), channel_id=1, source_target_pairs={{0,24},{2,26},{4,28},{6,30},{8,16},{10,18},{12,20},{14,22},{16,40}... | collective-permute-start | bytes 884744 | tf_op jit(solution)/shard_map/ppermute | solution.py:358
  30.5 0.0 copy-done
  30.5 1.9 %collective-permute-start.2 = (bf16[512,2048]{1,0:T(8,128)(2,1)S(1)}, bf16[512,2048]{1,0:T(8,128)(2,1)S(1)}, u32[]{:S(2)}, u32[]{:S(2)}) collective-permute-start(bf16[512,2048]{1,0:T(8,128)(2,1)S(1)} %copy-done), channel_id=1, source_target_pairs={{0,1},{1,0},{2,3},{3,2},{4,5},{5,4},{6,7},{7,6},{8,9},{9,8},{10,11... | collective-permute-start | bytes 6291464 | tf_op jit(solution)/shard_map/ppermute | solution.py:361
  32.5 0.0 copy-done.1
  32.5 0.0 copy-done.2
  32.5 0.0 copy-done.3
  32.5 8.1 %attend_own.1 = (f32[8,264,128]{2,1,0:T(8,128)S(1)}, f32[8,264,128]{2,1,0:T(8,128)S(1)}, bf16[8,272,128]{2,1,0:T(8,128)(2,1)S(1)}) custom-call(bf16[8,384,128]{2,1,0:T(8,128)(2,1)S(1)} %all_to_all.10.own_ref, f32[256,512]{1,0:T(8,128)S(1)} %copy-done.1, f32[128,256]{1,0:T(8,128)S(1)} %copy-done.3, f32[128,256]{1,0:T(8,128)S(1)} %copy-done.2), custom_call_target="tpu_custom_call" | custom-call | flops 20000000000 | bytes 2097152 | tf_op jit(solution)/shard_map/attend_own/pallas_call | solution.py:364
  40.6 0.0 collective-permute-done.halo_ref
  40.6 0.0 copy-start.4
  40.7 2.7 %attend_first.1 = (bf16[8,144,128]{2,1,0:T(8,128)(2,1)S(1)}, f32[128,128]{1,0:T(8,128)S(1)}, f32[128,128]{1,0:T(8,128)S(1)}) custom-call(s32[1]{0:T(128)} %bitcast.index_ref, f32[8,264,128]{2,1,0:T(8,128)S(1)} %get-tuple-element.14.acc_ref, f32[8,264,128]{2,1,0:T(8,128)S(1)} %get-tuple-element.15.top_ref, bf16[8,272,128]{2,1,0:T(8,128)(2,1)S(1)} %get-tuple-element.16.qs_ref, ...), custom_call_target="tpu_custom_call" | custom-call | flops 4000000000 | bytes 2097152 | tf_op jit(solution)/shard_map/attend_first/pallas_call | solution.py:375
  43.4 0.0 collective-permute-done.1.halo_ref
  43.4 0.0 copy-done.4
  43.4 3.1 %attend_last.1 = bf16[16,64,128]{2,1,0:T(8,128)(2,1)S(1)} custom-call(s32[1]{0:T(128)} %bitcast.index_ref, f32[8,264,128]{2,1,0:T(8,128)S(1)} %get-tuple-element.14.acc_ref, f32[8,264,128]{2,1,0:T(8,128)S(1)} %get-tuple-element.15.top_ref, f32[128,128]{1,0:T(8,128)S(1)} %get-tuple-element.17.acc0_ref, f32[128,128]{1,0:T(8,128)S(1)} %get-tuple-element.18.top0_ref, ...), custom_call_target="tpu_custom_call" | custom-call | flops 4000000000 | bytes 2097152 | tf_op jit(solution)/shard_map/attend_last/pallas_call | solution.py:387
  46.5 0.0 collective-permute-done.2.other_ref
  46.5 10.4 %all_to_all.11.rows_ref = bf16[16,64,128]{2,1,0:T(8,128)(2,1)S(1)} all-to-all(bf16[16,64,128]{2,1,0:T(8,128)(2,1)S(1)} %attend_last.1), channel_id=1, replica_groups=mesh['z'=16,'g'=2,'b'=2,'x'=4,'tp'=2] {'b','x','tp'}, dimensions={0} | all-to-all | bytes 524288 | tf_op jit(solution)/shard_map/all_to_all | solution.py:401
  57.0 1.6 %project.1 = bf16[128,2048]{1,0:T(8,128)(2,1)} custom-call(s32[1]{0:T(128)} %bitcast.index_ref, s32[1]{0:T(128)} %bitcast.1.core_ref, bf16[16,64,128]{2,1,0:T(8,128)(2,1)S(1)} %all_to_all.11.rows_ref, bf16[512,2048]{1,0:T(8,128)(2,1)S(1)} %copy-done, bf16[512,2048]{1,0:T(8,128)(2,1)S(1)} %collective-permute-done.2.other_ref), custom_call_target="tpu_custom_call" | custom-call | tf_op jit(solution)/shard_map/project/pallas_call | solution.py:402
  (3 shorter events, 0.1 us)
Async XLA Ops:
  2.5 28.1 %copy-start = (bf16[512,2048]{1,0:T(8,128)(2,1)S(1)}, bf16[512,2048]{1,0:T(8,128)(2,1)}, u32[]{:S(2)}) copy-start(bf16[512,2048]{1,0:T(8,128)(2,1)} %own_ref.1) | copy-start | bytes 6291460
  2.5 30.0 %copy-start.1 = (f32[256,512]{1,0:T(8,128)S(1)}, f32[256,512]{1,0:T(8,128)}, u32[]{:S(2)}) copy-start(f32[256,512]{1,0:T(8,128)} %constant.46.clone.mask1_ref) | copy-start | bytes 1572868
  2.5 30.0 %copy-start.2 = (f32[128,256]{1,0:T(8,128)S(1)}, f32[128,256]{1,0:T(8,128)}, u32[]{:S(2)}) copy-start(f32[128,256]{1,0:T(8,128)} %constant.48.clone.mask16_ref) | copy-start | bytes 393220
  2.5 30.0 %copy-start.3 = (f32[128,256]{1,0:T(8,128)S(1)}, f32[128,256]{1,0:T(8,128)}, u32[]{:S(2)}) copy-start(f32[128,256]{1,0:T(8,128)} %constant.47.clone.mask4_ref) | copy-start | bytes 393220
  20.8 22.6 %collective-permute-start.1 = (bf16[8,128,128]{2,1,0:T(8,128)(2,1)S(1)}, bf16[8,128,128]{2,1,0:T(8,128)(2,1)S(1)}, u32[]{:S(2)}, u32[]{:S(2)}) collective-permute-start(bf16[8,128,128]{2,1,0:T(8,128)(2,1)S(1)} %get-tuple-element.23), channel_id=1, source_target_pairs={{0,24},{2,26},{4,28},{6,30},{8,16},{10,18},{12,20},{14,22},{16,40}... | collective-permute-start | bytes 786440 | tf_op jit(solution)/shard_map/ppermute | solution.py:359
  24.8 15.8 %collective-permute-start = (bf16[9,128,128]{2,1,0:T(8,128)(2,1)S(1)}, bf16[9,128,128]{2,1,0:T(8,128)(2,1)S(1)}, u32[]{:S(2)}, u32[]{:S(2)}) collective-permute-start(bf16[9,128,128]{2,1,0:T(8,128)(2,1)S(1)} %pad_maximum_fusion), channel_id=1, source_target_pairs={{0,24},{2,26},{4,28},{6,30},{8,16},{10,18},{12,20},{14,22},{16,40}... | collective-permute-start | bytes 884744 | tf_op jit(solution)/shard_map/ppermute | solution.py:358
  30.5 16.0 %collective-permute-start.2 = (bf16[512,2048]{1,0:T(8,128)(2,1)S(1)}, bf16[512,2048]{1,0:T(8,128)(2,1)S(1)}, u32[]{:S(2)}, u32[]{:S(2)}) collective-permute-start(bf16[512,2048]{1,0:T(8,128)(2,1)S(1)} %copy-done), channel_id=1, source_target_pairs={{0,1},{1,0},{2,3},{3,2},{4,5},{5,4},{6,7},{7,6},{8,9},{9,8},{10,11... | collective-permute-start | bytes 6291464 | tf_op jit(solution)/shard_map/ppermute | solution.py:361
  40.6 2.8 %copy-start.4 = (bf16[256,256]{1,0:T(8,128)(2,1)S(1)}, bf16[256,256]{1,0:T(8,128)(2,1)}, u32[]{:S(2)}) copy-start(bf16[256,256]{1,0:T(8,128)(2,1)} %constant.49.clone.perm_ref) | copy-start | bytes 393220

commit v2 on v1

--- a/solution.py
+++ b/solution.py
@@ -127,18 +127,19 @@
     return jnp.where(low, 1.0, 0.0).astype(BF), jnp.where(low, 0.0, 1.0).astype(BF)
 
 
-def merge(total, before, query, keys, values, mask):
-    scores = dot_t(query, keys) + mask
-    peak = jnp.maximum(before, jnp.max(scores, axis=1, keepdims=True))
-    probs = jnp.exp(scores - wide(peak, scores.shape[1] // 128)).astype(BF)
-    return total * jnp.exp(before - peak) + dot(probs, values), peak
-
-
 def normal(total):
     return total / pltpu.roll(total, 64, 1)
 
 
-def own_kernel(own_ref, mask1_ref, mask4_ref, mask16_ref, acc_ref, top_ref, qs_ref, ks, vs):
+def row_max(scores):
+    return jnp.max(scores, axis=1, keepdims=True)
+
+
+def weights(scores, peak):
+    return jnp.exp(scores - wide(peak, scores.shape[1] // 128)).astype(BF)
+
+
+def own_kernel(own_ref, mask1_ref, mask4_ref, mask16_ref, acc_ref, top_ref, qs_ref, ks, vs, s16, s4, s1, p16, p4, p1):
     low256, high256 = value_masks(TOK)
     low_bf = low256[:128]
     for i in range(GROUP):
@@ -148,70 +149,92 @@
         key = own_ref[i, 0:TOK]
         ks[i, 0:TOK] = key
         vs[i, 0:TOK] = key * high256 + low256
+
+    def at4(n):
+        b, r = n // 4, n % 4
+        seen = slice(max(0, 2 * b - 2), 2 * b + 2)
+        return slice(2 * b, 2 * b + 2), slice(64 * r, 64 * r + 64), seen, 64 * (seen.stop - seen.start)
+
+    def at1(i):
+        seen = slice(max(0, i - 1), i + 1)
+        return seen, TOK * (seen.stop - seen.start)
+
     for r in range(16):
         rows = slice(16 * r, 16 * r + 16)
         scores = dot_t(qs_ref[:, rows].reshape(128, 128), ks[:, rows].reshape(128, 128)) + mask16_ref[:, 128:256]
-        peak = jnp.broadcast_to(jnp.max(scores, axis=1, keepdims=True), (128, 128))
-        probs = jnp.exp(scores - peak).astype(BF)
-        acc_ref[:, rows] = dot(probs, vs[:, rows].reshape(128, 128)).reshape(8, 16, 128)
-        top_ref[:, rows] = peak.reshape(8, 16, 128)
-    for b in range(4):
-        for r in range(4):
-            rows = slice(64 * r, 64 * r + 64)
-            at = slice(2 * b, 2 * b + 2)
-            seen = slice(max(0, 2 * b - 2), 2 * b + 2)
-            n = 64 * (seen.stop - seen.start)
-            total, peak = merge(
-                acc_ref[at, rows].reshape(128, 128),
-                top_ref[at, rows].reshape(128, 128),
-                qs_ref[at, rows].reshape(128, 128),
-                ks[seen, rows].reshape(n, 128),
-                vs[seen, rows].reshape(n, 128),
-                mask4_ref[:, 256 - n : 256],
-            )
-            acc_ref[at, rows] = total.reshape(2, 64, 128)
-            top_ref[at, rows] = peak.reshape(2, 64, 128)
-    for i in range(GROUP):
-        first = max(0, i - 1)
-        n = TOK * (i + 1 - first)
-        total, peak = merge(
-            acc_ref[i, 0:TOK],
-            top_ref[i, 0:TOK],
-            qs_ref[i, 0:TOK],
-            ks[first : i + 1, 0:TOK].reshape(n, 128),
-            vs[first : i + 1, 0:TOK].reshape(n, 128),
-            mask1_ref[:, 2 * TOK - n : 2 * TOK],
-        )
-        acc_ref[i, 0:TOK] = total
-        top_ref[i, 0:TOK] = peak
-
-
-def halo_rows(acc_ref, top_ref, qs_ref, ks, vs, mask4, mask16, new, head, base, store):
+        s16[r] = scores
+        top_ref[:, rows] = jnp.broadcast_to(row_max(scores), (128, 128)).reshape(8, 16, 128)
+    for n in range(16):
+        at, rows, seen, width = at4(n)
+        scores = dot_t(qs_ref[at, rows].reshape(128, 128), ks[seen, rows].reshape(width, 128))
+        scores = scores + mask4_ref[:, 256 - width : 256]
+        s4[n, :, 0:width] = scores
+        top_ref[at, rows] = jnp.maximum(top_ref[at, rows].reshape(128, 128), row_max(scores)).reshape(2, 64, 128)
+    for i in range(GROUP):
+        seen, width = at1(i)
+        scores = dot_t(qs_ref[i, 0:TOK], ks[seen, 0:TOK].reshape(width, 128)) + mask1_ref[:, 512 - width : 512]
+        s1[i, :, 0:width] = scores
+        top_ref[i, 0:TOK] = jnp.maximum(top_ref[i, 0:TOK], row_max(scores))
+    for r in range(16):
+        p16[r] = weights(s16[r], top_ref[:, 16 * r : 16 * r + 16].reshape(128, 128))
+    for n in range(16):
+        at, rows, seen, width = at4(n)
+        p4[n, :, 0:width] = weights(s4[n, :, 0:width], top_ref[at, rows].reshape(128, 128))
+    for i in range(GROUP):
+        seen, width = at1(i)
+        p1[i, :, 0:width] = weights(s1[i, :, 0:width], top_ref[i, 0:TOK])
+    for r in range(16):
+        rows = slice(16 * r, 16 * r + 16)
+        acc_ref[:, rows] = dot(p16[r], vs[:, rows].reshape(128, 128)).reshape(8, 16, 128)
+    for n in range(16):
+        at, rows, seen, width = at4(n)
+        acc_ref[at, rows] += dot(p4[n, :, 0:width], vs[seen, rows].reshape(width, 128)).reshape(2, 64, 128)
+    for i in range(GROUP):
+        seen, width = at1(i)
+        acc_ref[i, 0:TOK] += dot(p1[i, :, 0:width], vs[seen, 0:TOK].reshape(width, 128))
+
+
+def halo_rows(index_ref, acc_ref, top_ref, qs_ref, masks, scratch, base):
+    mask1_ref, mask4_ref, mask16_ref = masks
+    ks, vs, new, peak, s16, s4, s1, p16, p4, p1 = scratch
+    bias = jnp.where(index_ref[0] < GROUP, NEG, 0.0).astype(F32)
+    half_rows = slice(base, base + 128)
+    order = (7, 8) if base == 0 else (8, 7)
+
+    def both(ref):
+        return jnp.concatenate([ref[order[0], 0:128], ref[order[1], 0:128]], axis=0)
+
+    mask16 = mask16_ref[:, 0:128] + bias
+    for r in range(8):
+        rows = slice(16 * r, 16 * r + 16)
+        full = slice(base + 16 * r, base + 16 * r + 16)
+        scores = dot_t(qs_ref[:, full].reshape(128, 128), ks[0:8, rows].reshape(128, 128)) + mask16
+        s16[r] = scores
+        peak[:, rows] = jnp.maximum(top_ref[:, full].reshape(128, 128), row_max(scores)).reshape(8, 16, 128)
+    mask4 = mask4_ref[:, 0:128] + bias
     for r in range(2):
         rows = slice(64 * r, 64 * r + 64)
         full = slice(base + 64 * r, base + 64 * r + 64)
-        total, peak = merge(
-            acc_ref[0:2, full].reshape(128, 128),
-            top_ref[0:2, full].reshape(128, 128),
-            qs_ref[0:2, full].reshape(128, 128),
-            ks[6:8, rows].reshape(128, 128),
-            vs[6:8, rows].reshape(128, 128),
-            mask4,
-        )
-        new[0:2, rows] = total.reshape(2, 64, 128)
-        head[0:2, rows] = peak.reshape(2, 64, 128)
+        scores = dot_t(qs_ref[0:2, full].reshape(128, 128), ks[6:8, rows].reshape(128, 128)) + mask4
+        s4[r] = scores
+        peak[0:2, rows] = jnp.maximum(peak[0:2, rows].reshape(128, 128), row_max(scores)).reshape(2, 64, 128)
+    scores = dot_t(qs_ref[0, half_rows], both(ks)) + (mask1_ref[half_rows, 0:TOK] + bias)
+    s1[...] = scores
+    peak[0, 0:128] = jnp.maximum(peak[0, 0:128], row_max(scores))
+    for r in range(8):
+        p16[r] = weights(s16[r], peak[:, 16 * r : 16 * r + 16].reshape(128, 128))
+    for r in range(2):
+        p4[r] = weights(s4[r], peak[0:2, 64 * r : 64 * r + 64].reshape(128, 128))
+    p1[...] = weights(s1[...], peak[0, 0:128])
+    for i in range(GROUP):
+        new[i, 0:128] = acc_ref[i, half_rows] * jnp.exp(top_ref[i, half_rows] - peak[i, 0:128])
     for r in range(8):
         rows = slice(16 * r, 16 * r + 16)
-        full = slice(base + 16 * r, base + 16 * r + 16)
-        total, _ = merge(
-            jnp.concatenate([new[0:2, rows], acc_ref[2:8, full]], axis=0).reshape(128, 128),
-            jnp.concatenate([head[0:2, rows], top_ref[2:8, full]], axis=0).reshape(128, 128),
-            qs_ref[:, full].reshape(128, 128),
-            ks[0:8, rows].reshape(128, 128),
-            vs[0:8, rows].reshape(128, 128),
-            mask16,
-        )
-        store(rows, normal(total).reshape(8, 16, 128).astype(BF))
+        new[:, rows] += dot(p16[r], vs[0:8, rows].reshape(128, 128)).reshape(8, 16, 128)
+    for r in range(2):
+        rows = slice(64 * r, 64 * r + 64)
+        new[0:2, rows] += dot(p4[r], vs[6:8, rows].reshape(128, 128)).reshape(2, 64, 128)
+    new[0, 0:128] += dot(p1[...], both(vs))
 
 
 def spread(halo_ref, ks, vs, n):
@@ -222,71 +245,32 @@
         vs[i, 0:128] = key * high + low
 
 
-def first_kernel(
-    index_ref, acc_ref, top_ref, qs_ref, halo_ref, mask1_ref, mask4_ref, mask16_ref,
-    lo_ref, acc0_ref, top0_ref, ks, vs, new, head, state, peaks,
+def first_kernel(index_ref, acc_ref, top_ref, qs_ref, halo_ref, mask1_ref, mask4_ref, mask16_ref, lo_ref, *scratch):
+    ks, vs, new = scratch[:3]
+    spread(halo_ref, ks, vs, GROUP + 1)
+    halo_rows(index_ref, acc_ref, top_ref, qs_ref, (mask1_ref, mask4_ref, mask16_ref), scratch, 0)
+    _, high = value_masks(128)
+    for i in range(GROUP):
+        lo_ref[i, 0:128] = normal(new[i, 0:128]).astype(BF) * high
+
+
+def last_kernel(
+    index_ref, acc_ref, top_ref, qs_ref, lo_ref, before_ref, halo_ref, perm_ref, mask1_ref, mask4_ref, mask16_ref,
+    out_ref, *scratch,
 ):
-    bias = jnp.where(index_ref[0] < GROUP, NEG, 0.0).astype(F32)
-    spread(halo_ref, ks, vs, GROUP + 1)
-    total, peak = merge(
-        acc_ref[0, 0:TOK],
-        top_ref[0, 0:TOK],
-        qs_ref[0, 0:TOK],
-        ks[7:9, 0:128].reshape(TOK, 128),
-        vs[7:9, 0:128].reshape(TOK, 128),
-        mask1_ref[:, 0:TOK] + bias,
-    )
-    acc0_ref[...] = total[128:]
-    top0_ref[...] = peak[128:]
-    state[0, 0:128] = total[:128]
-    peaks[0, 0:128] = peak[:128]
-    state[1, 0:128] = acc_ref[1, 0:128]
-    peaks[1, 0:128] = top_ref[1, 0:128]
-
-    def store(rows, value):
-        lo_ref[:, rows] = value
-
-    halo_rows(
-        Stacked(state, acc_ref), Stacked(peaks, top_ref), qs_ref, ks, vs,
-        mask4_ref[:, 0:128] + bias, mask16_ref[:, 0:128] + bias, new, head, 0, store,
-    )
-
-
-def last_kernel(
-    index_ref, acc_ref, top_ref, acc0_ref, top0_ref, qs_ref, lo_ref, halo_ref, perm_ref, mask4_ref, mask16_ref,
-    out_ref, ks, vs, new, head, state, peaks, hi,
-):
-    bias = jnp.where(index_ref[0] < GROUP, NEG, 0.0).astype(F32)
+    ks, vs, new = scratch[:3]
     spread(halo_ref, ks, vs, GROUP)
-    state[0, 128:256] = acc0_ref[...]
-    peaks[0, 128:256] = top0_ref[...]
-    state[1, 128:256] = acc_ref[1, 128:256]
-    peaks[1, 128:256] = top_ref[1, 128:256]
-
-    def store(rows, value):
-        hi[:, rows] = value
-
-    halo_rows(
-        Stacked(state, acc_ref), Stacked(peaks, top_ref), qs_ref, ks, vs,
-        mask4_ref[:, 0:128] + bias, mask16_ref[:, 0:128] + bias, new, head, 128, store,
-    )
-    _, high = value_masks(TOK)
+    low, high = value_masks(128)
+    key = before_ref[7]
+    ks[GROUP, 0:128] = key
+    vs[GROUP, 0:128] = key * high + low
+    halo_rows(index_ref, acc_ref, top_ref, qs_ref, (mask1_ref, mask4_ref, mask16_ref), scratch, 128)
     low_rows = half(64)
     for i in range(GROUP):
-        mixed = jnp.concatenate([lo_ref[i, 0:128], hi[i, 0:128]], axis=0) * high
+        mixed = jnp.concatenate([lo_ref[i, 0:128], normal(new[i, 0:128]).astype(BF) * high], axis=0)
         natural = dot(perm_ref[...], mixed)
         out_ref[2 * i] = jnp.where(low_rows, pltpu.roll(natural[0:64], 64, 1), natural[64:128]).astype(BF)
         out_ref[2 * i + 1] = jnp.where(low_rows, pltpu.roll(natural[128:192], 64, 1), natural[192:256]).astype(BF)
-
-
-class Stacked:
-
-    def __init__(self, start, rest):
-        self.start, self.rest = start, rest
-
-    def __getitem__(self, at):
-        blocks, rows = at
-        return (self.start if blocks.stop <= 2 else self.rest)[blocks, rows]
 
 
 def project_kernel(index_ref, core_ref, rows_ref, own_ref, other_ref, out_ref, mixed):
@@ -366,20 +350,38 @@
         in_specs=[vmem()] * 4,
         out_specs=[vmem()] * 3,
         out_shape=[state, state, jax.ShapeDtypeStruct((GROUP, TOK + 16, 128), BF)],
-        scratch_shapes=[pltpu.VMEM((GROUP, TOK + 16, 128), BF)] * 2,
-        compiler_params=limit(16),
+        scratch_shapes=[
+            pltpu.VMEM((GROUP, TOK + 16, 128), BF),
+            pltpu.VMEM((GROUP, TOK + 16, 128), BF),
+            pltpu.VMEM((16, 128, 128), F32),
+            pltpu.VMEM((16, 128, 256), F32),
+            pltpu.VMEM((GROUP, TOK, 512), F32),
+            pltpu.VMEM((16, 128, 128), BF),
+            pltpu.VMEM((16, 128, 256), BF),
+            pltpu.VMEM((GROUP, TOK, 512), BF),
+        ],
+        compiler_params=limit(24),
         cost_estimate=pl.CostEstimate(flops=20 * 10**9, bytes_accessed=2 * 2**20, transcendentals=0),
         name="attend_own",
     )(own, mask1, mask4, mask16)
-    part = jax.ShapeDtypeStruct((128, 128), F32)
-    lo, acc0, top0 = pl.pallas_call(
+    scratch = [
+        pltpu.VMEM((GROUP + 1, 144, 128), BF),
+        pltpu.VMEM((GROUP + 1, 144, 128), BF),
+        pltpu.VMEM((GROUP, 136, 128), F32),
+        pltpu.VMEM((GROUP, 136, 128), F32),
+        pltpu.VMEM((8, 128, 128), F32),
+        pltpu.VMEM((2, 128, 128), F32),
+        pltpu.VMEM((128, TOK), F32),
+        pltpu.VMEM((8, 128, 128), BF),
+        pltpu.VMEM((2, 128, 128), BF),
+        pltpu.VMEM((128, TOK), BF),
+    ]
+    lo = pl.pallas_call(
         first_kernel,
         in_specs=[smem] + [vmem()] * 7,
-        out_specs=[vmem()] * 3,
-        out_shape=[jax.ShapeDtypeStruct((GROUP, 144, 128), BF), part, part],
-        scratch_shapes=[pltpu.VMEM((GROUP + 1, 144, 128), BF)] * 2
-        + [pltpu.VMEM((2, 136, 128), F32)] * 2
-        + [pltpu.VMEM((2, TOK + 8, 128), F32)] * 2,
+        out_specs=vmem(),
+        out_shape=jax.ShapeDtypeStruct((GROUP, 144, 128), BF),
+        scratch_shapes=scratch,
         compiler_params=limit(16),
         cost_estimate=pl.CostEstimate(flops=4 * 10**9, bytes_accessed=2 * 2**20, transcendentals=0),
         name="attend_first",
@@ -389,14 +391,11 @@
         in_specs=[smem] + [vmem()] * 10,
         out_specs=vmem(),
         out_shape=jax.ShapeDtypeStruct((2 * GROUP, 64, 128), BF),
-        scratch_shapes=[pltpu.VMEM((GROUP, 144, 128), BF)] * 2
-        + [pltpu.VMEM((2, 136, 128), F32)] * 2
-        + [pltpu.VMEM((2, TOK + 8, 128), F32)] * 2
-        + [pltpu.VMEM((GROUP, 144, 128), BF)],
+        scratch_shapes=scratch,
         compiler_params=limit(16),
         cost_estimate=pl.CostEstimate(flops=4 * 10**9, bytes_accessed=2 * 2**20, transcendentals=0),
         name="attend_last",
-    )(index, acc, top, acc0, top0, qs, lo, halo_b, jnp.asarray(tables["perm"].T, BF), mask4, mask16)
+    )(index, acc, top, qs, lo, halo_a, halo_b, jnp.asarray(tables["perm"].T, BF), mask1, mask4, mask16)
     back, other_weight = lax.optimization_barrier((back, other_weight))
     rows = lax.all_to_all(back, ("b", "x", "tp"), 0, 0, tiled=True)
     return pl.pallas_call(

time: 58.8 us -> 53.9 us (0.917)
  the two profiles are of different devices: /device:TPU:224 before, /device:TPU:256 now
where the time goes in v2:
time: 53.9 us; the launch traced here: 53.7 us
  blocking collectives  28.7 us (53%)
  starting transfers between devices  9.42 us (17%)
  Pallas kernels  9.09 us (17%)
  waiting for transfers between devices  6.17 us (11%)
    all_to_all x1, blocking collectives, per_device(): own = lax.all_to_all(send, ('b', 'x'), 0, 0, tiled=True)  18.3 us
    all_to_all x1, blocking collectives, per_device(): rows = lax.all_to_all(back, ('b', 'x', 'tp'), 0, 0, tiled=True)  10.4 us
    ppermute x1, waiting for transfers between devices, per_device(): lax.ppermute(jnp.concatenate([own[:, 0:128], own[7:8, 128:256]], axis=0),...  6.16 us
    ppermute x1, starting transfers between devices, per_device(): halo_b = lax.ppermute(own[:, 128:256], SP, following)  3.9 us
    ppermute x1, starting transfers between devices, per_device(): lax.ppermute(jnp.concatenate([own[:, 0:128], own[7:8, 128:256]], axis=0),...  3.6 us
    pallas_call x1, Pallas kernels, per_device(): pl.pallas_call(own_kernel, in_specs=[vmem()] * 4, out_specs=[vmem()] * 3,...  2.74 us
    pallas_call x1, Pallas kernels, per_device(): pl.pallas_call(pack_kernel, in_specs=[smem] * 2 + [hbm] * 7, out_specs=vm...  2.47 us
    ppermute x1, starting transfers between devices, per_device(): other_weight = lax.ppermute(weight, 'tp', [(0, 1), (1, 0)])  1.92 us
  transfers between devices with their start and end apart: 3, of which 1 were waited for; matrix products, arithmetic and copies ran while one was open for 0% of the time, Pallas kernels for 9%

profile of v2, /device:TPU:256, one launch (start us, length us, event | category | flops | bytes accessed | tf_op | source)
XLA Modules:
  0.0 53.7 jit_solution(7035694175445533066)
XLA Ops:
  0.0 2.5 %pack.1 = bf16[8,384,128]{2,1,0:T(8,128)(2,1)S(1)} custom-call(s32[1]{0:T(128)} %bitcast.index_ref, s32[1]{0:T(128)} %bitcast.1.core_ref, bf16[256,512]{1,0:T(8,128)(2,1)} %q_hbm.1, bf16[256,512]{1,0:T(8,128)(2,1)} %k_hbm.1, bf16[256,512]{1,0:T(8,128)(2,1)} %v_hbm.1, bf16[256,256]{1,0:T(8,128)(2,1)} %constant.42.clone.perm_hbm, ...), custom_call_target="tpu_custom_call" | custom-call | tf_op jit(solution)/shard_map/pack/pallas_call | solution.py:307
  2.5 0.0 copy-start
  2.5 0.0 copy-start.1
  2.5 0.0 copy-start.2
  2.5 0.0 copy-start.3
  2.5 18.3 %all_to_all.10.own_ref = bf16[8,384,128]{2,1,0:T(8,128)(2,1)S(1)} all-to-all(bf16[8,384,128]{2,1,0:T(8,128)(2,1)S(1)} %pack.1), channel_id=1, replica_groups=mesh['z'=16,'g'=2,'b'=2,'x'=4,'tp'=2] {'b','x'}, dimensions={0} | all-to-all | bytes 1572864 | tf_op jit(solution)/shard_map/all_to_all | solution.py:340
  20.8 3.9 %collective-permute-start.1 = (bf16[8,128,128]{2,1,0:T(8,128)(2,1)S(1)}, bf16[8,128,128]{2,1,0:T(8,128)(2,1)S(1)}, u32[]{:S(2)}, u32[]{:S(2)}) collective-permute-start(bf16[8,128,128]{2,1,0:T(8,128)(2,1)S(1)} %get-tuple-element.17), channel_id=1, source_target_pairs={{0,24},{2,26},{4,28},{6,30},{8,16},{10,18},{12,20},{14,22},{16,40}... | collective-permute-start | bytes 786440 | tf_op jit(solution)/shard_map/ppermute | solution.py:343
  24.8 3.6 %collective-permute-start = (bf16[9,128,128]{2,1,0:T(8,128)(2,1)S(1)}, bf16[9,128,128]{2,1,0:T(8,128)(2,1)S(1)}, u32[]{:S(2)}, u32[]{:S(2)}) collective-permute-start(bf16[9,128,128]{2,1,0:T(8,128)(2,1)S(1)} %pad_maximum_fusion), channel_id=1, source_target_pairs={{0,24},{2,26},{4,28},{6,30},{8,16},{10,18},{12,20},{14,22},{16,40}... | collective-permute-start | bytes 884744 | tf_op jit(solution)/shard_map/ppermute | solution.py:342
  28.4 0.0 copy-done
  28.4 1.9 %collective-permute-start.2 = (bf16[512,2048]{1,0:T(8,128)(2,1)S(1)}, bf16[512,2048]{1,0:T(8,128)(2,1)S(1)}, u32[]{:S(2)}, u32[]{:S(2)}) collective-permute-start(bf16[512,2048]{1,0:T(8,128)(2,1)S(1)} %copy-done), channel_id=1, source_target_pairs={{0,1},{1,0},{2,3},{3,2},{4,5},{5,4},{6,7},{7,6},{8,9},{9,8},{10,11... | collective-permute-start | bytes 6291464 | tf_op jit(solution)/shard_map/ppermute | solution.py:345
  30.4 0.0 copy-done.1
  30.4 0.0 copy-done.2
  30.4 0.0 copy-done.3
  30.4 2.7 %attend_own.1 = (f32[8,264,128]{2,1,0:T(8,128)S(1)}, f32[8,264,128]{2,1,0:T(8,128)S(1)}, bf16[8,272,128]{2,1,0:T(8,128)(2,1)S(1)}) custom-call(bf16[8,384,128]{2,1,0:T(8,128)(2,1)S(1)} %all_to_all.10.own_ref, f32[256,512]{1,0:T(8,128)S(1)} %copy-done.1, f32[128,256]{1,0:T(8,128)S(1)} %copy-done.3, f32[128,256]{1,0:T(8,128)S(1)} %copy-done.2), custom_call_target="tpu_custom_call" | custom-call | flops 20000000000 | bytes 2097152 | tf_op jit(solution)/shard_map/attend_own/pallas_call | solution.py:348
  33.1 6.2 %collective-permute-done.halo_ref.before_ref = bf16[9,128,128]{2,1,0:T(8,128)(2,1)S(1)} collective-permute-done((bf16[9,128,128]{2,1,0:T(8,128)(2,1)S(1)}, bf16[9,128,128]{2,1,0:T(8,128)(2,1)S(1)}, u32[]{:S(2)}, u32[]{:S(2)}) %collective-permute-start) | collective-permute-done | bytes 294944 | tf_op jit(solution)/shard_map/ppermute | solution.py:342
  39.3 0.0 copy-start.4
  39.3 0.9 %attend_first.1.lo_ref = bf16[8,144,128]{2,1,0:T(8,128)(2,1)S(1)} custom-call(s32[1]{0:T(128)} %bitcast.index_ref, f32[8,264,128]{2,1,0:T(8,128)S(1)} %get-tuple-element.11.acc_ref, f32[8,264,128]{2,1,0:T(8,128)S(1)} %get-tuple-element.12.top_ref, bf16[8,272,128]{2,1,0:T(8,128)(2,1)S(1)} %get-tuple-element.13.qs_ref, ...), custom_call_target="tpu_custom_call" | custom-call | flops 4000000000 | bytes 2097152 | tf_op jit(solution)/shard_map/attend_first/pallas_call | solution.py:379
  40.2 0.0 collective-permute-done.1.halo_ref
  40.2 0.0 copy-done.4
  40.2 1.4 %attend_last.1 = bf16[16,64,128]{2,1,0:T(8,128)(2,1)S(1)} custom-call(s32[1]{0:T(128)} %bitcast.index_ref, f32[8,264,128]{2,1,0:T(8,128)S(1)} %get-tuple-element.11.acc_ref, f32[8,264,128]{2,1,0:T(8,128)S(1)} %get-tuple-element.12.top_ref, bf16[8,272,128]{2,1,0:T(8,128)(2,1)S(1)} %get-tuple-element.13.qs_ref, bf16[8,144,128]{2,1,0:T(8,128)(2,1)S(1)} %attend_first.1.lo_ref, ...), custom_call_target="tpu_custom_call" | custom-call | flops 4000000000 | bytes 2097152 | tf_op jit(solution)/shard_map/attend_last/pallas_call | solution.py:389
  41.6 0.0 collective-permute-done.2.other_ref
  41.6 10.4 %all_to_all.11.rows_ref = bf16[16,64,128]{2,1,0:T(8,128)(2,1)S(1)} all-to-all(bf16[16,64,128]{2,1,0:T(8,128)(2,1)S(1)} %attend_last.1), channel_id=1, replica_groups=mesh['z'=16,'g'=2,'b'=2,'x'=4,'tp'=2] {'b','x','tp'}, dimensions={0} | all-to-all | bytes 524288 | tf_op jit(solution)/shard_map/all_to_all | solution.py:400
  52.1 1.6 %project.1 = bf16[128,2048]{1,0:T(8,128)(2,1)} custom-call(s32[1]{0:T(128)} %bitcast.index_ref, s32[1]{0:T(128)} %bitcast.1.core_ref, bf16[16,64,128]{2,1,0:T(8,128)(2,1)S(1)} %all_to_all.11.rows_ref, bf16[512,2048]{1,0:T(8,128)(2,1)S(1)} %copy-done, bf16[512,2048]{1,0:T(8,128)(2,1)S(1)} %collective-permute-done.2.other_ref), custom_call_target="tpu_custom_call" | custom-call | tf_op jit(solution)/shard_map/project/pallas_call | solution.py:401
  (3 shorter events, 0.1 us)
Async XLA Ops:
  2.5 25.9 %copy-start = (bf16[512,2048]{1,0:T(8,128)(2,1)S(1)}, bf16[512,2048]{1,0:T(8,128)(2,1)}, u32[]{:S(2)}) copy-start(bf16[512,2048]{1,0:T(8,128)(2,1)} %own_ref.1) | copy-start | bytes 6291460
  2.5 27.9 %copy-start.1 = (f32[256,512]{1,0:T(8,128)S(1)}, f32[256,512]{1,0:T(8,128)}, u32[]{:S(2)}) copy-start(f32[256,512]{1,0:T(8,128)} %constant.46.clone.mask1_ref) | copy-start | bytes 1572868
  2.5 27.9 %copy-start.2 = (f32[128,256]{1,0:T(8,128)S(1)}, f32[128,256]{1,0:T(8,128)}, u32[]{:S(2)}) copy-start(f32[128,256]{1,0:T(8,128)} %constant.48.clone.mask16_ref) | copy-start | bytes 393220
  2.5 27.9 %copy-start.3 = (f32[128,256]{1,0:T(8,128)S(1)}, f32[128,256]{1,0:T(8,128)}, u32[]{:S(2)}) copy-start(f32[128,256]{1,0:T(8,128)} %constant.47.clone.mask4_ref) | copy-start | bytes 393220
  20.8 19.4 %collective-permute-start.1 = (bf16[8,128,128]{2,1,0:T(8,128)(2,1)S(1)}, bf16[8,128,128]{2,1,0:T(8,128)(2,1)S(1)}, u32[]{:S(2)}, u32[]{:S(2)}) collective-permute-start(bf16[8,128,128]{2,1,0:T(8,128)(2,1)S(1)} %get-tuple-element.17), channel_id=1, source_target_pairs={{0,24},{2,26},{4,28},{6,30},{8,16},{10,18},{12,20},{14,22},{16,40}... | collective-permute-start | bytes 786440 | tf_op jit(solution)/shard_map/ppermute | solution.py:343
  24.8 14.5 %collective-permute-start = (bf16[9,128,128]{2,1,0:T(8,128)(2,1)S(1)}, bf16[9,128,128]{2,1,0:T(8,128)(2,1)S(1)}, u32[]{:S(2)}, u32[]{:S(2)}) collective-permute-start(bf16[9,128,128]{2,1,0:T(8,128)(2,1)S(1)} %pad_maximum_fusion), channel_id=1, source_target_pairs={{0,24},{2,26},{4,28},{6,30},{8,16},{10,18},{12,20},{14,22},{16,40}... | collective-permute-start | bytes 884744 | tf_op jit(solution)/shard_map/ppermute | solution.py:342
  28.4 13.2 %collective-permute-start.2 = (bf16[512,2048]{1,0:T(8,128)(2,1)S(1)}, bf16[512,2048]{1,0:T(8,128)(2,1)S(1)}, u32[]{:S(2)}, u32[]{:S(2)}) collective-permute-start(bf16[512,2048]{1,0:T(8,128)(2,1)S(1)} %copy-done), channel_id=1, source_target_pairs={{0,1},{1,0},{2,3},{3,2},{4,5},{5,4},{6,7},{7,6},{8,9},{9,8},{10,11... | collective-permute-start | bytes 6291464 | tf_op jit(solution)/shard_map/ppermute | solution.py:345
  39.3 0.9 %copy-start.4 = (bf16[256,256]{1,0:T(8,128)(2,1)S(1)}, bf16[256,256]{1,0:T(8,128)(2,1)}, u32[]{:S(2)}) copy-start(bf16[256,256]{1,0:T(8,128)(2,1)} %constant.49.clone.perm_ref) | copy-start | bytes 393220

commit v3 on v2

v3 whole, which is shorter than its diff:
```python
import functools
import math

import jax
import jax.numpy as jnp
import numpy as np
from jax import lax
from jax.experimental import pallas as pl
from jax.experimental.pallas import tpu as pltpu
from jax.sharding import Mesh, PartitionSpec as P


HD = 64
BACK = 128
THETA = 500000.0
TOK = 256
GROUP = 8
SP = ("z", "g", "b", "x")
NEG = -1e30
BF = jnp.bfloat16
F32 = jnp.float32


def row_tokens():
    p = np.arange(TOK)
    residue4, a, n = p // 64, (p % 64) // 16, p % 16
    return 16 * n + residue4 + 4 * a


def make_tables(blocks):
    t = row_tokens()
    inverse = np.float64(THETA) ** (-np.arange(32, dtype=np.float64) / 32)
    lanes = inverse[np.arange(128) % 32]
    inner = t[:, None] * lanes[None, :]
    fine = np.arange(16) * TOK
    coarse = np.arange(blocks // 16) * (16 * TOK)
    anchor = np.concatenate([fine, coarse])[:, None] * lanes[None, :]
    anchors = np.concatenate([np.cos(anchor), np.sin(anchor)], axis=1)
    perm = np.zeros((TOK, TOK), np.float32)
    perm[np.arange(TOK), t] = 1.0

    def band(query, key):
        distance = query[:, None] - key[None, :]
        return np.where((distance >= 0) & (distance <= BACK), 0.0, NEG).astype(np.float32)

    mask1 = band(t, np.concatenate([t - TOK, t]))
    row = np.arange(64)
    sub = 4 * (row % 16) + row // 16
    query4 = np.concatenate([sub, sub + 64])
    mask4 = band(query4, np.concatenate([query4 - 128, query4]))
    query16 = np.arange(128)
    mask16 = band(query16, np.concatenate([query16 - 128, query16]))
    return dict(
        cos=np.cos(inner).astype(np.float32),
        sin=np.sin(inner).astype(np.float32),
        anchors=anchors.astype(np.float32),
        perm=perm,
        mask1=mask1,
        mask4=mask4,
        mask16=mask16,
    )


def dot(a, b):
    return lax.dot_general(a, b, (((1,), (0,)), ((), ())), preferred_element_type=F32)


def dot_t(a, b):
    return lax.dot_general(a, b, (((1,), (1,)), ((), ())), preferred_element_type=F32)


def half(rows):
    return lax.broadcasted_iota(jnp.int32, (rows, 128), 1) < 64


def pack_kernel(
    index_ref, core_ref, q_hbm, k_hbm, v_hbm, perm_hbm, cos_hbm, sin_hbm, anchor_hbm, out_hbm, halo_ref,
    q_ref, k_ref, v_ref, perm_ref, cos_ref, sin_ref, anchor_ref, out_ref, sems, out_sems,
):
    pairs = (
        (anchor_hbm, anchor_ref), (cos_hbm, cos_ref), (sin_hbm, sin_ref), (perm_hbm, perm_ref),
        (q_hbm, q_ref), (k_hbm, k_ref), (v_hbm, v_ref),
    )
    copies = [pltpu.make_async_copy(source, target, sems.at[n]) for n, (source, target) in enumerate(pairs)]
    for copy in copies:
        copy.start()
    for copy in copies:
        copy.wait()
    block = index_ref[0]
    fine = anchor_ref[pl.ds(block % 16, 1), :]
    coarse = anchor_ref[pl.ds(16 + block // 16, 1), :]
    cos_a = fine[:, :128] * coarse[:, :128] - fine[:, 128:] * coarse[:, 128:]
    sin_a = fine[:, 128:] * coarse[:, :128] + fine[:, :128] * coarse[:, 128:]
    lane = lax.broadcasted_iota(jnp.int32, (TOK, 128), 1)
    low64 = lane < 64
    low32 = (lane & 63) < 32
    sign = jnp.where(low32[:1], -1.0, 1.0).astype(F32)
    cosine = cos_a * cos_ref[...] - sin_a * sin_ref[...]
    sine = (sin_a * sign) * cos_ref[...] + (cos_a * sign) * sin_ref[...]

    def turn(rows):
        other = jnp.where(low32, pltpu.roll(rows, 96, 1), pltpu.roll(rows, 32, 1))
        return rows * cosine + other * sine

    perm = perm_ref[...]
    outgoing = []
    for j in range(4):
        cols = slice(128 * j, 128 * j + 128)
        query = turn(dot(perm, q_ref[:, cols])) * (1.0 / math.sqrt(HD))
        key = turn(dot(perm, k_ref[:, cols]))
        value = dot(perm, v_ref[:, cols])
        even, odd = 2 * j, 2 * j + 1
        packed = jnp.where(low64, key, pltpu.roll(value, 64, 1)).astype(BF)
        out_ref[even, 0:TOK] = packed
        halo_ref[even] = packed
        packed = jnp.where(low64, pltpu.roll(key, 64, 1), value).astype(BF)
        out_ref[odd, 0:TOK] = packed
        halo_ref[odd] = packed
        first, second = query[:128], query[128:]
        out_ref[even, TOK : TOK + 128] = jnp.where(low64[:128], first, pltpu.roll(second, 64, 1)).astype(BF)
        out_ref[odd, TOK : TOK + 128] = jnp.where(low64[:128], pltpu.roll(first, 64, 1), second).astype(BF)
        copy = pltpu.make_async_copy(out_ref.at[pl.ds(2 * j, 2)], out_hbm.at[pl.ds(2 * j, 2)], out_sems.at[j])
        copy.start()
        outgoing.append(copy)
    for copy in outgoing:
        copy.wait()


def wide(x, n):
    return jnp.concatenate([x] * n, axis=1) if n > 1 else x


def value_masks(rows):
    low = half(rows)
    return jnp.where(low, 1.0, 0.0).astype(BF), jnp.where(low, 0.0, 1.0).astype(BF)


def normal(total):
    return total / pltpu.roll(total, 64, 1)


def start_all(pairs, sems):
    copies = [pltpu.make_async_copy(source, target, sems.at[n]) for n, (source, target) in enumerate(pairs)]
    for copy in copies:
        copy.start()
    return copies


def row_max(scores):
    return jnp.max(scores, axis=1, keepdims=True)


def weights(scores, peak):
    return jnp.exp(scores - wide(peak, scores.shape[1] // 128)).astype(BF)


def own_kernel(
    own_ref, mask1_hbm, mask4_hbm, mask16_hbm, acc_hbm, top_hbm, qs_hbm,
    acc_ref, top_ref, qs_ref, mask1_ref, mask4_ref, mask16_ref, vs, s16, s4, s1, p16, p4, p1, mask_sems, sems,
):
    loads = start_all(((mask16_hbm, mask16_ref), (mask4_hbm, mask4_ref), (mask1_hbm, mask1_ref)), mask_sems)
    low256, high256 = value_masks(TOK)
    low_bf = low256[:128]
    for i in range(GROUP):
        packed = own_ref[i, TOK : TOK + 128]
        qs_ref[i, 0:128] = packed * low_bf
        qs_ref[i, 128:256] = pltpu.roll(packed.astype(F32), 64, 1).astype(BF) * low_bf
        vs[i, 0:TOK] = own_ref[i, 0:TOK] * high256 + low256

    def at4(n):
        b, r = n // 4, n % 4
        seen = slice(max(0, 2 * b - 2), 2 * b + 2)
        return slice(2 * b, 2 * b + 2), slice(64 * r, 64 * r + 64), seen, 64 * (seen.stop - seen.start)

    def at1(i):
        seen = slice(max(0, i - 1), i + 1)
        return seen, TOK * (seen.stop - seen.start)

    for load in loads:
        load.wait()
    for r in range(16):
        rows = slice(16 * r, 16 * r + 16)
        scores = dot_t(qs_ref[:, rows].reshape(128, 128), own_ref[:, rows].reshape(128, 128)) + mask16_ref[:, 128:256]
        s16[r] = scores
        top_ref[:, rows] = jnp.broadcast_to(row_max(scores), (128, 128)).reshape(8, 16, 128)
    for n in range(16):
        at, rows, seen, width = at4(n)
        scores = dot_t(qs_ref[at, rows].reshape(128, 128), own_ref[seen, rows].reshape(width, 128))
        scores = scores + mask4_ref[:, 256 - width : 256]
        s4[n, :, 0:width] = scores
        top_ref[at, rows] = jnp.maximum(top_ref[at, rows].reshape(128, 128), row_max(scores)).reshape(2, 64, 128)
    for i in range(GROUP):
        seen, width = at1(i)
        scores = dot_t(qs_ref[i, 0:TOK], own_ref[seen, 0:TOK].reshape(width, 128)) + mask1_ref[:, 512 - width : 512]
        s1[i, :, 0:width] = scores
        top_ref[i, 0:TOK] = jnp.maximum(top_ref[i, 0:TOK], row_max(scores))
    copies = [
        pltpu.make_async_copy(source, target, sems.at[n])
        for n, (source, target) in enumerate(((qs_ref, qs_hbm), (top_ref, top_hbm), (acc_ref, acc_hbm)))
    ]
    copies[0].start()
    copies[1].start()
    for r in range(16):
        p16[r] = weights(s16[r], top_ref[:, 16 * r : 16 * r + 16].reshape(128, 128))
    for n in range(16):
        at, rows, seen, width = at4(n)
        p4[n, :, 0:width] = weights(s4[n, :, 0:width], top_ref[at, rows].reshape(128, 128))
    for i in range(GROUP):
        seen, width = at1(i)
        p1[i, :, 0:width] = weights(s1[i, :, 0:width], top_ref[i, 0:TOK])
    for r in range(16):
        rows = slice(16 * r, 16 * r + 16)
        acc_ref[:, rows] = dot(p16[r], vs[:, rows].reshape(128, 128)).reshape(8, 16, 128)
    for n in range(16):
        at, rows, seen, width = at4(n)
        acc_ref[at, rows] += dot(p4[n, :, 0:width], vs[seen, rows].reshape(width, 128)).reshape(2, 64, 128)
    for i in range(GROUP):
        seen, width = at1(i)
        acc_ref[i, 0:TOK] += dot(p1[i, :, 0:width], vs[seen, 0:TOK].reshape(width, 128))
    copies[2].start()
    for copy in copies:
        copy.wait()


def halo_kernel(
    index_ref, halo_ref, qs_hbm, top_hbm, mask16_hbm, mask4_hbm, mask1_hbm, acc_hbm, perm_hbm,
    out_ref, qs_ref, top_ref, mask16_ref, mask4_ref, mask1_ref, acc_ref, perm_ref,
    vs, peak, s16, s4, s1, p16, p4, p1, sems,
):
    copies = start_all(
        (
            (qs_hbm, qs_ref), (top_hbm, top_ref), (mask16_hbm, mask16_ref), (mask4_hbm, mask4_ref),
            (mask1_hbm, mask1_ref), (acc_hbm, acc_ref), (perm_hbm, perm_ref),
        ),
        sems,
    )
    bias = jnp.where(index_ref[0] < GROUP, NEG, 0.0).astype(F32)
    low256, high256 = value_masks(TOK)
    for i in range(GROUP):
        vs[i, 0:TOK] = halo_ref[i] * high256 + low256

    def blocks(ref, rows):
        return jnp.concatenate([ref[4:8, rows], ref[0:4, rows]], axis=0).reshape(128, 128)

    def last_two(ref, rows):
        return ref[2:4, rows].reshape(128, 128)

    for copy in copies[:5]:
        copy.wait()
    mask16 = mask16_ref[:, 0:128] + bias
    for r in range(16):
        rows = slice(16 * r, 16 * r + 16)
        scores = dot_t(qs_ref[:, rows].reshape(128, 128), blocks(halo_ref, rows)) + mask16
        s16[r] = scores
        peak[:, rows] = jnp.maximum(top_ref[:, rows].reshape(128, 128), row_max(scores)).reshape(8, 16, 128)
    mask4 = mask4_ref[:, 0:128] + bias
    for r in range(4):
        rows = slice(64 * r, 64 * r + 64)
        scores = dot_t(qs_ref[0:2, rows].reshape(128, 128), last_two(halo_ref, rows)) + mask4
        s4[r] = scores
        peak[0:2, rows] = jnp.maximum(peak[0:2, rows].reshape(128, 128), row_max(scores)).reshape(2, 64, 128)
    scores = dot_t(qs_ref[0, 0:TOK], halo_ref[3]) + (mask1_ref[:, 0:TOK] + bias)
    s1[...] = scores
    peak[0, 0:TOK] = jnp.maximum(peak[0, 0:TOK], row_max(scores))
    for r in range(16):
        p16[r] = weights(s16[r], peak[:, 16 * r : 16 * r + 16].reshape(128, 128))
    for r in range(4):
        p4[r] = weights(s4[r], peak[0:2, 64 * r : 64 * r + 64].reshape(128, 128))
    p1[...] = weights(s1[...], peak[0, 0:TOK])
    copies[5].wait()
    copies[6].wait()
    for i in range(GROUP):
        peak[i, 0:TOK] = acc_ref[i, 0:TOK] * jnp.exp(top_ref[i, 0:TOK] - peak[i, 0:TOK])
    new = peak
    for r in range(16):
        rows = slice(16 * r, 16 * r + 16)
        new[:, rows] += dot(p16[r], blocks(vs, rows)).reshape(8, 16, 128)
    for r in range(4):
        rows = slice(64 * r, 64 * r + 64)
        new[0:2, rows] += dot(p4[r], last_two(vs, rows)).reshape(2, 64, 128)
    new[0, 0:TOK] += dot(p1[...], vs[3, 0:TOK])
    low_rows = half(64)
    for i in range(GROUP):
        mixed = normal(new[i, 0:TOK]).astype(BF) * high256
        natural = dot(perm_ref[...], mixed)
        out_ref[2 * i] = jnp.where(low_rows, pltpu.roll(natural[0:64], 64, 1), natural[64:128]).astype(BF)
        out_ref[2 * i + 1] = jnp.where(low_rows, pltpu.roll(natural[128:192], 64, 1), natural[192:256]).astype(BF)


def project_kernel(core_ref, rows_ref, own_ref, other_ref, out_ref, mixed):
    low = half(64)
    for side in range(2):
        core = core_ref[0] if side == 0 else 1 - core_ref[0]
        for j in range(4):
            first = rows_ref[4 * j + core].astype(F32)
            second = rows_ref[4 * j + 2 + core].astype(F32)
            cols = slice(128 * j, 128 * j + 128)
            mixed[side, 0:64, cols] = jnp.where(low, first, pltpu.roll(second, 64, 1)).astype(BF)
            mixed[side, 64:128, cols] = jnp.where(low, pltpu.roll(first, 64, 1), second).astype(BF)
    for n in range(4):
        cols = slice(512 * n, 512 * n + 512)
        out_ref[:, cols] = (dot(mixed[0], own_ref[:, cols]) + dot(mixed[1], other_ref[:, cols])).astype(BF)


def vmem():
    return pl.BlockSpec(memory_space=pltpu.VMEM)


def limit(mib):
    return pltpu.CompilerParams(vmem_limit_bytes=mib * 2**20)


def per_device(query_rows, key_rows, value_rows, out_weight, blocks):
    tables = make_tables(blocks)
    index = lax.axis_index(SP).astype(jnp.int32).reshape(1)
    core = lax.axis_index("tp").astype(jnp.int32).reshape(1)

    smem = pl.BlockSpec(memory_space=pltpu.SMEM)
    hbm = pl.BlockSpec(memory_space=pltpu.HBM)
    send, keys_values = pl.pallas_call(
        pack_kernel,
        in_specs=[smem] * 2 + [hbm] * 7,
        out_specs=[hbm, vmem()],
        out_shape=[
            pltpu.HBM((GROUP, TOK + 128, 128), BF),
            jax.ShapeDtypeStruct((GROUP, TOK, 128), BF),
        ],
        scratch_shapes=[
            pltpu.VMEM((TOK, 512), BF),
            pltpu.VMEM((TOK, 512), BF),
            pltpu.VMEM((TOK, 512), BF),
            pltpu.VMEM((TOK, TOK), BF),
            pltpu.VMEM((TOK, 128), F32),
            pltpu.VMEM((TOK, 128), F32),
            pltpu.VMEM((16 + blocks // 16, 256), F32),
            pltpu.VMEM((GROUP, TOK + 128, 128), BF),
            pltpu.SemaphoreType.DMA((7,)),
            pltpu.SemaphoreType.DMA((4,)),
        ],
        compiler_params=limit(12),
        name="pack",
    )(
        index,
        core,
        *(
            pltpu.with_memory_space_constraint(array, pltpu.HBM)
            for array in (
                query_rows,
                key_rows,
                value_rows,
                jnp.asarray(tables["perm"], BF),
                jnp.asarray(tables["cos"]),
                jnp.asarray(tables["sin"]),
                jnp.asarray(tables["anchors"]),
            )
        ),
    )
    following = [(s, (s // GROUP + 1) * GROUP + ((s % GROUP) ^ 4)) for s in range(blocks - GROUP)]
    shifted = lax.ppermute(keys_values, SP, following)
    own = lax.all_to_all(send, ("b", "x"), 0, 0, tiled=True)
    shifted, _ = lax.optimization_barrier((shifted, own))
    halo = lax.all_to_all(shifted, ("b", "x"), 0, 0, tiled=True)
    weight, _ = lax.optimization_barrier((out_weight, keys_values))
    other_weight = lax.ppermute(weight, "tp", [(0, 1), (1, 0)])
    mask1, mask4, mask16 = (jnp.asarray(tables[name]) for name in ("mask1", "mask4", "mask16"))
    mask1, mask4, mask16 = (pltpu.with_memory_space_constraint(x, pltpu.HBM) for x in (mask1, mask4, mask16))
    acc, top, qs = pl.pallas_call(
        own_kernel,
        in_specs=[vmem()] + [hbm] * 3,
        out_specs=[hbm] * 3,
        out_shape=[
            pltpu.HBM((GROUP, TOK + 8, 128), F32),
            pltpu.HBM((GROUP, TOK + 8, 128), F32),
            pltpu.HBM((GROUP, TOK + 16, 128), BF),
        ],
        scratch_shapes=[
            pltpu.VMEM((GROUP, TOK + 8, 128), F32),
            pltpu.VMEM((GROUP, TOK + 8, 128), F32),
            pltpu.VMEM((GROUP, TOK + 16, 128), BF),
            pltpu.VMEM((TOK, 2 * TOK), F32),
            pltpu.VMEM((128, 256), F32),
            pltpu.VMEM((128, 256), F32),
            pltpu.VMEM((GROUP, TOK + 16, 128), BF),
            pltpu.VMEM((16, 128, 128), F32),
            pltpu.VMEM((16, 128, 256), F32),
            pltpu.VMEM((GROUP, TOK, 512), F32),
            pltpu.VMEM((16, 128, 128), BF),
            pltpu.VMEM((16, 128, 256), BF),
            pltpu.VMEM((GROUP, TOK, 512), BF),
            pltpu.SemaphoreType.DMA((3,)),
            pltpu.SemaphoreType.DMA((3,)),
        ],
        compiler_params=limit(24),
        cost_estimate=pl.CostEstimate(flops=20 * 10**9, bytes_accessed=2 * 2**20, transcendentals=0),
        name="attend_own",
    )(own, mask1, mask4, mask16)
    back = pl.pallas_call(
        halo_kernel,
        in_specs=[smem, vmem()] + [hbm] * 7,
        out_specs=vmem(),
        out_shape=jax.ShapeDtypeStruct((2 * GROUP, 64, 128), BF),
        scratch_shapes=[
            pltpu.VMEM((GROUP, TOK + 16, 128), BF),
            pltpu.VMEM((GROUP, TOK + 8, 128), F32),
            pltpu.VMEM((128, 256), F32),
            pltpu.VMEM((128, 256), F32),
            pltpu.VMEM((TOK, 2 * TOK), F32),
            pltpu.VMEM((GROUP, TOK + 8, 128), F32),
            pltpu.VMEM((TOK, TOK), BF),
            pltpu.VMEM((GROUP, TOK + 16, 128), BF),
            pltpu.VMEM((GROUP, TOK + 8, 128), F32),
            pltpu.VMEM((16, 128, 128), F32),
            pltpu.VMEM((4, 128, 128), F32),
            pltpu.VMEM((TOK, TOK), F32),
            pltpu.VMEM((16, 128, 128), BF),
            pltpu.VMEM((4, 128, 128), BF),
            pltpu.VMEM((TOK, TOK), BF),
            pltpu.SemaphoreType.DMA((7,)),
        ],
        compiler_params=limit(16),
        cost_estimate=pl.CostEstimate(flops=4 * 10**9, bytes_accessed=2 * 2**20, transcendentals=0),
        name="attend_halo",
    )(
        index,
        halo,
        *(
            pltpu.with_memory_space_constraint(x, pltpu.HBM)
            for x in (qs, top, mask16, mask4, mask1, acc, jnp.asarray(tables["perm"].T, BF))
        ),
    )
    back, other_weight = lax.optimization_barrier((back, other_weight))
    rows = lax.all_to_all(back, ("b", "x", "tp"), 0, 0, tiled=True)
    return pl.pallas_call(
        project_kernel,
        in_specs=[smem] + [vmem()] * 3,
        out_specs=vmem(),
        out_shape=jax.ShapeDtypeStruct((TOK // 2, 2048), BF),
        scratch_shapes=[pltpu.VMEM((2, TOK // 2, 512), BF)],
        compiler_params=limit(16),
        name="project",
    )(core, rows, out_weight, other_weight)


def solution(mesh):
    blocks = mesh.shape["sp"]
    fine = Mesh(mesh.devices.reshape(blocks // 16, 2, 2, 4, 2), SP + ("tp",))
    return jax.shard_map(
        functools.partial(per_device, blocks=blocks),
        mesh=fine,
        in_specs=(P(SP, "tp"), P(SP, "tp"), P(SP, "tp"), P("tp", None)),
        out_specs=P(SP + ("tp",), None),
        check_vma=False,
    )
```

time: 53.9 us -> 58.1 us (1.078)
  the two profiles are of different devices: /device:TPU:256 before, /device:TPU:384 now
where the time goes in v3:
time: 58.1 us; the launch traced here: 57.7 us
  starting transfers between devices  17.1 us (29%)
  waiting for transfers between devices  15.2 us (26%)
  Pallas kernels  14.8 us (25%)
  blocking collectives  10.5 us (18%)
    ppermute x1, waiting for transfers between devices, per_device(): shifted = lax.ppermute(keys_values, SP, following)  11.4 us
    all_to_all x1, blocking collectives, per_device(): rows = lax.all_to_all(back, ('b', 'x', 'tp'), 0, 0, tiled=True)  10.5 us
    ppermute x1, starting transfers between devices, per_device(): shifted = lax.ppermute(keys_values, SP, following)  5.35 us
    all_to_all x1, starting transfers between devices, per_device(): own = lax.all_to_all(send, ('b', 'x'), 0, 0, tiled=True)  5.33 us
    pallas_call x1, Pallas kernels, per_device(): pl.pallas_call(own_kernel, in_specs=[vmem()] + [hbm] * 3, out_specs=[hbm]...  4.85 us
    all_to_all x1, starting transfers between devices, per_device(): halo = lax.all_to_all(shifted, ('b', 'x'), 0, 0, tiled=True)  4.52 us
    all_to_all x1, waiting for transfers between devices, per_device(): halo = lax.all_to_all(shifted, ('b', 'x'), 0, 0, tiled=True)  3.83 us
    pallas_call x1, Pallas kernels, per_device(): pl.pallas_call(halo_kernel, in_specs=[smem, vmem()] + [hbm] * 7, out_spec...  3.43 us
  transfers between devices with their start and end apart: 4, of which 2 were waited for; matrix products, arithmetic and copies ran while one was open for 0% of the time, Pallas kernels for 14%

profile of v3, /device:TPU:384, one launch (start us, length us, event | category | flops | bytes accessed | tf_op | source)
XLA Modules:
  0.0 57.7 jit_solution(2980861435984385939)
XLA Ops:
  0.0 0.0 copy-start
  0.0 3.3 %pack.1 = (bf16[8,384,128]{2,1,0:T(8,128)(2,1)}, bf16[8,256,128]{2,1,0:T(8,128)(2,1)S(1)}) custom-call(s32[1]{0:T(128)} %bitcast.1.index_ref, s32[1]{0:T(128)} %bitcast.core_ref, bf16[256,512]{1,0:T(8,128)(2,1)} %q_hbm.1, bf16[256,512]{1,0:T(8,128)(2,1)} %k_hbm.1, bf16[256,512]{1,0:T(8,128)(2,1)} %v_hbm.1, bf16[256,256]{1,0:T(8,128)(2,1)} %constant.42.clone.perm_hbm, ...), custom_call_target="tpu_custom_call" | custom-call | tf_op jit(solution)/shard_map/pack/pallas_call | solution.py:320
  3.3 5.3 %all-to-all-start = ((bf16[8,384,128]{2,1,0:T(8,128)(2,1)}), bf16[8,384,128]{2,1,0:T(8,128)(2,1)S(1)}, u32[]{:S(2)}, u32[]{:S(2)}) async-start(bf16[8,384,128]{2,1,0:T(8,128)(2,1)} %get-tuple-element.15), calls=%async_computation | async-start | bytes 1572864 | tf_op jit(solution)/shard_map/all_to_all | solution.py:360
  8.7 5.4 %collective-permute-start = (bf16[8,256,128]{2,1,0:T(8,128)(2,1)S(1)}, bf16[8,256,128]{2,1,0:T(8,128)(2,1)}, u32[]{:S(2)}, u32[]{:S(2)}) collective-permute-start(bf16[8,256,128]{2,1,0:T(8,128)(2,1)S(1)} %get-tuple-element.14), channel_id=1, source_target_pairs={{0,24},{2,26},{4,28},{6,30},{8,16},{10,18},{12,20},{14,22},{16,40}... | collective-permute-start | bytes 1572872 | tf_op jit(solution)/shard_map/ppermute | solution.py:359
  14.0 0.0 copy-done
  14.0 1.9 %collective-permute-start.1 = (bf16[512,2048]{1,0:T(8,128)(2,1)S(1)}, bf16[512,2048]{1,0:T(8,128)(2,1)}, u32[]{:S(2)}, u32[]{:S(2)}) collective-permute-start(bf16[512,2048]{1,0:T(8,128)(2,1)S(1)} %copy-done), channel_id=1, source_target_pairs={{0,1},{1,0},{2,3},{3,2},{4,5},{5,4},{6,7},{7,6},{8,9},{9,8},{10,11... | collective-permute-start | bytes 6291464 | tf_op jit(solution)/shard_map/ppermute | solution.py:364
  16.0 11.4 %collective-permute-done = bf16[8,256,128]{2,1,0:T(8,128)(2,1)} collective-permute-done((bf16[8,256,128]{2,1,0:T(8,128)(2,1)S(1)}, bf16[8,256,128]{2,1,0:T(8,128)(2,1)}, u32[]{:S(2)}, u32[]{:S(2)}) %collective-permute-start) | collective-permute-done | bytes 524320 | tf_op jit(solution)/shard_map/ppermute | solution.py:359
  27.4 0.0 all-to-all-done.own_ref
  27.4 4.5 %all-to-all-start.1 = ((bf16[8,256,128]{2,1,0:T(8,128)(2,1)}), bf16[8,256,128]{2,1,0:T(8,128)(2,1)S(1)}, u32[]{:S(2)}, u32[]{:S(2)}) async-start(bf16[8,256,128]{2,1,0:T(8,128)(2,1)} %collective-permute-done), calls=%async_computation.1 | async-start | bytes 1048576 | tf_op jit(solution)/shard_map/all_to_all | solution.py:362
  31.9 4.9 %attend_own.1 = (f32[8,264,128]{2,1,0:T(8,128)}, f32[8,264,128]{2,1,0:T(8,128)}, bf16[8,272,128]{2,1,0:T(8,128)(2,1)}) custom-call(bf16[8,384,128]{2,1,0:T(8,128)(2,1)S(1)} %all-to-all-done.own_ref, f32[256,512]{1,0:T(8,128)} %constant.46.clone.mask1_hbm, f32[128,256]{1,0:T(8,128)} %constant.47.clone.mask4_hbm, f32[128,256]{1,0:T(8,128)} %constant.48.clone.mask16_hbm), custom_call_target="tpu_custom_call" | custom-call | flops 20000000000 | bytes 2097152 | tf_op jit(solution)/shard_map/attend_own/pallas_call | solution.py:367
  36.7 3.8 %all-to-all-done.1.halo_ref = bf16[8,256,128]{2,1,0:T(8,128)(2,1)S(1)} async-done(((bf16[8,256,128]{2,1,0:T(8,128)(2,1)}), bf16[8,256,128]{2,1,0:T(8,128)(2,1)S(1)}, u32[]{:S(2)}, u32[]{:S(2)}) %all-to-all-start.1) | async-done | bytes 524320 | tf_op jit(solution)/shard_map/all_to_all | solution.py:362
  40.6 3.4 %attend_halo.1 = bf16[16,64,128]{2,1,0:T(8,128)(2,1)S(1)} custom-call(s32[1]{0:T(128)} %bitcast.1.index_ref, bf16[8,256,128]{2,1,0:T(8,128)(2,1)S(1)} %all-to-all-done.1.halo_ref, bf16[8,272,128]{2,1,0:T(8,128)(2,1)} %get-tuple-element.17.qs_hbm, f32[8,264,128]{2,1,0:T(8,128)} %get-tuple-element.18.top_hbm, f32[128,256]{1,0:T(8,128)} %constant.48.clone.mask16_hbm, ...), custom_call_target="tpu_custom_call" | custom-call | flops 4000000000 | bytes 2097152 | tf_op jit(solution)/shard_map/attend_halo/pallas_call | solution.py:397
  44.0 0.0 collective-permute-done.1.other_ref
  44.0 10.5 %all_to_all.15.rows_ref = bf16[16,64,128]{2,1,0:T(8,128)(2,1)S(1)} all-to-all(bf16[16,64,128]{2,1,0:T(8,128)(2,1)S(1)} %attend_halo.1), channel_id=1, replica_groups=mesh['z'=16,'g'=2,'b'=2,'x'=4,'tp'=2] {'b','x','tp'}, dimensions={0} | all-to-all | bytes 524288 | tf_op jit(solution)/shard_map/all_to_all | solution.py:432
  54.5 3.2 %project.1 = bf16[128,2048]{1,0:T(8,128)(2,1)} custom-call(s32[1]{0:T(128)} %bitcast.core_ref, bf16[16,64,128]{2,1,0:T(8,128)(2,1)S(1)} %all_to_all.15.rows_ref, bf16[512,2048]{1,0:T(8,128)(2,1)S(1)} %copy-done, bf16[512,2048]{1,0:T(8,128)(2,1)} %collective-permute-done.1.other_ref), custom_call_target="tpu_custom_call" | custom-call | tf_op jit(solution)/shard_map/project/pallas_call | solution.py:433
Async XLA Ops:
  0.0 14.0 %copy-start = (bf16[512,2048]{1,0:T(8,128)(2,1)S(1)}, bf16[512,2048]{1,0:T(8,128)(2,1)}, u32[]{:S(2)}) copy-start(bf16[512,2048]{1,0:T(8,128)(2,1)} %own_ref.1) | copy-start | bytes 6291460
  3.3 24.0 %all-to-all-start = ((bf16[8,384,128]{2,1,0:T(8,128)(2,1)}), bf16[8,384,128]{2,1,0:T(8,128)(2,1)S(1)}, u32[]{:S(2)}, u32[]{:S(2)}) async-start(bf16[8,384,128]{2,1,0:T(8,128)(2,1)} %get-tuple-element.15), calls=%async_computation | async-start | bytes 1572864 | tf_op jit(solution)/shard_map/all_to_all | solution.py:360
  8.7 18.7 %collective-permute-start = (bf16[8,256,128]{2,1,0:T(8,128)(2,1)S(1)}, bf16[8,256,128]{2,1,0:T(8,128)(2,1)}, u32[]{:S(2)}, u32[]{:S(2)}) collective-permute-start(bf16[8,256,128]{2,1,0:T(8,128)(2,1)S(1)} %get-tuple-element.14), channel_id=1, source_target_pairs={{0,24},{2,26},{4,28},{6,30},{8,16},{10,18},{12,20},{14,22},{16,40}... | collective-permute-start | bytes 1572872 | tf_op jit(solution)/shard_map/ppermute | solution.py:359
  14.0 30.0 %collective-permute-start.1 = (bf16[512,2048]{1,0:T(8,128)(2,1)S(1)}, bf16[512,2048]{1,0:T(8,128)(2,1)}, u32[]{:S(2)}, u32[]{:S(2)}) collective-permute-start(bf16[512,2048]{1,0:T(8,128)(2,1)S(1)} %copy-done), channel_id=1, source_target_pairs={{0,1},{1,0},{2,3},{3,2},{4,5},{5,4},{6,7},{7,6},{8,9},{9,8},{10,11... | collective-permute-start | bytes 6291464 | tf_op jit(solution)/shard_map/ppermute | solution.py:364
  27.4 13.2 %all-to-all-start.1 = ((bf16[8,256,128]{2,1,0:T(8,128)(2,1)}), bf16[8,256,128]{2,1,0:T(8,128)(2,1)S(1)}, u32[]{:S(2)}, u32[]{:S(2)}) async-start(bf16[8,256,128]{2,1,0:T(8,128)(2,1)} %collective-permute-done), calls=%async_computation.1 | async-start | bytes 1048576 | tf_op jit(solution)/shard_map/all_to_all | solution.py:362

commit v4 on v2

--- a/solution.py
+++ b/solution.py
@@ -17,6 +17,7 @@
 GROUP = 8
 SP = ("z", "g", "b", "x")
 NEG = -1e30
+FIRST = 192
 BF = jnp.bfloat16
 F32 = jnp.float32
 
@@ -78,13 +79,13 @@
     q_ref, k_ref, v_ref, perm_ref, cos_ref, sin_ref, anchor_ref, sems,
 ):
     pairs = (
-        (anchor_hbm, anchor_ref), (cos_hbm, cos_ref), (sin_hbm, sin_ref), (perm_hbm, perm_ref),
-        (q_hbm, q_ref), (k_hbm, k_ref), (v_hbm, v_ref),
+        (perm_hbm, perm_ref), (k_hbm, k_ref), (anchor_hbm, anchor_ref), (cos_hbm, cos_ref), (sin_hbm, sin_ref),
+        (v_hbm, v_ref), (q_hbm, q_ref),
     )
     copies = [pltpu.make_async_copy(source, target, sems.at[n]) for n, (source, target) in enumerate(pairs)]
     for copy in copies:
         copy.start()
-    for copy in copies:
+    for copy in copies[2:5]:
         copy.wait()
     block = index_ref[0]
     flip = 4 * ((block // GROUP) % 2)
@@ -103,16 +104,23 @@
         other = jnp.where(low32, pltpu.roll(rows, 96, 1), pltpu.roll(rows, 32, 1))
         return rows * cosine + other * sine
 
+    copies[0].wait()
+    copies[1].wait()
     perm = perm_ref[...]
+    keys = [turn(dot(perm, k_ref[:, 128 * j : 128 * j + 128])) for j in range(4)]
+    copies[5].wait()
     for j in range(4):
-        cols = slice(128 * j, 128 * j + 128)
-        query = turn(dot(perm, q_ref[:, cols])) * (1.0 / math.sqrt(HD))
-        key = turn(dot(perm, k_ref[:, cols]))
-        value = dot(perm, v_ref[:, cols])
+        key = keys[j]
+        value = dot(perm, v_ref[:, 128 * j : 128 * j + 128])
         even = (2 * j) ^ flip
         odd = even + 1
         out_ref[even, 0:TOK] = jnp.where(low64, key, pltpu.roll(value, 64, 1)).astype(BF)
         out_ref[odd, 0:TOK] = jnp.where(low64, pltpu.roll(key, 64, 1), value).astype(BF)
+    copies[6].wait()
+    for j in range(4):
+        query = turn(dot(perm, q_ref[:, 128 * j : 128 * j + 128])) * (1.0 / math.sqrt(HD))
+        even = (2 * j) ^ flip
+        odd = even + 1
         first, second = query[:128], query[128:]
         out_ref[even, TOK : TOK + 128] = jnp.where(low64[:128], first, pltpu.roll(second, 64, 1)).astype(BF)
         out_ref[odd, TOK : TOK + 128] = jnp.where(low64[:128], pltpu.roll(first, 64, 1), second).astype(BF)
@@ -139,16 +147,14 @@
     return jnp.exp(scores - wide(peak, scores.shape[1] // 128)).astype(BF)
 
 
-def own_kernel(own_ref, mask1_ref, mask4_ref, mask16_ref, acc_ref, top_ref, qs_ref, ks, vs, s16, s4, s1, p16, p4, p1):
+def own_kernel(own_ref, mask1_ref, mask4_ref, mask16_ref, acc_ref, top_ref, qs_ref, vs, s16, s4, s1, p16, p4, p1):
     low256, high256 = value_masks(TOK)
     low_bf = low256[:128]
     for i in range(GROUP):
         packed = own_ref[i, TOK : TOK + 128]
         qs_ref[i, 0:128] = packed * low_bf
         qs_ref[i, 128:256] = pltpu.roll(packed.astype(F32), 64, 1).astype(BF) * low_bf
-        key = own_ref[i, 0:TOK]
-        ks[i, 0:TOK] = key
-        vs[i, 0:TOK] = key * high256 + low256
+        vs[i, 0:TOK] = own_ref[i, 0:TOK] * high256 + low256
 
     def at4(n):
         b, r = n // 4, n % 4
@@ -161,18 +167,18 @@
 
     for r in range(16):
         rows = slice(16 * r, 16 * r + 16)
-        scores = dot_t(qs_ref[:, rows].reshape(128, 128), ks[:, rows].reshape(128, 128)) + mask16_ref[:, 128:256]
+        scores = dot_t(qs_ref[:, rows].reshape(128, 128), own_ref[:, rows].reshape(128, 128)) + mask16_ref[:, 128:256]
         s16[r] = scores
         top_ref[:, rows] = jnp.broadcast_to(row_max(scores), (128, 128)).reshape(8, 16, 128)
     for n in range(16):
         at, rows, seen, width = at4(n)
-        scores = dot_t(qs_ref[at, rows].reshape(128, 128), ks[seen, rows].reshape(width, 128))
+        scores = dot_t(qs_ref[at, rows].reshape(128, 128), own_ref[seen, rows].reshape(width, 128))
         scores = scores + mask4_ref[:, 256 - width : 256]
         s4[n, :, 0:width] = scores
         top_ref[at, rows] = jnp.maximum(top_ref[at, rows].reshape(128, 128), row_max(scores)).reshape(2, 64, 128)
     for i in range(GROUP):
         seen, width = at1(i)
-        scores = dot_t(qs_ref[i, 0:TOK], ks[seen, 0:TOK].reshape(width, 128)) + mask1_ref[:, 512 - width : 512]
+        scores = dot_t(qs_ref[i, 0:TOK], own_ref[seen, 0:TOK].reshape(width, 128)) + mask1_ref[:, 512 - width : 512]
         s1[i, :, 0:width] = scores
         top_ref[i, 0:TOK] = jnp.maximum(top_ref[i, 0:TOK], row_max(scores))
     for r in range(16):
@@ -194,86 +200,92 @@
         acc_ref[i, 0:TOK] += dot(p1[i, :, 0:width], vs[seen, 0:TOK].reshape(width, 128))
 
 
-def halo_rows(index_ref, acc_ref, top_ref, qs_ref, masks, scratch, base):
+def gather(ref, count, start, n, blocks):
+    return jnp.concatenate([ref[count * i + start : count * i + start + n] for i in blocks], axis=0)
+
+
+def halo_rows(index_ref, acc_ref, top_ref, qs_ref, masks, base, count, ks, vs, near, near_values, scratch):
     mask1_ref, mask4_ref, mask16_ref = masks
-    ks, vs, new, peak, s16, s4, s1, p16, p4, p1 = scratch
+    new, peak, s16, s4, s1, p16, p4, p1 = scratch
     bias = jnp.where(index_ref[0] < GROUP, NEG, 0.0).astype(F32)
-    half_rows = slice(base, base + 128)
-    order = (7, 8) if base == 0 else (8, 7)
-
-    def both(ref):
-        return jnp.concatenate([ref[order[0], 0:128], ref[order[1], 0:128]], axis=0)
+    span = slice(base, base + count)
+    every, last_two = range(GROUP), (6, 7)
 
     mask16 = mask16_ref[:, 0:128] + bias
-    for r in range(8):
+    for r in range(count // 16):
         rows = slice(16 * r, 16 * r + 16)
         full = slice(base + 16 * r, base + 16 * r + 16)
-        scores = dot_t(qs_ref[:, full].reshape(128, 128), ks[0:8, rows].reshape(128, 128)) + mask16
+        scores = dot_t(qs_ref[:, full].reshape(128, 128), gather(ks, count, 16 * r, 16, every)) + mask16
         s16[r] = scores
         peak[:, rows] = jnp.maximum(top_ref[:, full].reshape(128, 128), row_max(scores)).reshape(8, 16, 128)
     mask4 = mask4_ref[:, 0:128] + bias
-    for r in range(2):
+    for r in range(count // 64):
         rows = slice(64 * r, 64 * r + 64)
         full = slice(base + 64 * r, base + 64 * r + 64)
-        scores = dot_t(qs_ref[0:2, full].reshape(128, 128), ks[6:8, rows].reshape(128, 128)) + mask4
+        scores = dot_t(qs_ref[0:2, full].reshape(128, 128), gather(ks, count, 64 * r, 64, last_two)) + mask4
         s4[r] = scores
         peak[0:2, rows] = jnp.maximum(peak[0:2, rows].reshape(128, 128), row_max(scores)).reshape(2, 64, 128)
-    scores = dot_t(qs_ref[0, half_rows], both(ks)) + (mask1_ref[half_rows, 0:TOK] + bias)
+    scores = dot_t(qs_ref[0, span], near) + (mask1_ref[span, 0:TOK] + bias)
     s1[...] = scores
-    peak[0, 0:128] = jnp.maximum(peak[0, 0:128], row_max(scores))
-    for r in range(8):
+    peak[0, 0:count] = jnp.maximum(peak[0, 0:count], row_max(scores))
+    for r in range(count // 16):
         p16[r] = weights(s16[r], peak[:, 16 * r : 16 * r + 16].reshape(128, 128))
-    for r in range(2):
+    for r in range(count // 64):
         p4[r] = weights(s4[r], peak[0:2, 64 * r : 64 * r + 64].reshape(128, 128))
-    p1[...] = weights(s1[...], peak[0, 0:128])
-    for i in range(GROUP):
-        new[i, 0:128] = acc_ref[i, half_rows] * jnp.exp(top_ref[i, half_rows] - peak[i, 0:128])
-    for r in range(8):
+    p1[...] = weights(s1[...], peak[0, 0:count])
+    for i in range(GROUP):
+        new[i, 0:count] = acc_ref[i, span] * jnp.exp(top_ref[i, span] - peak[i, 0:count])
+    for r in range(count // 16):
         rows = slice(16 * r, 16 * r + 16)
-        new[:, rows] += dot(p16[r], vs[0:8, rows].reshape(128, 128)).reshape(8, 16, 128)
-    for r in range(2):
+        new[:, rows] += dot(p16[r], gather(vs, count, 16 * r, 16, every)).reshape(8, 16, 128)
+    for r in range(count // 64):
         rows = slice(64 * r, 64 * r + 64)
-        new[0:2, rows] += dot(p4[r], vs[6:8, rows].reshape(128, 128)).reshape(2, 64, 128)
-    new[0, 0:128] += dot(p1[...], both(vs))
-
-
-def spread(halo_ref, ks, vs, n):
-    low, high = value_masks(128)
-    for i in range(n):
-        key = halo_ref[i]
-        ks[i, 0:128] = key
-        vs[i, 0:128] = key * high + low
-
-
-def first_kernel(index_ref, acc_ref, top_ref, qs_ref, halo_ref, mask1_ref, mask4_ref, mask16_ref, lo_ref, *scratch):
-    ks, vs, new = scratch[:3]
-    spread(halo_ref, ks, vs, GROUP + 1)
-    halo_rows(index_ref, acc_ref, top_ref, qs_ref, (mask1_ref, mask4_ref, mask16_ref), scratch, 0)
-    _, high = value_masks(128)
-    for i in range(GROUP):
-        lo_ref[i, 0:128] = normal(new[i, 0:128]).astype(BF) * high
+        new[0:2, rows] += dot(p4[r], gather(vs, count, 64 * r, 64, last_two)).reshape(2, 64, 128)
+    new[0, 0:count] += dot(p1[...], near_values)
+
+
+def with_ones(keys_values):
+    low, high = value_masks(keys_values.shape[0])
+    return keys_values * high + low
+
+
+def first_kernel(index_ref, acc_ref, top_ref, qs_ref, halo_ref, mask1_ref, mask4_ref, mask16_ref, lo_ref, vs, *scratch):
+    for n in range(0, GROUP * FIRST + TOK - FIRST, 64):
+        vs[n : n + 64] = with_ones(halo_ref[n : n + 64])
+    near = slice(7 * FIRST, 7 * FIRST + TOK)
+    halo_rows(
+        index_ref, acc_ref, top_ref, qs_ref, (mask1_ref, mask4_ref, mask16_ref), 0, FIRST,
+        halo_ref, vs, halo_ref[near], vs[near], scratch,
+    )
+    new = scratch[0]
+    _, high = value_masks(FIRST)
+    for i in range(GROUP):
+        lo_ref[i] = normal(new[i, 0:FIRST]).astype(BF) * high
 
 
 def last_kernel(
     index_ref, acc_ref, top_ref, qs_ref, lo_ref, before_ref, halo_ref, perm_ref, mask1_ref, mask4_ref, mask16_ref,
-    out_ref, *scratch,
+    out_ref, vs, *scratch,
 ):
-    ks, vs, new = scratch[:3]
-    spread(halo_ref, ks, vs, GROUP)
-    low, high = value_masks(128)
-    key = before_ref[7]
-    ks[GROUP, 0:128] = key
-    vs[GROUP, 0:128] = key * high + low
-    halo_rows(index_ref, acc_ref, top_ref, qs_ref, (mask1_ref, mask4_ref, mask16_ref), scratch, 128)
+    count = TOK - FIRST
+    for n in range(0, GROUP * count, 64):
+        vs[n : n + 64] = with_ones(halo_ref[n : n + 64])
+    near = before_ref[7 * FIRST : 7 * FIRST + TOK]
+    halo_rows(
+        index_ref, acc_ref, top_ref, qs_ref, (mask1_ref, mask4_ref, mask16_ref), FIRST, count,
+        halo_ref, vs, near, with_ones(near), scratch,
+    )
+    new = scratch[0]
+    _, high = value_masks(count)
     low_rows = half(64)
     for i in range(GROUP):
-        mixed = jnp.concatenate([lo_ref[i, 0:128], normal(new[i, 0:128]).astype(BF) * high], axis=0)
+        mixed = jnp.concatenate([lo_ref[i], normal(new[i, 0:count]).astype(BF) * high], axis=0)
         natural = dot(perm_ref[...], mixed)
         out_ref[2 * i] = jnp.where(low_rows, pltpu.roll(natural[0:64], 64, 1), natural[64:128]).astype(BF)
         out_ref[2 * i + 1] = jnp.where(low_rows, pltpu.roll(natural[128:192], 64, 1), natural[192:256]).astype(BF)
 
 
-def project_kernel(index_ref, core_ref, rows_ref, own_ref, other_ref, out_ref, mixed):
+def project_kernel(index_ref, core_ref, rows_ref, own_ref, other_ref, out_hbm, mixed, out_ref, sems):
     low = half(64)
     flip = 4 * ((index_ref[0] // GROUP) % 2)
     for side in range(2):
@@ -284,9 +296,15 @@
             cols = slice(128 * j, 128 * j + 128)
             mixed[side, 0:64, cols] = jnp.where(low, first, pltpu.roll(second, 64, 1)).astype(BF)
             mixed[side, 64:128, cols] = jnp.where(low, pltpu.roll(first, 64, 1), second).astype(BF)
+    copies = []
     for n in range(4):
         cols = slice(512 * n, 512 * n + 512)
         out_ref[:, cols] = (dot(mixed[0], own_ref[:, cols]) + dot(mixed[1], other_ref[:, cols])).astype(BF)
+        copy = pltpu.make_async_copy(out_ref.at[:, cols], out_hbm.at[:, cols], sems.at[n])
+        copy.start()
+        copies.append(copy)
+    for copy in copies:
+        copy.wait()
 
 
 def vmem():
@@ -339,8 +357,9 @@
     )
     own = lax.all_to_all(send, ("b", "x"), 0, 0, tiled=True)
     following = [(s, (s // GROUP + 1) * GROUP + ((s % GROUP) ^ 4)) for s in range(blocks - GROUP)]
-    halo_a = lax.ppermute(jnp.concatenate([own[:, 0:128], own[7:8, 128:256]], axis=0), SP, following)
-    halo_b = lax.ppermute(own[:, 128:256], SP, following)
+    early = jnp.concatenate([own[:, 0:FIRST].reshape(GROUP * FIRST, 128), own[7, FIRST:TOK]], axis=0)
+    halo_a = lax.ppermute(early, SP, following)
+    halo_b = lax.ppermute(own[:, FIRST:TOK].reshape(GROUP * (TOK - FIRST), 128), SP, following)
     weight, _ = lax.optimization_barrier((out_weight, own))
     other_weight = lax.ppermute(weight, "tp", [(0, 1), (1, 0)])
     mask1, mask4, mask16 = (jnp.asarray(tables[name]) for name in ("mask1", "mask4", "mask16"))
@@ -351,7 +370,6 @@
         out_specs=[vmem()] * 3,
         out_shape=[state, state, jax.ShapeDtypeStruct((GROUP, TOK + 16, 128), BF)],
         scratch_shapes=[
-            pltpu.VMEM((GROUP, TOK + 16, 128), BF),
             pltpu.VMEM((GROUP, TOK + 16, 128), BF),
             pltpu.VMEM((16, 128, 128), F32),
             pltpu.VMEM((16, 128, 256), F32),
@@ -364,24 +382,26 @@
         cost_estimate=pl.CostEstimate(flops=20 * 10**9, bytes_accessed=2 * 2**20, transcendentals=0),
         name="attend_own",
     )(own, mask1, mask4, mask16)
-    scratch = [
-        pltpu.VMEM((GROUP + 1, 144, 128), BF),
-        pltpu.VMEM((GROUP + 1, 144, 128), BF),
-        pltpu.VMEM((GROUP, 136, 128), F32),
-        pltpu.VMEM((GROUP, 136, 128), F32),
-        pltpu.VMEM((8, 128, 128), F32),
-        pltpu.VMEM((2, 128, 128), F32),
-        pltpu.VMEM((128, TOK), F32),
-        pltpu.VMEM((8, 128, 128), BF),
-        pltpu.VMEM((2, 128, 128), BF),
-        pltpu.VMEM((128, TOK), BF),
-    ]
+
+    def scratch(total, count):
+        return [
+            pltpu.VMEM((total, 128), BF),
+            pltpu.VMEM((GROUP, count + 8, 128), F32),
+            pltpu.VMEM((GROUP, count + 8, 128), F32),
+            pltpu.VMEM((count // 16, 128, 128), F32),
+            pltpu.VMEM((count // 64, 128, 128), F32),
+            pltpu.VMEM((count, TOK), F32),
+            pltpu.VMEM((count // 16, 128, 128), BF),
+            pltpu.VMEM((count // 64, 128, 128), BF),
+            pltpu.VMEM((count, TOK), BF),
+        ]
+
     lo = pl.pallas_call(
         first_kernel,
         in_specs=[smem] + [vmem()] * 7,
         out_specs=vmem(),
-        out_shape=jax.ShapeDtypeStruct((GROUP, 144, 128), BF),
-        scratch_shapes=scratch,
+        out_shape=jax.ShapeDtypeStruct((GROUP, FIRST, 128), BF),
+        scratch_shapes=scratch(GROUP * FIRST + TOK - FIRST, FIRST),
         compiler_params=limit(16),
         cost_estimate=pl.CostEstimate(flops=4 * 10**9, bytes_accessed=2 * 2**20, transcendentals=0),
         name="attend_first",
@@ -391,7 +411,7 @@
         in_specs=[smem] + [vmem()] * 10,
         out_specs=vmem(),
         out_shape=jax.ShapeDtypeStruct((2 * GROUP, 64, 128), BF),
-        scratch_shapes=scratch,
+        scratch_shapes=scratch(GROUP * (TOK - FIRST), TOK - FIRST),
         compiler_params=limit(16),
         cost_estimate=pl.CostEstimate(flops=4 * 10**9, bytes_accessed=2 * 2**20, transcendentals=0),
         name="attend_last",
@@ -401,9 +421,13 @@
     return pl.pallas_call(
         project_kernel,
         in_specs=[smem] * 2 + [vmem()] * 3,
-        out_specs=vmem(),
-        out_shape=jax.ShapeDtypeStruct((TOK // 2, 2048), BF),
-        scratch_shapes=[pltpu.VMEM((2, TOK // 2, 512), BF)],
+        out_specs=hbm,
+        out_shape=pltpu.HBM((TOK // 2, 2048), BF),
+        scratch_shapes=[
+            pltpu.VMEM((2, TOK // 2, 512), BF),
+            pltpu.VMEM((TOK // 2, 2048), BF),
+            pltpu.SemaphoreType.DMA((4,)),
+        ],
         compiler_params=limit(16),
         name="project",
     )(index, core, rows, out_weight, other_weight)

time: 53.9 us -> 54.6 us (1.013)
  the two profiles are of different devices: /device:TPU:256 before, /device:TPU:384 now
where the time goes in v4:
time: 54.6 us; the launch traced here: 54.3 us
  blocking collectives  28.8 us (53%)
  starting transfers between devices  9.43 us (17%)
  Pallas kernels  9.18 us (17%)
  waiting for transfers between devices  6.68 us (12%)
    all_to_all x1, blocking collectives, per_device(): own = lax.all_to_all(send, ('b', 'x'), 0, 0, tiled=True)  18.3 us
    all_to_all x1, blocking collectives, per_device(): rows = lax.all_to_all(back, ('b', 'x', 'tp'), 0, 0, tiled=True)  10.5 us
    ppermute x1, waiting for transfers between devices, per_device(): halo_a = lax.ppermute(early, SP, following)  6.67 us
    ppermute x1, starting transfers between devices, per_device(): lax.ppermute(own[:, FIRST:TOK].reshape(GROUP * (TOK - FIRST), 128), SP, f...  3.91 us
    ppermute x1, starting transfers between devices, per_device(): halo_a = lax.ppermute(early, SP, following)  3.6 us
    pallas_call x1, Pallas kernels, per_device(): pl.pallas_call(own_kernel, in_specs=[vmem()] * 4, out_specs=[vmem()] * 3,...  2.75 us
    pallas_call x1, Pallas kernels, per_device(): pl.pallas_call(pack_kernel, in_specs=[smem] * 2 + [hbm] * 7, out_specs=vm...  2.71 us
    ppermute x1, starting transfers between devices, per_device(): other_weight = lax.ppermute(weight, 'tp', [(0, 1), (1, 0)])  1.92 us
  transfers between devices with their start and end apart: 3, of which 1 were waited for; matrix products, arithmetic and copies ran while one was open for 0% of the time, Pallas kernels for 9%

profile of v4, /device:TPU:384, one launch (start us, length us, event | category | flops | bytes accessed | tf_op | source)
XLA Modules:
  0.0 54.3 jit_solution(3747633414528547210)
XLA Ops:
  0.0 2.7 %pack.1 = bf16[8,384,128]{2,1,0:T(8,128)(2,1)S(1)} custom-call(s32[1]{0:T(128)} %bitcast.index_ref, s32[1]{0:T(128)} %bitcast.1.core_ref, bf16[256,512]{1,0:T(8,128)(2,1)} %q_hbm.1, bf16[256,512]{1,0:T(8,128)(2,1)} %k_hbm.1, bf16[256,512]{1,0:T(8,128)(2,1)} %v_hbm.1, bf16[256,256]{1,0:T(8,128)(2,1)} %constant.42.clone.perm_hbm, ...), custom_call_target="tpu_custom_call" | custom-call | tf_op jit(solution)/shard_map/pack/pallas_call | solution.py:325
  2.7 0.0 copy-start
  2.7 0.0 copy-start.1
  2.7 0.0 copy-start.2
  2.8 0.0 copy-start.3
  2.8 18.3 %all_to_all.10.own_ref = bf16[8,384,128]{2,1,0:T(8,128)(2,1)S(1)} all-to-all(bf16[8,384,128]{2,1,0:T(8,128)(2,1)S(1)} %pack.1), channel_id=1, replica_groups=mesh['z'=16,'g'=2,'b'=2,'x'=4,'tp'=2] {'b','x'}, dimensions={0} | all-to-all | bytes 1572864 | tf_op jit(solution)/shard_map/all_to_all | solution.py:358
  21.0 3.9 %collective-permute-start.1 = (bf16[512,128]{1,0:T(8,128)(2,1)S(1)}, bf16[512,128]{1,0:T(8,128)(2,1)S(1)}, u32[]{:S(2)}, u32[]{:S(2)}) collective-permute-start(bf16[512,128]{1,0:T(8,128)(2,1)S(1)} %bitcast.7), channel_id=1, source_target_pairs={{0,24},{2,26},{4,28},{6,30},{8,16},{10,18},{12,20},{14,22},{16,40}... | collective-permute-start | bytes 393224 | tf_op jit(solution)/shard_map/ppermute | solution.py:362
  25.0 3.6 %collective-permute-start = (bf16[1600,128]{1,0:T(8,128)(2,1)S(1)}, bf16[1600,128]{1,0:T(8,128)(2,1)S(1)}, u32[]{:S(2)}, u32[]{:S(2)}) collective-permute-start(bf16[1600,128]{1,0:T(8,128)(2,1)S(1)} %pad_maximum_fusion), channel_id=1, source_target_pairs={{0,24},{2,26},{4,28},{6,30},{8,16},{10,18},{12,20},{14,22},{16,40}... | collective-permute-start | bytes 1228808 | tf_op jit(solution)/shard_map/ppermute | solution.py:361
  28.7 0.0 copy-done
  28.7 1.9 %collective-permute-start.2 = (bf16[512,2048]{1,0:T(8,128)(2,1)S(1)}, bf16[512,2048]{1,0:T(8,128)(2,1)S(1)}, u32[]{:S(2)}, u32[]{:S(2)}) collective-permute-start(bf16[512,2048]{1,0:T(8,128)(2,1)S(1)} %copy-done), channel_id=1, source_target_pairs={{0,1},{1,0},{2,3},{3,2},{4,5},{5,4},{6,7},{7,6},{8,9},{9,8},{10,11... | collective-permute-start | bytes 6291464 | tf_op jit(solution)/shard_map/ppermute | solution.py:364
  30.6 0.0 copy-done.1
  30.6 0.0 copy-done.2
  30.6 0.0 copy-done.3
  30.6 2.7 %attend_own.1 = (f32[8,264,128]{2,1,0:T(8,128)S(1)}, f32[8,264,128]{2,1,0:T(8,128)S(1)}, bf16[8,272,128]{2,1,0:T(8,128)(2,1)S(1)}) custom-call(bf16[8,384,128]{2,1,0:T(8,128)(2,1)S(1)} %all_to_all.10.own_ref, f32[256,512]{1,0:T(8,128)S(1)} %copy-done.1, f32[128,256]{1,0:T(8,128)S(1)} %copy-done.3, f32[128,256]{1,0:T(8,128)S(1)} %copy-done.2), custom_call_target="tpu_custom_call" | custom-call | flops 20000000000 | bytes 2097152 | tf_op jit(solution)/shard_map/attend_own/pallas_call | solution.py:367
  33.4 6.7 %collective-permute-done.halo_ref.before_ref = bf16[1600,128]{1,0:T(8,128)(2,1)S(1)} collective-permute-done((bf16[1600,128]{1,0:T(8,128)(2,1)S(1)}, bf16[1600,128]{1,0:T(8,128)(2,1)S(1)}, u32[]{:S(2)}, u32[]{:S(2)}) %collective-permute-start) | collective-permute-done | bytes 409632 | tf_op jit(solution)/shard_map/ppermute | solution.py:361
  40.1 0.0 copy-start.4
  40.1 1.1 %attend_first.1.lo_ref = bf16[8,192,128]{2,1,0:T(8,128)(2,1)S(1)} custom-call(s32[1]{0:T(128)} %bitcast.index_ref, f32[8,264,128]{2,1,0:T(8,128)S(1)} %get-tuple-element.11.acc_ref, f32[8,264,128]{2,1,0:T(8,128)S(1)} %get-tuple-element.12.top_ref, bf16[8,272,128]{2,1,0:T(8,128)(2,1)S(1)} %get-tuple-element.13.qs_ref, ...), custom_call_target="tpu_custom_call" | custom-call | flops 4000000000 | bytes 2097152 | tf_op jit(solution)/shard_map/attend_first/pallas_call | solution.py:399
  41.2 0.0 collective-permute-done.1.halo_ref
  41.2 0.0 copy-done.4
  41.2 1.1 %attend_last.1 = bf16[16,64,128]{2,1,0:T(8,128)(2,1)S(1)} custom-call(s32[1]{0:T(128)} %bitcast.index_ref, f32[8,264,128]{2,1,0:T(8,128)S(1)} %get-tuple-element.11.acc_ref, f32[8,264,128]{2,1,0:T(8,128)S(1)} %get-tuple-element.12.top_ref, bf16[8,272,128]{2,1,0:T(8,128)(2,1)S(1)} %get-tuple-element.13.qs_ref, bf16[8,192,128]{2,1,0:T(8,128)(2,1)S(1)} %attend_first.1.lo_ref, ...), custom_call_target="tpu_custom_call" | custom-call | flops 4000000000 | bytes 2097152 | tf_op jit(solution)/shard_map/attend_last/pallas_call | solution.py:409
  42.3 0.0 collective-permute-done.2.other_ref
  42.3 10.5 %all_to_all.11.rows_ref = bf16[16,64,128]{2,1,0:T(8,128)(2,1)S(1)} all-to-all(bf16[16,64,128]{2,1,0:T(8,128)(2,1)S(1)} %attend_last.1), channel_id=1, replica_groups=mesh['z'=16,'g'=2,'b'=2,'x'=4,'tp'=2] {'b','x','tp'}, dimensions={0} | all-to-all | bytes 524288 | tf_op jit(solution)/shard_map/all_to_all | solution.py:420
  52.9 1.5 %project.1 = bf16[128,2048]{1,0:T(8,128)(2,1)} custom-call(s32[1]{0:T(128)} %bitcast.index_ref, s32[1]{0:T(128)} %bitcast.1.core_ref, bf16[16,64,128]{2,1,0:T(8,128)(2,1)S(1)} %all_to_all.11.rows_ref, bf16[512,2048]{1,0:T(8,128)(2,1)S(1)} %copy-done, bf16[512,2048]{1,0:T(8,128)(2,1)S(1)} %collective-permute-done.2.other_ref), custom_call_target="tpu_custom_call" | custom-call | tf_op jit(solution)/shard_map/project/pallas_call | solution.py:421
  (4 shorter events, 0.1 us)
Async XLA Ops:
  2.7 25.9 %copy-start = (bf16[512,2048]{1,0:T(8,128)(2,1)S(1)}, bf16[512,2048]{1,0:T(8,128)(2,1)}, u32[]{:S(2)}) copy-start(bf16[512,2048]{1,0:T(8,128)(2,1)} %own_ref.1) | copy-start | bytes 6291460
  2.7 27.9 %copy-start.1 = (f32[256,512]{1,0:T(8,128)S(1)}, f32[256,512]{1,0:T(8,128)}, u32[]{:S(2)}) copy-start(f32[256,512]{1,0:T(8,128)} %constant.46.clone.mask1_ref) | copy-start | bytes 1572868
  2.7 27.9 %copy-start.2 = (f32[128,256]{1,0:T(8,128)S(1)}, f32[128,256]{1,0:T(8,128)}, u32[]{:S(2)}) copy-start(f32[128,256]{1,0:T(8,128)} %constant.48.clone.mask16_ref) | copy-start | bytes 393220
  2.8 27.9 %copy-start.3 = (f32[128,256]{1,0:T(8,128)S(1)}, f32[128,256]{1,0:T(8,128)}, u32[]{:S(2)}) copy-start(f32[128,256]{1,0:T(8,128)} %constant.47.clone.mask4_ref) | copy-start | bytes 393220
  21.0 20.1 %collective-permute-start.1 = (bf16[512,128]{1,0:T(8,128)(2,1)S(1)}, bf16[512,128]{1,0:T(8,128)(2,1)S(1)}, u32[]{:S(2)}, u32[]{:S(2)}) collective-permute-start(bf16[512,128]{1,0:T(8,128)(2,1)S(1)} %bitcast.7), channel_id=1, source_target_pairs={{0,24},{2,26},{4,28},{6,30},{8,16},{10,18},{12,20},{14,22},{16,40}... | collective-permute-start | bytes 393224 | tf_op jit(solution)/shard_map/ppermute | solution.py:362
  25.0 15.0 %collective-permute-start = (bf16[1600,128]{1,0:T(8,128)(2,1)S(1)}, bf16[1600,128]{1,0:T(8,128)(2,1)S(1)}, u32[]{:S(2)}, u32[]{:S(2)}) collective-permute-start(bf16[1600,128]{1,0:T(8,128)(2,1)S(1)} %pad_maximum_fusion), channel_id=1, source_target_pairs={{0,24},{2,26},{4,28},{6,30},{8,16},{10,18},{12,20},{14,22},{16,40}... | collective-permute-start | bytes 1228808 | tf_op jit(solution)/shard_map/ppermute | solution.py:361
  28.7 13.6 %collective-permute-start.2 = (bf16[512,2048]{1,0:T(8,128)(2,1)S(1)}, bf16[512,2048]{1,0:T(8,128)(2,1)S(1)}, u32[]{:S(2)}, u32[]{:S(2)}) collective-permute-start(bf16[512,2048]{1,0:T(8,128)(2,1)S(1)} %copy-done), channel_id=1, source_target_pairs={{0,1},{1,0},{2,3},{3,2},{4,5},{5,4},{6,7},{7,6},{8,9},{9,8},{10,11... | collective-permute-start | bytes 6291464 | tf_op jit(solution)/shard_map/ppermute | solution.py:364
  40.1 1.1 %copy-start.4 = (bf16[256,256]{1,0:T(8,128)(2,1)S(1)}, bf16[256,256]{1,0:T(8,128)(2,1)}, u32[]{:S(2)}) copy-start(bf16[256,256]{1,0:T(8,128)(2,1)} %constant.49.clone.perm_ref) | copy-start | bytes 393220

commit v5 on v3

--- a/solution.py
+++ b/solution.py
@@ -55,9 +55,7 @@
         sin=np.sin(inner).astype(np.float32),
         anchors=anchors.astype(np.float32),
         perm=perm,
-        mask1=mask1,
-        mask4=mask4,
-        mask16=mask16,
+        masks=np.concatenate([mask1, np.concatenate([mask4, mask16], axis=0)], axis=1),
     )
 
 
@@ -74,12 +72,12 @@
 
 
 def pack_kernel(
-    index_ref, core_ref, q_hbm, k_hbm, v_hbm, perm_hbm, cos_hbm, sin_hbm, anchor_hbm, out_hbm, halo_ref,
-    q_ref, k_ref, v_ref, perm_ref, cos_ref, sin_ref, anchor_ref, out_ref, sems, out_sems,
+    index_ref, core_ref, q_hbm, k_hbm, v_hbm, perm_hbm, cos_hbm, sin_hbm, anchor_hbm, kv_ref, packed_ref,
+    q_ref, k_ref, v_ref, perm_ref, cos_ref, sin_ref, anchor_ref, sems,
 ):
     pairs = (
         (anchor_hbm, anchor_ref), (cos_hbm, cos_ref), (sin_hbm, sin_ref), (perm_hbm, perm_ref),
-        (q_hbm, q_ref), (k_hbm, k_ref), (v_hbm, v_ref),
+        (k_hbm, k_ref), (v_hbm, v_ref), (q_hbm, q_ref),
     )
     copies = [pltpu.make_async_copy(source, target, sems.at[n]) for n, (source, target) in enumerate(pairs)]
     for copy in copies:
@@ -87,6 +85,7 @@
     for copy in copies:
         copy.wait()
     block = index_ref[0]
+    flip = 4 * ((block // GROUP) % 2)
     fine = anchor_ref[pl.ds(block % 16, 1), :]
     coarse = anchor_ref[pl.ds(16 + block // 16, 1), :]
     cos_a = fine[:, :128] * coarse[:, :128] - fine[:, 128:] * coarse[:, 128:]
@@ -103,27 +102,18 @@
         return rows * cosine + other * sine
 
     perm = perm_ref[...]
-    outgoing = []
     for j in range(4):
         cols = slice(128 * j, 128 * j + 128)
         query = turn(dot(perm, q_ref[:, cols])) * (1.0 / math.sqrt(HD))
         key = turn(dot(perm, k_ref[:, cols]))
         value = dot(perm, v_ref[:, cols])
-        even, odd = 2 * j, 2 * j + 1
-        packed = jnp.where(low64, key, pltpu.roll(value, 64, 1)).astype(BF)
-        out_ref[even, 0:TOK] = packed
-        halo_ref[even] = packed
-        packed = jnp.where(low64, pltpu.roll(key, 64, 1), value).astype(BF)
-        out_ref[odd, 0:TOK] = packed
-        halo_ref[odd] = packed
+        even = (2 * j) ^ flip
+        odd = even + 1
+        kv_ref[even] = jnp.where(low64, key, pltpu.roll(value, 64, 1)).astype(BF)
+        kv_ref[odd] = jnp.where(low64, pltpu.roll(key, 64, 1), value).astype(BF)
         first, second = query[:128], query[128:]
-        out_ref[even, TOK : TOK + 128] = jnp.where(low64[:128], first, pltpu.roll(second, 64, 1)).astype(BF)
-        out_ref[odd, TOK : TOK + 128] = jnp.where(low64[:128], pltpu.roll(first, 64, 1), second).astype(BF)
-        copy = pltpu.make_async_copy(out_ref.at[pl.ds(2 * j, 2)], out_hbm.at[pl.ds(2 * j, 2)], out_sems.at[j])
-        copy.start()
-        outgoing.append(copy)
-    for copy in outgoing:
-        copy.wait()
+        packed_ref[even] = jnp.where(low64[:128], first, pltpu.roll(second, 64, 1)).astype(BF)
+        packed_ref[odd] = jnp.where(low64[:128], pltpu.roll(first, 64, 1), second).astype(BF)
 
 
 def wide(x, n):
@@ -139,13 +129,6 @@
     return total / pltpu.roll(total, 64, 1)
 
 
-def start_all(pairs, sems):
-    copies = [pltpu.make_async_copy(source, target, sems.at[n]) for n, (source, target) in enumerate(pairs)]
-    for copy in copies:
-        copy.start()
-    return copies
-
-
 def row_max(scores):
     return jnp.max(scores, axis=1, keepdims=True)
 
@@ -154,15 +137,14 @@
     return jnp.exp(scores - wide(peak, scores.shape[1] // 128)).astype(BF)
 
 
-def own_kernel(
-    own_ref, mask1_hbm, mask4_hbm, mask16_hbm, acc_hbm, top_hbm, qs_hbm,
-    acc_ref, top_ref, qs_ref, mask1_ref, mask4_ref, mask16_ref, vs, s16, s4, s1, p16, p4, p1, mask_sems, sems,
-):
-    loads = start_all(((mask16_hbm, mask16_ref), (mask4_hbm, mask4_ref), (mask1_hbm, mask1_ref)), mask_sems)
+def own_kernel(own_ref, packed_ref, mask_ref, acc_ref, top_ref, qs_ref, vs, s16, s4, s1, p16, p4, p1):
+    mask1_ref, mask4_ref, mask16_ref = (
+        mask_ref.at[:, 0:512], mask_ref.at[0:128, 512:768], mask_ref.at[128:256, 512:768]
+    )
     low256, high256 = value_masks(TOK)
     low_bf = low256[:128]
     for i in range(GROUP):
-        packed = own_ref[i, TOK : TOK + 128]
+        packed = packed_ref[i]
         qs_ref[i, 0:128] = packed * low_bf
         qs_ref[i, 128:256] = pltpu.roll(packed.astype(F32), 64, 1).astype(BF) * low_bf
         vs[i, 0:TOK] = own_ref[i, 0:TOK] * high256 + low256
@@ -176,8 +158,6 @@
         seen = slice(max(0, i - 1), i + 1)
         return seen, TOK * (seen.stop - seen.start)
 
-    for load in loads:
-        load.wait()
     for r in range(16):
         rows = slice(16 * r, 16 * r + 16)
         scores = dot_t(qs_ref[:, rows].reshape(128, 128), own_ref[:, rows].reshape(128, 128)) + mask16_ref[:, 128:256]
@@ -194,12 +174,6 @@
         scores = dot_t(qs_ref[i, 0:TOK], own_ref[seen, 0:TOK].reshape(width, 128)) + mask1_ref[:, 512 - width : 512]
         s1[i, :, 0:width] = scores
         top_ref[i, 0:TOK] = jnp.maximum(top_ref[i, 0:TOK], row_max(scores))
-    copies = [
-        pltpu.make_async_copy(source, target, sems.at[n])
-        for n, (source, target) in enumerate(((qs_ref, qs_hbm), (top_ref, top_hbm), (acc_ref, acc_hbm)))
-    ]
-    copies[0].start()
-    copies[1].start()
     for r in range(16):
         p16[r] = weights(s16[r], top_ref[:, 16 * r : 16 * r + 16].reshape(128, 128))
     for n in range(16):
@@ -217,22 +191,14 @@
     for i in range(GROUP):
         seen, width = at1(i)
         acc_ref[i, 0:TOK] += dot(p1[i, :, 0:width], vs[seen, 0:TOK].reshape(width, 128))
-    copies[2].start()
-    for copy in copies:
-        copy.wait()
 
 
 def halo_kernel(
-    index_ref, halo_ref, qs_hbm, top_hbm, mask16_hbm, mask4_hbm, mask1_hbm, acc_hbm, perm_hbm,
-    out_ref, qs_ref, top_ref, mask16_ref, mask4_ref, mask1_ref, acc_ref, perm_ref,
-    vs, peak, s16, s4, s1, p16, p4, p1, sems,
+    index_ref, halo_ref, acc_ref, top_ref, qs_ref, perm_ref, mask_ref,
+    out_ref, vs, peak, s16, s4, s1, p16, p4, p1,
 ):
-    copies = start_all(
-        (
-            (qs_hbm, qs_ref), (top_hbm, top_ref), (mask16_hbm, mask16_ref), (mask4_hbm, mask4_ref),
-            (mask1_hbm, mask1_ref), (acc_hbm, acc_ref), (perm_hbm, perm_ref),
-        ),
-        sems,
+    mask1_ref, mask4_ref, mask16_ref = (
+        mask_ref.at[:, 0:512], mask_ref.at[0:128, 512:768], mask_ref.at[128:256, 512:768]
     )
     bias = jnp.where(index_ref[0] < GROUP, NEG, 0.0).astype(F32)
     low256, high256 = value_masks(TOK)
@@ -240,13 +206,11 @@
         vs[i, 0:TOK] = halo_ref[i] * high256 + low256
 
     def blocks(ref, rows):
-        return jnp.concatenate([ref[4:8, rows], ref[0:4, rows]], axis=0).reshape(128, 128)
+        return ref[:, rows].reshape(128, 128)
 
     def last_two(ref, rows):
-        return ref[2:4, rows].reshape(128, 128)
-
-    for copy in copies[:5]:
-        copy.wait()
+        return ref[6:8, rows].reshape(128, 128)
+
     mask16 = mask16_ref[:, 0:128] + bias
     for r in range(16):
         rows = slice(16 * r, 16 * r + 16)
@@ -259,7 +223,7 @@
         scores = dot_t(qs_ref[0:2, rows].reshape(128, 128), last_two(halo_ref, rows)) + mask4
         s4[r] = scores
         peak[0:2, rows] = jnp.maximum(peak[0:2, rows].reshape(128, 128), row_max(scores)).reshape(2, 64, 128)
-    scores = dot_t(qs_ref[0, 0:TOK], halo_ref[3]) + (mask1_ref[:, 0:TOK] + bias)
+    scores = dot_t(qs_ref[0, 0:TOK], halo_ref[7]) + (mask1_ref[:, 0:TOK] + bias)
     s1[...] = scores
     peak[0, 0:TOK] = jnp.maximum(peak[0, 0:TOK], row_max(scores))
     for r in range(16):
@@ -267,8 +231,6 @@
     for r in range(4):
         p4[r] = weights(s4[r], peak[0:2, 64 * r : 64 * r + 64].reshape(128, 128))
     p1[...] = weights(s1[...], peak[0, 0:TOK])
-    copies[5].wait()
-    copies[6].wait()
     for i in range(GROUP):
         peak[i, 0:TOK] = acc_ref[i, 0:TOK] * jnp.exp(top_ref[i, 0:TOK] - peak[i, 0:TOK])
     new = peak
@@ -278,7 +240,7 @@
     for r in range(4):
         rows = slice(64 * r, 64 * r + 64)
         new[0:2, rows] += dot(p4[r], last_two(vs, rows)).reshape(2, 64, 128)
-    new[0, 0:TOK] += dot(p1[...], vs[3, 0:TOK])
+    new[0, 0:TOK] += dot(p1[...], vs[7, 0:TOK])
     low_rows = half(64)
     for i in range(GROUP):
         mixed = normal(new[i, 0:TOK]).astype(BF) * high256
@@ -287,19 +249,26 @@
         out_ref[2 * i + 1] = jnp.where(low_rows, pltpu.roll(natural[128:192], 64, 1), natural[192:256]).astype(BF)
 
 
-def project_kernel(core_ref, rows_ref, own_ref, other_ref, out_ref, mixed):
+def project_kernel(index_ref, core_ref, rows_ref, own_ref, other_ref, out_hbm, mixed, out_ref, sems):
     low = half(64)
+    flip = 4 * ((index_ref[0] // GROUP) % 2)
     for side in range(2):
         core = core_ref[0] if side == 0 else 1 - core_ref[0]
         for j in range(4):
-            first = rows_ref[4 * j + core].astype(F32)
-            second = rows_ref[4 * j + 2 + core].astype(F32)
+            first = rows_ref[2 * ((2 * j) ^ flip) + core].astype(F32)
+            second = rows_ref[2 * ((2 * j) ^ flip) + 2 + core].astype(F32)
             cols = slice(128 * j, 128 * j + 128)
             mixed[side, 0:64, cols] = jnp.where(low, first, pltpu.roll(second, 64, 1)).astype(BF)
             mixed[side, 64:128, cols] = jnp.where(low, pltpu.roll(first, 64, 1), second).astype(BF)
+    copies = []
     for n in range(4):
         cols = slice(512 * n, 512 * n + 512)
         out_ref[:, cols] = (dot(mixed[0], own_ref[:, cols]) + dot(mixed[1], other_ref[:, cols])).astype(BF)
+        copy = pltpu.make_async_copy(out_ref.at[:, cols], out_hbm.at[:, cols], sems.at[n])
+        copy.start()
+        copies.append(copy)
+    for copy in copies:
+        copy.wait()
 
 
 def vmem():
@@ -317,13 +286,13 @@
 
     smem = pl.BlockSpec(memory_space=pltpu.SMEM)
     hbm = pl.BlockSpec(memory_space=pltpu.HBM)
-    send, keys_values = pl.pallas_call(
+    send_kv, send_q = pl.pallas_call(
         pack_kernel,
         in_specs=[smem] * 2 + [hbm] * 7,
-        out_specs=[hbm, vmem()],
+        out_specs=[vmem()] * 2,
         out_shape=[
-            pltpu.HBM((GROUP, TOK + 128, 128), BF),
             jax.ShapeDtypeStruct((GROUP, TOK, 128), BF),
+            jax.ShapeDtypeStruct((GROUP, 128, 128), BF),
         ],
         scratch_shapes=[
             pltpu.VMEM((TOK, 512), BF),
@@ -333,9 +302,7 @@
             pltpu.VMEM((TOK, 128), F32),
             pltpu.VMEM((TOK, 128), F32),
             pltpu.VMEM((16 + blocks // 16, 256), F32),
-            pltpu.VMEM((GROUP, TOK + 128, 128), BF),
             pltpu.SemaphoreType.DMA((7,)),
-            pltpu.SemaphoreType.DMA((4,)),
         ],
         compiler_params=limit(12),
         name="pack",
@@ -356,30 +323,20 @@
         ),
     )
     following = [(s, (s // GROUP + 1) * GROUP + ((s % GROUP) ^ 4)) for s in range(blocks - GROUP)]
-    shifted = lax.ppermute(keys_values, SP, following)
-    own = lax.all_to_all(send, ("b", "x"), 0, 0, tiled=True)
-    shifted, _ = lax.optimization_barrier((shifted, own))
-    halo = lax.all_to_all(shifted, ("b", "x"), 0, 0, tiled=True)
-    weight, _ = lax.optimization_barrier((out_weight, keys_values))
+    own = lax.all_to_all(send_kv, ("b", "x"), 0, 0, tiled=True)
+    halo = lax.ppermute(own, SP, following)
+    send_q, _ = lax.optimization_barrier((send_q, own))
+    packed = lax.all_to_all(send_q, ("b", "x"), 0, 0, tiled=True)
+    weight, _ = lax.optimization_barrier((out_weight, packed))
     other_weight = lax.ppermute(weight, "tp", [(0, 1), (1, 0)])
-    mask1, mask4, mask16 = (jnp.asarray(tables[name]) for name in ("mask1", "mask4", "mask16"))
-    mask1, mask4, mask16 = (pltpu.with_memory_space_constraint(x, pltpu.HBM) for x in (mask1, mask4, mask16))
+    masks = jnp.asarray(tables["masks"])
+    state = jax.ShapeDtypeStruct((GROUP, TOK + 8, 128), F32)
     acc, top, qs = pl.pallas_call(
         own_kernel,
-        in_specs=[vmem()] + [hbm] * 3,
-        out_specs=[hbm] * 3,
-        out_shape=[
-            pltpu.HBM((GROUP, TOK + 8, 128), F32),
-            pltpu.HBM((GROUP, TOK + 8, 128), F32),
-            pltpu.HBM((GROUP, TOK + 16, 128), BF),
-        ],
+        in_specs=[vmem()] * 3,
+        out_specs=[vmem()] * 3,
+        out_shape=[state, state, jax.ShapeDtypeStruct((GROUP, TOK + 16, 128), BF)],
         scratch_shapes=[
-            pltpu.VMEM((GROUP, TOK + 8, 128), F32),
-            pltpu.VMEM((GROUP, TOK + 8, 128), F32),
-            pltpu.VMEM((GROUP, TOK + 16, 128), BF),
-            pltpu.VMEM((TOK, 2 * TOK), F32),
-            pltpu.VMEM((128, 256), F32),
-            pltpu.VMEM((128, 256), F32),
             pltpu.VMEM((GROUP, TOK + 16, 128), BF),
             pltpu.VMEM((16, 128, 128), F32),
             pltpu.VMEM((16, 128, 256), F32),
@@ -387,26 +344,17 @@
             pltpu.VMEM((16, 128, 128), BF),
             pltpu.VMEM((16, 128, 256), BF),
             pltpu.VMEM((GROUP, TOK, 512), BF),
-            pltpu.SemaphoreType.DMA((3,)),
-            pltpu.SemaphoreType.DMA((3,)),
         ],
         compiler_params=limit(24),
         cost_estimate=pl.CostEstimate(flops=20 * 10**9, bytes_accessed=2 * 2**20, transcendentals=0),
         name="attend_own",
-    )(own, mask1, mask4, mask16)
+    )(own, packed, masks)
     back = pl.pallas_call(
         halo_kernel,
-        in_specs=[smem, vmem()] + [hbm] * 7,
+        in_specs=[smem] + [vmem()] * 6,
         out_specs=vmem(),
         out_shape=jax.ShapeDtypeStruct((2 * GROUP, 64, 128), BF),
         scratch_shapes=[
-            pltpu.VMEM((GROUP, TOK + 16, 128), BF),
-            pltpu.VMEM((GROUP, TOK + 8, 128), F32),
-            pltpu.VMEM((128, 256), F32),
-            pltpu.VMEM((128, 256), F32),
-            pltpu.VMEM((TOK, 2 * TOK), F32),
-            pltpu.VMEM((GROUP, TOK + 8, 128), F32),
-            pltpu.VMEM((TOK, TOK), BF),
             pltpu.VMEM((GROUP, TOK + 16, 128), BF),
             pltpu.VMEM((GROUP, TOK + 8, 128), F32),
             pltpu.VMEM((16, 128, 128), F32),
@@ -415,30 +363,26 @@
             pltpu.VMEM((16, 128, 128), BF),
             pltpu.VMEM((4, 128, 128), BF),
             pltpu.VMEM((TOK, TOK), BF),
-            pltpu.SemaphoreType.DMA((7,)),
         ],
         compiler_params=limit(16),
         cost_estimate=pl.CostEstimate(flops=4 * 10**9, bytes_accessed=2 * 2**20, transcendentals=0),
         name="attend_halo",
-    )(
-        index,
-        halo,
-        *(
-            pltpu.with_memory_space_constraint(x, pltpu.HBM)
-            for x in (qs, top, mask16, mask4, mask1, acc, jnp.asarray(tables["perm"].T, BF))
-        ),
-    )
+    )(index, halo, acc, top, qs, jnp.asarray(tables["perm"].T, BF), masks)
     back, other_weight = lax.optimization_barrier((back, other_weight))
     rows = lax.all_to_all(back, ("b", "x", "tp"), 0, 0, tiled=True)
     return pl.pallas_call(
         project_kernel,
-        in_specs=[smem] + [vmem()] * 3,
-        out_specs=vmem(),
-        out_shape=jax.ShapeDtypeStruct((TOK // 2, 2048), BF),
-        scratch_shapes=[pltpu.VMEM((2, TOK // 2, 512), BF)],
+        in_specs=[smem] * 2 + [vmem()] * 3,
+        out_specs=hbm,
+        out_shape=pltpu.HBM((TOK // 2, 2048), BF),
+        scratch_shapes=[
+            pltpu.VMEM((2, TOK // 2, 512), BF),
+            pltpu.VMEM((TOK // 2, 2048), BF),
+            pltpu.SemaphoreType.DMA((4,)),
+        ],
         compiler_params=limit(16),
         name="project",
-    )(core, rows, out_weight, other_weight)
+    )(index, core, rows, out_weight, other_weight)
 
 
 def solution(mesh):

time: 58.1 us -> 55.8 us (0.960)
  the two profiles are of different devices: /device:TPU:384 before, /device:TPU:256 now
where the time goes in v5:
time: 55.8 us; the launch traced here: 55.4 us
  blocking collectives  27.4 us (49%)
  starting transfers between devices  10.7 us (19%)
  Pallas kernels  9.46 us (17%)
  waiting for transfers between devices  6.65 us (12%)
  local copies, waits for them, and re-layouts  1.14 us (2%)
    all_to_all x1, blocking collectives, per_device(): own = lax.all_to_all(send_kv, ('b', 'x'), 0, 0, tiled=True)  15.2 us
    all_to_all x1, blocking collectives, per_device(): rows = lax.all_to_all(back, ('b', 'x', 'tp'), 0, 0, tiled=True)  12.2 us
    ppermute x1, starting transfers between devices, per_device(): halo = lax.ppermute(own, SP, following)  5.28 us
    ppermute x1, waiting for transfers between devices, per_device(): halo = lax.ppermute(own, SP, following)  4.71 us
    all_to_all x1, starting transfers between devices, per_device(): packed = lax.all_to_all(send_q, ('b', 'x'), 0, 0, tiled=True)  3.54 us
    pallas_call x1, Pallas kernels, per_device(): pl.pallas_call(pack_kernel, in_specs=[smem] * 2 + [hbm] * 7, out_specs=[v...  3.32 us
    pallas_call x1, Pallas kernels, per_device(): pl.pallas_call(own_kernel, in_specs=[vmem()] * 3, out_specs=[vmem()] * 3,...  2.75 us
    all_to_all x1, waiting for transfers between devices, per_device(): packed = lax.all_to_all(send_q, ('b', 'x'), 0, 0, tiled=True)  1.94 us
  transfers between devices with their start and end apart: 3, of which 2 were waited for; matrix products, arithmetic and copies ran while one was open for 0% of the time, Pallas kernels for 8%

profile of v5, /device:TPU:256, one launch (start us, length us, event | category | flops | bytes accessed | tf_op | source)
XLA Modules:
  0.0 55.4 jit_solution(15384702918410999658)
XLA Ops:
  0.0 0.0 copy-start
  0.0 3.3 %pack.1 = (bf16[8,256,128]{2,1,0:T(8,128)(2,1)S(1)}, bf16[8,128,128]{2,1,0:T(8,128)(2,1)}) custom-call(s32[1]{0:T(128)} %bitcast.index_ref, s32[1]{0:T(128)} %bitcast.1.core_ref, bf16[256,512]{1,0:T(8,128)(2,1)} %q_hbm.1, bf16[256,512]{1,0:T(8,128)(2,1)} %k_hbm.1, bf16[256,512]{1,0:T(8,128)(2,1)} %v_hbm.1, bf16[256,256]{1,0:T(8,128)(2,1)} %constant.38.clone.perm_hbm, ...), custom_call_target="tpu_custom_call" | custom-call | tf_op jit(solution)/shard_map/pack/pallas_call | solution.py:289
  3.3 15.2 %all_to_all.15.own_ref = bf16[8,256,128]{2,1,0:T(8,128)(2,1)S(1)} all-to-all(bf16[8,256,128]{2,1,0:T(8,128)(2,1)S(1)} %get-tuple-element.14), channel_id=1, replica_groups=mesh['z'=16,'g'=2,'b'=2,'x'=4,'tp'=2] {'b','x'}, dimensions={0} | all-to-all | bytes 1048576 | tf_op jit(solution)/shard_map/all_to_all | solution.py:326
  18.5 0.0 copy-start.2
  18.5 3.5 %all-to-all-start.1 = ((bf16[8,128,128]{2,1,0:T(8,128)(2,1)}), bf16[8,128,128]{2,1,0:T(8,128)(2,1)S(1)}, u32[]{:S(2)}, u32[]{:S(2)}) async-start(bf16[8,128,128]{2,1,0:T(8,128)(2,1)} %get-tuple-element.16), calls=%async_computation.1 | async-start | bytes 524288 | tf_op jit(solution)/shard_map/all_to_all | solution.py:329
  22.1 5.3 %collective-permute-start = (bf16[8,256,128]{2,1,0:T(8,128)(2,1)S(1)}, bf16[8,256,128]{2,1,0:T(8,128)(2,1)S(1)}, u32[]{:S(2)}, u32[]{:S(2)}) collective-permute-start(bf16[8,256,128]{2,1,0:T(8,128)(2,1)S(1)} %all_to_all.15.own_ref), channel_id=1, source_target_pairs={{0,24},{2,26},{4,28},{6,30},{8,16},{10,18},{12,20},{14,22},{16,40}... | collective-permute-start | bytes 1572872 | tf_op jit(solution)/shard_map/ppermute | solution.py:327
  27.4 1.9 %all-to-all-done.1.packed_ref = bf16[8,128,128]{2,1,0:T(8,128)(2,1)S(1)} async-done(((bf16[8,128,128]{2,1,0:T(8,128)(2,1)}), bf16[8,128,128]{2,1,0:T(8,128)(2,1)S(1)}, u32[]{:S(2)}, u32[]{:S(2)}) %all-to-all-start.1) | async-done | bytes 262176 | tf_op jit(solution)/shard_map/all_to_all | solution.py:329
  29.3 0.0 copy-done
  29.3 1.9 %collective-permute-start.1 = (bf16[512,2048]{1,0:T(8,128)(2,1)S(1)}, bf16[512,2048]{1,0:T(8,128)(2,1)S(1)}, u32[]{:S(2)}, u32[]{:S(2)}) collective-permute-start(bf16[512,2048]{1,0:T(8,128)(2,1)S(1)} %copy-done), channel_id=1, source_target_pairs={{0,1},{1,0},{2,3},{3,2},{4,5},{5,4},{6,7},{7,6},{8,9},{9,8},{10,11... | collective-permute-start | bytes 6291464 | tf_op jit(solution)/shard_map/ppermute | solution.py:331
  31.2 0.0 copy-start.1
  31.2 1.1 %copy-done.1 = f32[256,768]{1,0:T(8,128)S(1)} copy-done((f32[256,768]{1,0:T(8,128)S(1)}, f32[256,768]{1,0:T(8,128)}, u32[]{:S(2)}) %copy-start.1) | copy-done | bytes 786456
  32.4 2.7 %attend_own.1 = (f32[8,264,128]{2,1,0:T(8,128)S(1)}, f32[8,264,128]{2,1,0:T(8,128)S(1)}, bf16[8,272,128]{2,1,0:T(8,128)(2,1)S(1)}) custom-call(bf16[8,256,128]{2,1,0:T(8,128)(2,1)S(1)} %all_to_all.15.own_ref, bf16[8,128,128]{2,1,0:T(8,128)(2,1)S(1)} %all-to-all-done.1.packed_ref, f32[256,768]{1,0:T(8,128)S(1)} %copy-done.1), custom_call_target="tpu_custom_call" | custom-call | flops 20000000000 | bytes 2097152 | tf_op jit(solution)/shard_map/attend_own/pallas_call | solution.py:334
  35.1 4.7 %collective-permute-done.halo_ref = bf16[8,256,128]{2,1,0:T(8,128)(2,1)S(1)} collective-permute-done((bf16[8,256,128]{2,1,0:T(8,128)(2,1)S(1)}, bf16[8,256,128]{2,1,0:T(8,128)(2,1)S(1)}, u32[]{:S(2)}, u32[]{:S(2)}) %collective-permute-start) | collective-permute-done | bytes 524320 | tf_op jit(solution)/shard_map/ppermute | solution.py:327
  39.8 0.0 copy-done.2
  39.8 1.9 %attend_halo.1 = bf16[16,64,128]{2,1,0:T(8,128)(2,1)S(1)} custom-call(s32[1]{0:T(128)} %bitcast.index_ref, bf16[8,256,128]{2,1,0:T(8,128)(2,1)S(1)} %collective-permute-done.halo_ref, f32[8,264,128]{2,1,0:T(8,128)S(1)} %get-tuple-element.17.acc_ref, f32[8,264,128]{2,1,0:T(8,128)S(1)} %get-tuple-element.18.top_ref, ...), custom_call_target="tpu_custom_call" | custom-call | flops 4000000000 | bytes 2097152 | tf_op jit(solution)/shard_map/attend_halo/pallas_call | solution.py:352
  41.7 0.0 collective-permute-done.1.other_ref
  41.7 12.2 %all_to_all.16.rows_ref = bf16[16,64,128]{2,1,0:T(8,128)(2,1)S(1)} all-to-all(bf16[16,64,128]{2,1,0:T(8,128)(2,1)S(1)} %attend_halo.1), channel_id=1, replica_groups=mesh['z'=16,'g'=2,'b'=2,'x'=4,'tp'=2] {'b','x','tp'}, dimensions={0} | all-to-all | bytes 524288 | tf_op jit(solution)/shard_map/all_to_all | solution.py:372
  53.9 1.5 %project.1 = bf16[128,2048]{1,0:T(8,128)(2,1)} custom-call(s32[1]{0:T(128)} %bitcast.index_ref, s32[1]{0:T(128)} %bitcast.1.core_ref, bf16[16,64,128]{2,1,0:T(8,128)(2,1)S(1)} %all_to_all.16.rows_ref, bf16[512,2048]{1,0:T(8,128)(2,1)S(1)} %copy-done, bf16[512,2048]{1,0:T(8,128)(2,1)S(1)} %collective-permute-done.1.other_ref), custom_call_target="tpu_custom_call" | custom-call | tf_op jit(solution)/shard_map/project/pallas_call | solution.py:373
Async XLA Ops:
  0.0 29.3 %copy-start = (bf16[512,2048]{1,0:T(8,128)(2,1)S(1)}, bf16[512,2048]{1,0:T(8,128)(2,1)}, u32[]{:S(2)}) copy-start(bf16[512,2048]{1,0:T(8,128)(2,1)} %own_ref.1) | copy-start | bytes 6291460
  18.5 21.3 %copy-start.2 = (bf16[256,256]{1,0:T(8,128)(2,1)S(1)}, bf16[256,256]{1,0:T(8,128)(2,1)}, u32[]{:S(2)}) copy-start(bf16[256,256]{1,0:T(8,128)(2,1)} %constant.43.clone.perm_ref) | copy-start | bytes 393220
  18.5 10.8 %all-to-all-start.1 = ((bf16[8,128,128]{2,1,0:T(8,128)(2,1)}), bf16[8,128,128]{2,1,0:T(8,128)(2,1)S(1)}, u32[]{:S(2)}, u32[]{:S(2)}) async-start(bf16[8,128,128]{2,1,0:T(8,128)(2,1)} %get-tuple-element.16), calls=%async_computation.1 | async-start | bytes 524288 | tf_op jit(solution)/shard_map/all_to_all | solution.py:329
  22.1 17.7 %collective-permute-start = (bf16[8,256,128]{2,1,0:T(8,128)(2,1)S(1)}, bf16[8,256,128]{2,1,0:T(8,128)(2,1)S(1)}, u32[]{:S(2)}, u32[]{:S(2)}) collective-permute-start(bf16[8,256,128]{2,1,0:T(8,128)(2,1)S(1)} %all_to_all.15.own_ref), channel_id=1, source_target_pairs={{0,24},{2,26},{4,28},{6,30},{8,16},{10,18},{12,20},{14,22},{16,40}... | collective-permute-start | bytes 1572872 | tf_op jit(solution)/shard_map/ppermute | solution.py:327
  29.3 12.4 %collective-permute-start.1 = (bf16[512,2048]{1,0:T(8,128)(2,1)S(1)}, bf16[512,2048]{1,0:T(8,128)(2,1)S(1)}, u32[]{:S(2)}, u32[]{:S(2)}) collective-permute-start(bf16[512,2048]{1,0:T(8,128)(2,1)S(1)} %copy-done), channel_id=1, source_target_pairs={{0,1},{1,0},{2,3},{3,2},{4,5},{5,4},{6,7},{7,6},{8,9},{9,8},{10,11... | collective-permute-start | bytes 6291464 | tf_op jit(solution)/shard_map/ppermute | solution.py:331
  31.2 1.1 %copy-start.1 = (f32[256,768]{1,0:T(8,128)S(1)}, f32[256,768]{1,0:T(8,128)}, u32[]{:S(2)}) copy-start(f32[256,768]{1,0:T(8,128)} %constant.42.clone.mask_ref) | copy-start | bytes 2359300

commit v6 on v5

v6 whole, which is shorter than its diff:
```python
import functools
import math

import jax
import jax.numpy as jnp
import numpy as np
from jax import lax
from jax.experimental import pallas as pl
from jax.experimental.pallas import tpu as pltpu
from jax.sharding import Mesh, PartitionSpec as P


HD = 64
BACK = 128
THETA = 500000.0
TOK = 256
HALF = 128
GROUP = 8
SP = ("z", "g", "b", "x")
NEG = -1e30
BF = jnp.bfloat16
F32 = jnp.float32


def make_tables(blocks):
    p = np.arange(HALF)
    t = 16 * (p % 8) + p // 32 + 4 * ((p % 32) // 8)
    perm = np.zeros((HALF, HALF), np.float32)
    perm[p, t] = 1.0
    inverse = np.float64(THETA) ** (-np.arange(32, dtype=np.float64) / 32)
    lanes = inverse[np.arange(128) % 32]
    inner = t[:, None] * lanes[None, :]
    anchor = np.concatenate([np.arange(32) * HALF, np.arange(blocks // 16) * (16 * TOK)])[:, None] * lanes[None, :]
    return dict(
        cos=np.cos(inner).astype(np.float32),
        sin=np.sin(inner).astype(np.float32),
        anchors=np.concatenate([np.cos(anchor), np.sin(anchor)], axis=1).astype(np.float32),
        perm=perm,
    )


def dot(a, b):
    return lax.dot_general(a, b, (((1,), (0,)), ((), ())), preferred_element_type=F32)


def dot_t(a, b):
    return lax.dot_general(a, b, (((1,), (1,)), ((), ())), preferred_element_type=F32)


def half(rows):
    return lax.broadcasted_iota(jnp.int32, (rows, 128), 1) < 64


def pack_kernel(
    index_ref, core_ref, q_hbm, k_hbm, v_hbm, perm_hbm, cos_hbm, sin_hbm, anchor_hbm, kv_ref, packed_ref,
    q_ref, k_ref, v_ref, perm_ref, cos_ref, sin_ref, anchor_ref, kf, vf, qf, sems,
):
    pairs = (
        (anchor_hbm, anchor_ref), (cos_hbm, cos_ref), (sin_hbm, sin_ref), (perm_hbm, perm_ref),
        (k_hbm, k_ref), (v_hbm, v_ref), (q_hbm, q_ref),
    )
    copies = [pltpu.make_async_copy(source, target, sems.at[n]) for n, (source, target) in enumerate(pairs)]
    for copy in copies:
        copy.start()
    for copy in copies:
        copy.wait()
    block = index_ref[0]
    flip = 4 * ((block // GROUP) % 2)
    coarse = anchor_ref[pl.ds(32 + block // 16, 1), :]
    lane = lax.broadcasted_iota(jnp.int32, (HALF, 128), 1)
    low64 = lane < 64
    low32 = (lane & 63) < 32
    sign = jnp.where(low32[:1], -1.0, 1.0).astype(F32)

    def turn(rows, cosine, sine):
        other = jnp.where(low32, pltpu.roll(rows, 96, 1), pltpu.roll(rows, 32, 1))
        return rows * cosine + other * sine

    perm = perm_ref[...]
    for side in range(2):
        rows = slice(HALF * side, HALF * side + HALF)
        for source, target in ((k_ref, kf), (v_ref, vf), (q_ref, qf)):
            target[rows] = dot(perm, source[rows])
    for side in range(2):
        rows = slice(HALF * side, HALF * side + HALF)
        fine = anchor_ref[pl.ds(2 * (block % 16) + side, 1), :]
        cos_a = fine[:, :128] * coarse[:, :128] - fine[:, 128:] * coarse[:, 128:]
        sin_a = fine[:, 128:] * coarse[:, :128] + fine[:, :128] * coarse[:, 128:]
        cosine = cos_a * cos_ref[...] - sin_a * sin_ref[...]
        sine = (sin_a * sign) * cos_ref[...] + (cos_a * sign) * sin_ref[...]
        for j in range(4):
            cols = slice(128 * j, 128 * j + 128)
            key = turn(kf[rows, cols], cosine, sine)
            value = vf[rows, cols]
            even = (2 * j) ^ flip
            odd = even + 1
            kv_ref[even, rows] = jnp.where(low64, key, pltpu.roll(value, 64, 1)).astype(BF)
            kv_ref[odd, rows] = jnp.where(low64, pltpu.roll(key, 64, 1), value).astype(BF)
            qf[rows, cols] = turn(qf[rows, cols], cosine, sine) * (1.0 / math.sqrt(HD))
    for j in range(4):
        cols = slice(128 * j, 128 * j + 128)
        even = (2 * j) ^ flip
        odd = even + 1
        first, second = qf[0:HALF, cols], qf[HALF:TOK, cols]
        packed_ref[even] = jnp.where(low64, first, pltpu.roll(second, 64, 1)).astype(BF)
        packed_ref[odd] = jnp.where(low64, pltpu.roll(first, 64, 1), second).astype(BF)


def wide(x, n):
    return jnp.concatenate([x] * n, axis=1) if n > 1 else x


def value_masks(rows):
    low = half(rows)
    return jnp.where(low, 1.0, 0.0).astype(BF), jnp.where(low, 0.0, 1.0).astype(BF)


def normal(total):
    return total / pltpu.roll(total, 64, 1)


def row_max(scores):
    return jnp.max(scores, axis=1, keepdims=True)


def weights(scores, peak):
    return jnp.exp(scores - wide(peak, scores.shape[1] // 128)).astype(BF)


def band(query, key):
    distance = query - key
    return jnp.where((distance >= 0) & (distance <= BACK), 0.0, NEG).astype(F32)


def positions(rows, axis):
    shape = (rows, 128) if axis == 0 else (1, rows)
    p = lax.broadcasted_iota(jnp.int32, shape, axis)
    one = 16 * (p & 7) + (p >> 5) + 4 * ((p >> 3) & 3)
    four = 32 * (p >> 5) + 4 * (p & 7) + ((p >> 3) & 3)
    return one, four, p


def make_masks(before_ref, same_ref, bias):
    for n, (query, key) in enumerate(zip(positions(128, 0), positions(128, 1), strict=True)):
        before_ref[n] = band(query, key - 128) + bias
        if same_ref is not None:
            same_ref[n] = band(query, key)


def pieces16(ref, r):
    return ref[:, 8 * r : 8 * r + 8].reshape(128, 128)


def pieces4(ref, b, r):
    return ref[4 * b : 4 * b + 4, 32 * r : 32 * r + 32].reshape(128, 128)


def own_kernel(own_ref, packed_ref, acc_ref, top_ref, qs_ref, before, same, ks, vs, s16, s4, s1, p16, p4, p1):
    low, high = value_masks(128)
    for i in range(GROUP):
        packed = packed_ref[i]
        qs_ref[2 * i] = packed * low
        qs_ref[2 * i + 1] = pltpu.roll(packed.astype(F32), 64, 1).astype(BF) * low
        for side in range(2):
            key = own_ref[i, HALF * side : HALF * side + HALF]
            ks[2 * i + side] = key
            vs[2 * i + side] = key * high + low
    make_masks(before, same, 0.0)
    pair = lambda n: jnp.concatenate([before[n], same[n]], axis=1)

    def keys4(ref, b, r):
        return pieces4(ref, b, r) if b == 0 else jnp.concatenate([pieces4(ref, b - 1, r), pieces4(ref, b, r)], axis=0)

    def keys1(ref, i):
        return ref[0] if i == 0 else ref[i - 1 : i + 1].reshape(256, 128)

    for r in range(16):
        scores = dot_t(pieces16(qs_ref, r), pieces16(ks, r)) + same[2]
        s16[r] = scores
        top_ref[:, 8 * r : 8 * r + 8] = jnp.broadcast_to(row_max(scores), (128, 128)).reshape(16, 8, 128)
    for n in range(16):
        b, r = n // 4, n % 4
        scores = dot_t(pieces4(qs_ref, b, r), keys4(ks, b, r)) + (same[1] if b == 0 else pair(1))
        s4[n, :, 0 : scores.shape[1]] = scores
        peak = jnp.maximum(pieces4(top_ref, b, r), row_max(scores))
        top_ref[4 * b : 4 * b + 4, 32 * r : 32 * r + 32] = peak.reshape(4, 32, 128)
    for i in range(16):
        scores = dot_t(qs_ref[i], keys1(ks, i)) + (same[0] if i == 0 else pair(0))
        s1[i, :, 0 : scores.shape[1]] = scores
        top_ref[i] = jnp.maximum(top_ref[i], row_max(scores))
    for r in range(16):
        p16[r] = weights(s16[r], pieces16(top_ref, r))
    for n in range(16):
        width = 128 if n < 4 else 256
        p4[n, :, 0:width] = weights(s4[n, :, 0:width], pieces4(top_ref, n // 4, n % 4))
    for i in range(16):
        width = 128 if i == 0 else 256
        p1[i, :, 0:width] = weights(s1[i, :, 0:width], top_ref[i])
    for r in range(16):
        acc_ref[:, 8 * r : 8 * r + 8] = dot(p16[r], pieces16(vs, r)).reshape(16, 8, 128)
    for n in range(16):
        b, r = n // 4, n % 4
        width = 128 if n < 4 else 256
        acc_ref[4 * b : 4 * b + 4, 32 * r : 32 * r + 32] += dot(p4[n, :, 0:width], keys4(vs, b, r)).reshape(4, 32, 128)
    for i in range(16):
        width = 128 if i == 0 else 256
        acc_ref[i] += dot(p1[i, :, 0:width], keys1(vs, i))


def halo_kernel(
    index_ref, halo_ref, acc_ref, top_ref, qs_ref, perm_ref, out_ref, before, ks, vs, peak, s16, s4, s1, p16, p4, p1
):
    low, high = value_masks(128)
    for i in range(GROUP):
        for side in range(2):
            key = halo_ref[i, HALF * side : HALF * side + HALF]
            ks[2 * i + side] = key
            vs[2 * i + side] = key * high + low
    make_masks(before, None, jnp.where(index_ref[0] < GROUP, NEG, 0.0).astype(F32))
    for r in range(16):
        scores = dot_t(pieces16(qs_ref, r), pieces16(ks, r)) + before[2]
        s16[r] = scores
        peak[:, 8 * r : 8 * r + 8] = jnp.maximum(pieces16(top_ref, r), row_max(scores)).reshape(16, 8, 128)
    for r in range(4):
        scores = dot_t(pieces4(qs_ref, 0, r), pieces4(ks, 3, r)) + before[1]
        s4[r] = scores
        best = jnp.maximum(pieces4(peak, 0, r), row_max(scores))
        peak[0:4, 32 * r : 32 * r + 32] = best.reshape(4, 32, 128)
    scores = dot_t(qs_ref[0], ks[15]) + before[0]
    s1[...] = scores
    peak[0] = jnp.maximum(peak[0], row_max(scores))
    for r in range(16):
        p16[r] = weights(s16[r], pieces16(peak, r))
    for r in range(4):
        p4[r] = weights(s4[r], pieces4(peak, 0, r))
    p1[...] = weights(s1[...], peak[0])
    new = peak
    for i in range(16):
        new[i] = acc_ref[i] * jnp.exp(top_ref[i] - peak[i])
    for r in range(16):
        new[:, 8 * r : 8 * r + 8] += dot(p16[r], pieces16(vs, r)).reshape(16, 8, 128)
    for r in range(4):
        new[0:4, 32 * r : 32 * r + 32] += dot(p4[r], pieces4(vs, 3, r)).reshape(4, 32, 128)
    new[0] += dot(p1[...], vs[15])
    low_rows = half(64)
    for i in range(16):
        natural = dot(perm_ref[...], normal(new[i]).astype(BF) * high)
        out_ref[i] = jnp.where(low_rows, pltpu.roll(natural[0:64], 64, 1), natural[64:128]).astype(BF)


def project_kernel(index_ref, core_ref, rows_ref, own_ref, other_ref, out_hbm, mixed, out_ref, sems):
    low = half(64)
    flip = 4 * ((index_ref[0] // GROUP) % 2)
    for side in range(2):
        core = core_ref[0] if side == 0 else 1 - core_ref[0]
        for j in range(4):
            first = rows_ref[2 * ((2 * j) ^ flip) + core].astype(F32)
            second = rows_ref[2 * ((2 * j) ^ flip) + 2 + core].astype(F32)
            cols = slice(128 * j, 128 * j + 128)
            mixed[side, 0:64, cols] = jnp.where(low, first, pltpu.roll(second, 64, 1)).astype(BF)
            mixed[side, 64:128, cols] = jnp.where(low, pltpu.roll(first, 64, 1), second).astype(BF)
    copies = []
    for n in range(4):
        cols = slice(512 * n, 512 * n + 512)
        out_ref[:, cols] = (dot(mixed[0], own_ref[:, cols]) + dot(mixed[1], other_ref[:, cols])).astype(BF)
        copy = pltpu.make_async_copy(out_ref.at[:, cols], out_hbm.at[:, cols], sems.at[n])
        copy.start()
        copies.append(copy)
    for copy in copies:
        copy.wait()


def vmem():
    return pl.BlockSpec(memory_space=pltpu.VMEM)


def limit(mib):
    return pltpu.CompilerParams(vmem_limit_bytes=mib * 2**20)


def per_device(query_rows, key_rows, value_rows, out_weight, blocks):
    tables = make_tables(blocks)
    index = lax.axis_index(SP).astype(jnp.int32).reshape(1)
    core = lax.axis_index("tp").astype(jnp.int32).reshape(1)

    smem = pl.BlockSpec(memory_space=pltpu.SMEM)
    hbm = pl.BlockSpec(memory_space=pltpu.HBM)
    send_kv, send_q = pl.pallas_call(
        pack_kernel,
        in_specs=[smem] * 2 + [hbm] * 7,
        out_specs=[vmem()] * 2,
        out_shape=[
            jax.ShapeDtypeStruct((GROUP, TOK, 128), BF),
            jax.ShapeDtypeStruct((GROUP, 128, 128), BF),
        ],
        scratch_shapes=[
            pltpu.VMEM((TOK, 512), BF),
            pltpu.VMEM((TOK, 512), BF),
            pltpu.VMEM((TOK, 512), BF),
            pltpu.VMEM((HALF, HALF), BF),
            pltpu.VMEM((HALF, 128), F32),
            pltpu.VMEM((HALF, 128), F32),
            pltpu.VMEM((32 + blocks // 16, 256), F32),
            pltpu.VMEM((TOK, 512), F32),
            pltpu.VMEM((TOK, 512), F32),
            pltpu.VMEM((TOK, 512), F32),
            pltpu.SemaphoreType.DMA((7,)),
        ],
        compiler_params=limit(12),
        name="pack",
    )(
        index,
        core,
        *(
            pltpu.with_memory_space_constraint(array, pltpu.HBM)
            for array in (
                query_rows,
                key_rows,
                value_rows,
                jnp.asarray(tables["perm"], BF),
                jnp.asarray(tables["cos"]),
                jnp.asarray(tables["sin"]),
                jnp.asarray(tables["anchors"]),
            )
        ),
    )
    following = [(s, (s // GROUP + 1) * GROUP + ((s % GROUP) ^ 4)) for s in range(blocks - GROUP)]
    own = lax.all_to_all(send_kv, ("b", "x"), 0, 0, tiled=True)
    halo = lax.ppermute(own, SP, following)
    send_q, _ = lax.optimization_barrier((send_q, own))
    packed = lax.all_to_all(send_q, ("b", "x"), 0, 0, tiled=True)
    weight, _ = lax.optimization_barrier((out_weight, packed))
    other_weight = lax.ppermute(weight, "tp", [(0, 1), (1, 0)])
    state = jax.ShapeDtypeStruct((16, HALF, 128), F32)
    rows16 = pltpu.VMEM((16, HALF, 128), BF)
    acc, top, qs = pl.pallas_call(
        own_kernel,
        in_specs=[vmem()] * 2,
        out_specs=[vmem()] * 3,
        out_shape=[state, state, jax.ShapeDtypeStruct((16, HALF, 128), BF)],
        scratch_shapes=[
            pltpu.VMEM((3, 128, 128), F32),
            pltpu.VMEM((3, 128, 128), F32),
            rows16,
            rows16,
            pltpu.VMEM((16, 128, 128), F32),
            pltpu.VMEM((16, 128, 256), F32),
            pltpu.VMEM((16, 128, 256), F32),
            pltpu.VMEM((16, 128, 128), BF),
            pltpu.VMEM((16, 128, 256), BF),
            pltpu.VMEM((16, 128, 256), BF),
        ],
        compiler_params=limit(24),
        cost_estimate=pl.CostEstimate(flops=20 * 10**9, bytes_accessed=2 * 2**20, transcendentals=0),
        name="attend_own",
    )(own, packed)
    back = pl.pallas_call(
        halo_kernel,
        in_specs=[smem] + [vmem()] * 5,
        out_specs=vmem(),
        out_shape=jax.ShapeDtypeStruct((2 * GROUP, 64, 128), BF),
        scratch_shapes=[
            pltpu.VMEM((3, 128, 128), F32),
            rows16,
            rows16,
            pltpu.VMEM((16, HALF, 128), F32),
            pltpu.VMEM((16, 128, 128), F32),
            pltpu.VMEM((4, 128, 128), F32),
            pltpu.VMEM((128, 128), F32),
            pltpu.VMEM((16, 128, 128), BF),
            pltpu.VMEM((4, 128, 128), BF),
            pltpu.VMEM((128, 128), BF),
        ],
        compiler_params=limit(16),
        cost_estimate=pl.CostEstimate(flops=4 * 10**9, bytes_accessed=2 * 2**20, transcendentals=0),
        name="attend_halo",
    )(index, halo, acc, top, qs, jnp.asarray(tables["perm"].T, BF))
    back, other_weight = lax.optimization_barrier((back, other_weight))
    rows = lax.all_to_all(back, ("b", "x", "tp"), 0, 0, tiled=True)
    return pl.pallas_call(
        project_kernel,
        in_specs=[smem] * 2 + [vmem()] * 3,
        out_specs=hbm,
        out_shape=pltpu.HBM((TOK // 2, 2048), BF),
        scratch_shapes=[
            pltpu.VMEM((2, TOK // 2, 512), BF),
            pltpu.VMEM((TOK // 2, 2048), BF),
            pltpu.SemaphoreType.DMA((4,)),
        ],
        compiler_params=limit(16),
        name="project",
    )(index, core, rows, out_weight, other_weight)


def solution(mesh):
    blocks = mesh.shape["sp"]
    fine = Mesh(mesh.devices.reshape(blocks // 16, 2, 2, 4, 2), SP + ("tp",))
    return jax.shard_map(
        functools.partial(per_device, blocks=blocks),
        mesh=fine,
        in_specs=(P(SP, "tp"), P(SP, "tp"), P(SP, "tp"), P("tp", None)),
        out_specs=P(SP + ("tp",), None),
        check_vma=False,
    )
```

time: 55.8 us -> 55.7 us (level)
  waiting for transfers between devices: 6.65 us -> 7.8 us
  local copies, waits for them, and re-layouts: 1.14 us -> 0.01 us
    ppermute x1, waiting for transfers between devices: 4.71 us -> 5.99 us  [per_device(): halo = lax.ppermute(own, SP, following)]
    unnamed x6 -> x4, local copies, waits for them, and re-layouts: 1.14 us -> 0.01 us
where the time goes in v6:
time: 55.7 us; the launch traced here: 55.3 us
  blocking collectives  27.5 us (49%)
  starting transfers between devices  10.7 us (19%)
  Pallas kernels  9.26 us (17%)
  waiting for transfers between devices  7.8 us (14%)
    all_to_all x1, blocking collectives, per_device(): own = lax.all_to_all(send_kv, ('b', 'x'), 0, 0, tiled=True)  15.2 us
    all_to_all x1, blocking collectives, per_device(): rows = lax.all_to_all(back, ('b', 'x', 'tp'), 0, 0, tiled=True)  12.3 us
    ppermute x1, waiting for transfers between devices, per_device(): halo = lax.ppermute(own, SP, following)  5.99 us
    ppermute x1, starting transfers between devices, per_device(): halo = lax.ppermute(own, SP, following)  5.39 us
    all_to_all x1, starting transfers between devices, per_device(): packed = lax.all_to_all(send_q, ('b', 'x'), 0, 0, tiled=True)  3.41 us
    pallas_call x1, Pallas kernels, per_device(): pl.pallas_call(pack_kernel, in_specs=[smem] * 2 + [hbm] * 7, out_specs=[v...  3.41 us
    pallas_call x1, Pallas kernels, per_device(): pl.pallas_call(own_kernel, in_specs=[vmem()] * 2, out_specs=[vmem()] * 3,...  2.61 us
    ppermute x1, starting transfers between devices, per_device(): other_weight = lax.ppermute(weight, 'tp', [(0, 1), (1, 0)])  1.91 us
  transfers between devices with their start and end apart: 3, of which 2 were waited for; matrix products, arithmetic and copies ran while one was open for 0% of the time, Pallas kernels for 8%

profile of v6, /device:TPU:256, one launch (start us, length us, event | category | flops | bytes accessed | tf_op | source)
XLA Modules:
  0.0 55.3 jit_solution(6997891346863475461)
XLA Ops:
  0.0 0.0 copy-start
  0.0 3.4 %pack.1 = (bf16[8,256,128]{2,1,0:T(8,128)(2,1)S(1)}, bf16[8,128,128]{2,1,0:T(8,128)(2,1)}) custom-call(s32[1]{0:T(128)} %bitcast.index_ref, s32[1]{0:T(128)} %bitcast.1.core_ref, bf16[256,512]{1,0:T(8,128)(2,1)} %q_hbm.1, bf16[256,512]{1,0:T(8,128)(2,1)} %k_hbm.1, bf16[256,512]{1,0:T(8,128)(2,1)} %v_hbm.1, bf16[128,128]{1,0:T(8,128)(2,1)} %constant.36.clone.perm_hbm, ...), custom_call_target="tpu_custom_call" | custom-call | tf_op jit(solution)/shard_map/pack/pallas_call | solution.py:288
  3.4 15.2 %all_to_all.15.own_ref = bf16[8,256,128]{2,1,0:T(8,128)(2,1)S(1)} all-to-all(bf16[8,256,128]{2,1,0:T(8,128)(2,1)S(1)} %get-tuple-element.14), channel_id=1, replica_groups=mesh['z'=16,'g'=2,'b'=2,'x'=4,'tp'=2] {'b','x'}, dimensions={0} | all-to-all | bytes 1048576 | tf_op jit(solution)/shard_map/all_to_all | solution.py:328
  18.6 3.4 %all-to-all-start.1 = ((bf16[8,128,128]{2,1,0:T(8,128)(2,1)}), bf16[8,128,128]{2,1,0:T(8,128)(2,1)S(1)}, u32[]{:S(2)}, u32[]{:S(2)}) async-start(bf16[8,128,128]{2,1,0:T(8,128)(2,1)} %get-tuple-element.16), calls=%async_computation.1 | async-start | bytes 524288 | tf_op jit(solution)/shard_map/all_to_all | solution.py:331
  22.0 0.0 copy-start.1
  22.0 5.4 %collective-permute-start = (bf16[8,256,128]{2,1,0:T(8,128)(2,1)S(1)}, bf16[8,256,128]{2,1,0:T(8,128)(2,1)S(1)}, u32[]{:S(2)}, u32[]{:S(2)}) collective-permute-start(bf16[8,256,128]{2,1,0:T(8,128)(2,1)S(1)} %all_to_all.15.own_ref), channel_id=1, source_target_pairs={{0,24},{2,26},{4,28},{6,30},{8,16},{10,18},{12,20},{14,22},{16,40}... | collective-permute-start | bytes 1572872 | tf_op jit(solution)/shard_map/ppermute | solution.py:329
  27.4 1.8 %all-to-all-done.1.packed_ref = bf16[8,128,128]{2,1,0:T(8,128)(2,1)S(1)} async-done(((bf16[8,128,128]{2,1,0:T(8,128)(2,1)}), bf16[8,128,128]{2,1,0:T(8,128)(2,1)S(1)}, u32[]{:S(2)}, u32[]{:S(2)}) %all-to-all-start.1) | async-done | bytes 262176 | tf_op jit(solution)/shard_map/all_to_all | solution.py:331
  29.2 0.0 copy-done
  29.3 1.9 %collective-permute-start.1 = (bf16[512,2048]{1,0:T(8,128)(2,1)S(1)}, bf16[512,2048]{1,0:T(8,128)(2,1)S(1)}, u32[]{:S(2)}, u32[]{:S(2)}) collective-permute-start(bf16[512,2048]{1,0:T(8,128)(2,1)S(1)} %copy-done), channel_id=1, source_target_pairs={{0,1},{1,0},{2,3},{3,2},{4,5},{5,4},{6,7},{7,6},{8,9},{9,8},{10,11... | collective-permute-start | bytes 6291464 | tf_op jit(solution)/shard_map/ppermute | solution.py:333
  31.2 2.6 %attend_own.1 = (f32[16,128,128]{2,1,0:T(8,128)S(1)}, f32[16,128,128]{2,1,0:T(8,128)S(1)}, bf16[16,128,128]{2,1,0:T(8,128)(2,1)S(1)}) custom-call(bf16[8,256,128]{2,1,0:T(8,128)(2,1)S(1)} %all_to_all.15.own_ref, bf16[8,128,128]{2,1,0:T(8,128)(2,1)S(1)} %all-to-all-done.1.packed_ref), custom_call_target="tpu_custom_call" | custom-call | flops 20000000000 | bytes 2097152 | tf_op jit(solution)/shard_map/attend_own/pallas_call | solution.py:336
  33.8 6.0 %collective-permute-done.halo_ref = bf16[8,256,128]{2,1,0:T(8,128)(2,1)S(1)} collective-permute-done((bf16[8,256,128]{2,1,0:T(8,128)(2,1)S(1)}, bf16[8,256,128]{2,1,0:T(8,128)(2,1)S(1)}, u32[]{:S(2)}, u32[]{:S(2)}) %collective-permute-start) | collective-permute-done | bytes 524320 | tf_op jit(solution)/shard_map/ppermute | solution.py:329
  39.8 0.0 copy-done.1
  39.8 1.7 %attend_halo.1 = bf16[16,64,128]{2,1,0:T(8,128)(2,1)S(1)} custom-call(s32[1]{0:T(128)} %bitcast.index_ref, bf16[8,256,128]{2,1,0:T(8,128)(2,1)S(1)} %collective-permute-done.halo_ref, f32[16,128,128]{2,1,0:T(8,128)S(1)} %get-tuple-element.17.acc_ref, f32[16,128,128]{2,1,0:T(8,128)S(1)} %get-tuple-element.18.top_ref, ...), custom_call_target="tpu_custom_call" | custom-call | flops 4000000000 | bytes 2097152 | tf_op jit(solution)/shard_map/attend_halo/pallas_call | solution.py:357
  41.5 0.0 collective-permute-done.1.other_ref
  41.6 12.3 %all_to_all.16.rows_ref = bf16[16,64,128]{2,1,0:T(8,128)(2,1)S(1)} all-to-all(bf16[16,64,128]{2,1,0:T(8,128)(2,1)S(1)} %attend_halo.1), channel_id=1, replica_groups=mesh['z'=16,'g'=2,'b'=2,'x'=4,'tp'=2] {'b','x','tp'}, dimensions={0} | all-to-all | bytes 524288 | tf_op jit(solution)/shard_map/all_to_all | solution.py:379
  53.8 1.5 %project.1 = bf16[128,2048]{1,0:T(8,128)(2,1)} custom-call(s32[1]{0:T(128)} %bitcast.index_ref, s32[1]{0:T(128)} %bitcast.1.core_ref, bf16[16,64,128]{2,1,0:T(8,128)(2,1)S(1)} %all_to_all.16.rows_ref, bf16[512,2048]{1,0:T(8,128)(2,1)S(1)} %copy-done, bf16[512,2048]{1,0:T(8,128)(2,1)S(1)} %collective-permute-done.1.other_ref), custom_call_target="tpu_custom_call" | custom-call | tf_op jit(solution)/shard_map/project/pallas_call | solution.py:380
Async XLA Ops:
  0.0 29.3 %copy-start = (bf16[512,2048]{1,0:T(8,128)(2,1)S(1)}, bf16[512,2048]{1,0:T(8,128)(2,1)}, u32[]{:S(2)}) copy-start(bf16[512,2048]{1,0:T(8,128)(2,1)} %own_ref.1) | copy-start | bytes 6291460
  18.6 10.6 %all-to-all-start.1 = ((bf16[8,128,128]{2,1,0:T(8,128)(2,1)}), bf16[8,128,128]{2,1,0:T(8,128)(2,1)S(1)}, u32[]{:S(2)}, u32[]{:S(2)}) async-start(bf16[8,128,128]{2,1,0:T(8,128)(2,1)} %get-tuple-element.16), calls=%async_computation.1 | async-start | bytes 524288 | tf_op jit(solution)/shard_map/all_to_all | solution.py:331
  22.0 17.8 %copy-start.1 = (bf16[128,128]{1,0:T(8,128)(2,1)S(1)}, bf16[128,128]{1,0:T(8,128)(2,1)}, u32[]{:S(2)}) copy-start(bf16[128,128]{1,0:T(8,128)(2,1)} %constant.40.clone.perm_ref) | copy-start | bytes 98308
  22.0 17.7 %collective-permute-start = (bf16[8,256,128]{2,1,0:T(8,128)(2,1)S(1)}, bf16[8,256,128]{2,1,0:T(8,128)(2,1)S(1)}, u32[]{:S(2)}, u32[]{:S(2)}) collective-permute-start(bf16[8,256,128]{2,1,0:T(8,128)(2,1)S(1)} %all_to_all.15.own_ref), channel_id=1, source_target_pairs={{0,24},{2,26},{4,28},{6,30},{8,16},{10,18},{12,20},{14,22},{16,40}... | collective-permute-start | bytes 1572872 | tf_op jit(solution)/shard_map/ppermute | solution.py:329
  29.3 12.3 %collective-permute-start.1 = (bf16[512,2048]{1,0:T(8,128)(2,1)S(1)}, bf16[512,2048]{1,0:T(8,128)(2,1)S(1)}, u32[]{:S(2)}, u32[]{:S(2)}) collective-permute-start(bf16[512,2048]{1,0:T(8,128)(2,1)S(1)} %copy-done), channel_id=1, source_target_pairs={{0,1},{1,0},{2,3},{3,2},{4,5},{5,4},{6,7},{7,6},{8,9},{9,8},{10,11... | collective-permute-start | bytes 6291464 | tf_op jit(solution)/shard_map/ppermute | solution.py:333
